TPU v7x, 512 devices: a whole 4x8x8 slice. The times are simulated.
512 devices in a mesh: ep: 32 (over z, x), tp: 16 (over y, core).
Axes of the slice: x: 4, y: 8, z: 8, core: 2. Of those that a mesh axis runs over, the one named last changes fastest.
Arguments:
- tokens: bfloat16 [8192, 2048], P('ep', 'tp'), may hold values from -6 to 6
- row_ids: int32 [8192, 16], P('ep'), may hold values from 0 to 131071, as said below
- row_gates: float32 [8192, 16], P('ep'), may hold values from 0.02 to 0.5
- key_table: bfloat16 [131072, 2048], P('ep', 'tp'), may hold values from -0.125 to 0.125
- value_table: bfloat16 [131072, 2048], P('ep', 'tp'), may hold values from -14 to 14
- norm_gain: float32 [2048], P('tp'), may hold values from 0.1 to 1.9
Outputs:
- output: bfloat16 [8192, 2048], P('ep', 'tp')
Inputs may be any that keep to these rules, and one draw needn't show every extreme that they name: `row_ids`: table row r belongs to index r // 4096 of ep. The 256 tokens of one index of ep choose at most 384 rows belonging to any one index, exactly 384 from some index, and at least one from every index.
All inputs are finite; a program needn't handle non-finite values.
Results may differ from a plain program's by a relative error of at most 0.0065.
Values may be sent and summed in bfloat16 or wider, within the bound.
No kernel may reach another device: no remote copies, remote signals or barrier semaphores. Data moves between devices by JAX's collectives and lax.ppermute only.
A program may use at most 64 MiB of HBM per device.

v0:
```python
import jax
import jax.numpy as jnp
from jax import lax
from jax.sharding import PartitionSpec as P

D = 2048


def items_in_groups(value, axis, split_dim, concat_dim, work, item_dim, out_dim):
    items = jax.tree.leaves(value)[0].shape[item_dim]
    count = 2 if items % 2 == 0 else 1
    outs = []
    for k in range(count):
        group = jax.tree.map(
            lambda a: lax.slice_in_dim(
                a, k * (items // count), (k + 1) * (items // count), axis=item_dim
            ),
            value,
        )
        outs.append(
            work(
                lax.all_to_all(
                    group, axis, split_axis=split_dim, concat_axis=concat_dim, tiled=True
                )
            )
        )
    return jax.tree.map(lambda *parts: jnp.concatenate(parts, axis=out_dim), *outs)


def over_pieces(value, axis):
    return lax.all_gather(value, axis).sum(0)


def copy_for_each(value, axis):
    length = lax.axis_size(axis)
    return lax.all_to_all(
        jnp.broadcast_to(value[None], (length, *value.shape)), axis, 0, 0, tiled=True
    )


def of_everyone(value, axis):
    everything = copy_for_each(value, axis)
    return jnp.sum(everything, axis=0)


def slot_layout(row_ids, row_gates, exp_dev, n_ep, cap):
    tok_dev, picks = row_ids.shape
    total = tok_dev * picks
    flat = row_ids.reshape(total)
    owner = flat // exp_dev
    local = flat - owner * exp_dev
    onehot = (owner[:, None] == jnp.arange(n_ep, dtype=jnp.int32)[None, :]).astype(jnp.int32)
    before = jnp.cumsum(onehot, axis=0) - onehot
    place = jnp.sum(before * onehot, axis=1)
    target = owner * cap + place
    source = (
        jnp.full((n_ep * cap,), total, jnp.int32).at[target].set(jnp.arange(total, dtype=jnp.int32))
    )
    valid = source < total
    safe = jnp.minimum(source, total - 1)
    token_index = jnp.where(valid, safe // picks, tok_dev)
    gate_slot = jnp.where(valid, row_gates.reshape(total)[safe], 0.0)
    send_local = jnp.where(valid, local[safe], 0).reshape(n_ep, cap)
    return (token_index, gate_slot, send_local)


def body(tokens, row_ids, row_gates, key_table, value_table, norm_gain):
    tok_dev, width = tokens.shape
    picks = row_ids.shape[1]
    exp_dev = key_table.shape[0]
    n_ep = lax.axis_size("ep")
    cap = 3 * tok_dev * picks // n_ep
    slots = n_ep * cap
    joined = jnp.concatenate([key_table, value_table], axis=1)
    tok_iota = jnp.arange(tok_dev, dtype=jnp.int32)
    token_index, gate_slot, send_local = slot_layout(row_ids, row_gates, exp_dev, n_ep, cap)

    def supply(wanted):
        return lax.all_to_all(joined[wanted], "ep", split_axis=0, concat_axis=0, tiled=True)

    back = items_in_groups(send_local, "ep", 0, 0, supply, 1, 1).reshape(slots, 2 * width)
    placing = (token_index[:, None] == tok_iota[None, :]).astype(jnp.bfloat16)
    slot_rows = jnp.dot(placing, tokens, preferred_element_type=jnp.float32).astype(jnp.bfloat16)
    partial_value = jnp.einsum(
        "si,si->s", slot_rows, back[:, :width], preferred_element_type=jnp.float32
    )
    score = over_pieces(partial_value, "tp")
    hidden = jax.nn.gelu(score, approximate=False) * gate_slot
    combine = jnp.where(token_index[None, :] == tok_iota[:, None], hidden[None, :], 0.0)
    mixed = jnp.dot(
        combine,
        back[:, width:].astype(jnp.float32),
        precision=lax.Precision.HIGHEST,
        preferred_element_type=jnp.float32,
    )
    squares = of_everyone(jnp.sum(mixed * mixed, axis=1), "tp")
    strength = squares / D
    return (mixed * lax.rsqrt(strength + 1e-06)[:, None] * norm_gain).astype(jnp.bfloat16)


def solution(mesh):
    in_specs = (P("ep", "tp"), P("ep", None), P("ep", None), P("ep", "tp"), P("ep", "tp"), P("tp"))
    out_specs = P("ep", "tp")
    return jax.shard_map(body, mesh=mesh, in_specs=in_specs, out_specs=out_specs, check_vma=False)
```

profile of v0, /device:TPU:1, one launch (start us, length us, event | category | flops | bytes accessed | tf_op | source)
XLA Modules:
  0.0 360.9 jit_solution(5727772682972233227)
XLA Ops:
  0.0 0.8 copy.25
  0.9 0.1 reshape.211
  1.0 0.1 reshape.210
  1.1 0.1 reshape.209
  1.2 0.1 fusion.13
  1.3 9.2 %reduce-window.6 = s32[32,32,128]{2,1,0:T(8,128)S(1)} reduce-window(s32[32,32,128]{2,1,0:T(8,128)S(1)} %fusion.13, s32[]{:T(128)} %constant.45.clone.1), window={size=1x1x128 pad=0_0x0_0x127_0}, to_apply=%region_0.1 | reduce-window | flops 16646144 | bytes 1048580 | tf_op jit(solution)/shard_map/reduce-window
  10.5 0.8 slice_reduce_fusion
  11.3 0.2 reduce-window.9
  11.5 0.2 broadcast_add_fusion
  11.7 0.4 fusion.12
  12.1 0.1 compare_select_fusion.2
  12.2 15.5 %scatter_custom_fusion = s32[12288]{0:T(1024)S(1)} fusion(s32[4096]{0:T(1024)S(1)} %bitcast.38, s32[4096]{0:T(1024)S(1)} %iota.18, s32[]{:T(128)} %constant.43.clone.1), kind=kCustom, calls=%fused_computation.79 | custom fusion | bytes 49156 | tf_op jit(solution)/shard_map/scatter | solution.py:57
  27.8 0.0 copy-start.2
  27.8 68.0 %gather_fusion = s32[12288]{0:T(1024)S(1)} fusion(s32[4096]{0:T(1024)S(1)} %get-tuple-element.9, s32[12288]{0:T(1024)S(1)} %get-tuple-element.6), kind=kCustom, calls=%fused_computation | custom fusion | bytes 147456 | tf_op jit(solution)/shard_map/gather | solution.py:63
  95.9 0.1 fusion.37
  96.0 0.7 copy.28
  96.6 13.7 %all-to-all-start.2 = ((s32[32,1,192]{2,1,0:T(1,128)}), s32[32,1,192]{2,1,0:T(1,128)S(1)}, u32[]{:S(2)}, u32[]{:S(2)}) async-start(s32[32,1,192]{2,1,0:T(1,128)} %copy.28), calls=%async_computation.2 | async-start | bytes 65536 | tf_op jit(solution)/shard_map/all_to_all | solution.py:22
  110.4 0.2 constant_dynamic-update-slice_fusion.1
  110.5 1.5 constant_dynamic-update-slice_fusion
  112.0 0.6 all_to_all.26
  112.6 6.4 %all-to-all-done.2 = s32[32,1,192]{2,1,0:T(1,128)S(1)} async-done(((s32[32,1,192]{2,1,0:T(1,128)}), s32[32,1,192]{2,1,0:T(1,128)S(1)}, u32[]{:S(2)}, u32[]{:S(2)}) %all-to-all-start.2) | async-done | bytes 24608 | tf_op jit(solution)/shard_map/all_to_all | solution.py:22
  119.0 3.9 %all-to-all-start = ((s32[32,1,192]{2,1,0:T(1,128)}), s32[32,1,192]{2,1,0:T(1,128)S(1)}, u32[]{:S(2)}, u32[]{:S(2)}) async-start(s32[32,1,192]{2,1,0:T(1,128)} %all_to_all.26), calls=%async_computation | async-start | bytes 65536 | tf_op jit(solution)/shard_map/all_to_all | solution.py:22
  122.9 0.1 fusion.29
  123.0 0.1 reshape.234
  123.1 24.9 %gather_fusion.2 = bf16[6144,256]{1,0:T(8,128)(2,1)} fusion(bf16[4096,256]{1,0:T(8,128)(2,1)S(1)} %constant_dynamic-update-slice_fusion, s32[6144]{0:T(1024)S(1)} %broadcast_clamp_fusion), kind=kCustom, calls=%fused_computation.2 | custom fusion | bytes 6316032 | tf_op jit(solution)/shard_map/gather | solution.py:79
  148.0 0.0 all-to-all-done
  148.0 9.3 %all-to-all-start.3 = ((bf16[32,192,256]{2,1,0:T(8,128)(2,1)}), bf16[32,192,256]{2,1,0:T(8,128)(2,1)}, u32[]{:S(2)}, u32[]{:S(2)}) async-start(bf16[32,192,256]{2,1,0:T(8,128)(2,1)} %bitcast.31), calls=%async_computation.3 | async-start | bytes 6291456 | tf_op jit(solution)/shard_map/all_to_all | solution.py:79
  157.3 0.1 fusion.28
  157.4 0.1 reshape.226
  157.5 24.9 %gather_fusion.1 = bf16[6144,256]{1,0:T(8,128)(2,1)} fusion(bf16[4096,256]{1,0:T(8,128)(2,1)S(1)} %constant_dynamic-update-slice_fusion, s32[6144]{0:T(1024)S(1)} %broadcast_clamp_fusion.1), kind=kCustom, calls=%fused_computation.1 | custom fusion | bytes 6316032 | tf_op jit(solution)/shard_map/gather | solution.py:79
  182.4 44.4 %all-to-all-done.3 = bf16[32,192,256]{2,1,0:T(8,128)(2,1)} async-done(((bf16[32,192,256]{2,1,0:T(8,128)(2,1)}), bf16[32,192,256]{2,1,0:T(8,128)(2,1)}, u32[]{:S(2)}, u32[]{:S(2)}) %all-to-all-start.3) | async-done | bytes 3145760 | tf_op jit(solution)/shard_map/all_to_all | solution.py:79
  226.8 6.8 %all-to-all-start.1 = ((bf16[32,192,256]{2,1,0:T(8,128)(2,1)}), bf16[32,192,256]{2,1,0:T(8,128)(2,1)S(1)}, u32[]{:S(2)}, u32[]{:S(2)}) async-start(bf16[32,192,256]{2,1,0:T(8,128)(2,1)} %bitcast.32), calls=%async_computation.1 | async-start | bytes 6291456 | tf_op jit(solution)/shard_map/all_to_all | solution.py:79
  233.7 0.1 copy.29
  233.8 0.1 reshape.215
  233.9 68.0 %gather_fusion.3 = f32[12288]{0:T(1024)S(1)} fusion(f32[4096]{0:T(1024)S(1)} %reshape.215, s32[12288]{0:T(1024)S(1)} %get-tuple-element.6), kind=kCustom, calls=%fused_computation.3 | custom fusion | bytes 147456 | tf_op jit(solution)/shard_map/gather | solution.py:62
  301.9 0.4 all-to-all-done.1
  302.3 2.4 pad_maximum_fusion
  304.8 7.5 %fusion.9 = f32[12288]{0:T(1024)S(1)} fusion(bf16[12288,256]{1,0:T(8,128)(2,1)S(1)} %bitcast.33, bf16[256,128]{1,0:T(8,128)(2,1)S(1)} %copy-done, s32[12288]{0:T(1024)S(1)} %get-tuple-element.5), kind=kOutput, calls=%fused_computation.18 | convolution fusion | flops 816304128 | bytes 3309568 | tf_op jit(solution)/shard_map/dot_general | solution.py:83
  312.3 0.0 copy-done.1
  312.3 25.4 %all-gather = f32[196608]{0:T(1024)S(1)} all-gather(f32[12288]{0:T(1024)S(1)} %fusion.9), channel_id=2, replica_groups=mesh['ep'=32,'tp'=16] {'tp'}, dimensions={0}, use_global_device_ids=true | all-gather | bytes 835584 | tf_op jit(solution)/shard_map/all_gather | solution.py:31
  337.7 0.1 reshape.256
  337.9 0.1 reduce_sum.40
  338.0 0.1 fusion.19
  338.1 0.0 copy-start.4
  338.1 10.2 %multiply_reduce_fusion = (f32[256]{0:T(256)S(1)}, f32[256,128]{0,1:T(8,128)S(1)}) fusion(bf16[12288,256]{1,0:T(8,128)(2,1)} %bitcast.34, f32[12288]{0:T(1024)S(1)} %fusion.19, s32[12288]{0:T(1024)S(1)} %get-tuple-element.5), kind=kOutput, calls=%fused_computation.31 | convolution fusion | flops 4838195200 | bytes 3376128 | tf_op jit(solution)/shard_map/dot_general | solution.py:90
  348.4 11.6 %all_to_all.40 = f32[16,1,256]{2,1,0:T(1,128)S(1)} all-to-all(f32[16,1,256]{2,1,0:T(1,128)S(1)} %broadcast_in_dim.27), channel_id=1, replica_groups=mesh['ep'=32,'tp'=16] {'tp'}, dimensions={0} | all-to-all | bytes 32768 | tf_op jit(solution)/shard_map/all_to_all | solution.py:36
  360.1 0.1 multiply_convert_fusion
  360.1 0.7 copy.31
  (18 shorter events, 0.2 us)
Async XLA Ops:
  0.0 304.8 %copy-start = (bf16[256,128]{1,0:T(8,128)(2,1)S(1)}, bf16[256,128]{1,0:T(8,128)(2,1)}, u32[]{:S(2)}) copy-start(bf16[256,128]{1,0:T(8,128)(2,1)} %param.6) | copy-start | bytes 196612
  27.8 82.5 %copy-start.2 = (bf16[4096,128]{1,0:T(8,128)(2,1)S(1)}, bf16[4096,128]{1,0:T(8,128)(2,1)}, u32[]{:S(2)}) copy-start(bf16[4096,128]{1,0:T(8,128)(2,1)} %param.9) | copy-start | bytes 3145732
  96.6 22.4 %all-to-all-start.2 = ((s32[32,1,192]{2,1,0:T(1,128)}), s32[32,1,192]{2,1,0:T(1,128)S(1)}, u32[]{:S(2)}, u32[]{:S(2)}) async-start(s32[32,1,192]{2,1,0:T(1,128)} %copy.28), calls=%async_computation.2 | async-start | bytes 65536 | tf_op jit(solution)/shard_map/all_to_all | solution.py:22
  119.0 29.0 %all-to-all-start = ((s32[32,1,192]{2,1,0:T(1,128)}), s32[32,1,192]{2,1,0:T(1,128)S(1)}, u32[]{:S(2)}, u32[]{:S(2)}) async-start(s32[32,1,192]{2,1,0:T(1,128)} %all_to_all.26), calls=%async_computation | async-start | bytes 65536 | tf_op jit(solution)/shard_map/all_to_all | solution.py:22
  148.0 78.8 %all-to-all-start.3 = ((bf16[32,192,256]{2,1,0:T(8,128)(2,1)}), bf16[32,192,256]{2,1,0:T(8,128)(2,1)}, u32[]{:S(2)}, u32[]{:S(2)}) async-start(bf16[32,192,256]{2,1,0:T(8,128)(2,1)} %bitcast.31), calls=%async_computation.3 | async-start | bytes 6291456 | tf_op jit(solution)/shard_map/all_to_all | solution.py:79
  226.8 6.8 %copy-start.3 = (f32[256,16]{0,1:T(8,128)S(1)}, f32[256,16]{0,1:T(8,128)}, u32[]{:S(2)}) copy-start(f32[256,16]{0,1:T(8,128)} %param.8) | copy-start | bytes 49156
  226.8 75.5 %all-to-all-start.1 = ((bf16[32,192,256]{2,1,0:T(8,128)(2,1)}), bf16[32,192,256]{2,1,0:T(8,128)(2,1)S(1)}, u32[]{:S(2)}, u32[]{:S(2)}) async-start(bf16[32,192,256]{2,1,0:T(8,128)(2,1)} %bitcast.32), calls=%async_computation.1 | async-start | bytes 6291456 | tf_op jit(solution)/shard_map/all_to_all | solution.py:79
  304.8 7.5 %copy-start.1 = (bf16[32,384,256]{2,1,0:T(8,128)(2,1)}, bf16[32,384,256]{2,1,0:T(8,128)(2,1)S(1)}, u32[]{:S(2)}) copy-start(bf16[32,384,256]{2,1,0:T(8,128)(2,1)S(1)} %pad_maximum_fusion) | copy-start | bytes 18874372
  338.1 21.9 %copy-start.4 = (f32[128]{0:T(128)S(1)}, f32[128]{0:T(128)}, u32[]{:S(2)}) copy-start(f32[128]{0:T(128)} %param.11) | copy-start | bytes 1540
where the time goes:
time: 361 us
  local copies, waits for them, and re-layouts  208 us (58%)
  waiting for transfers between devices  51.2 us (14%)
  blocking collectives  37.1 us (10%)
  starting transfers between devices  33.7 us (9%)
  matrix products  17.7 us (5%)
  other arithmetic  13.2 us (4%)
    gather x1, local copies, waits for them, and re-layouts, slot_layout(): send_local = jnp.where(valid, local[safe], 0).reshape(n_ep, cap)  68 us
    gather x1, local copies, waits for them, and re-layouts, slot_layout(): gate_slot = jnp.where(valid, row_gates.reshape(total)[safe], 0.0)  68 us
    gather x2, local copies, waits for them, and re-layouts, supply(): joined[wanted]  49.8 us
    all_to_all x2, waiting for transfers between devices, supply(): lax.all_to_all(joined[wanted], 'ep', split_axis=0, concat_axis=0, tiled=T...  44.8 us
    all_gather x1, blocking collectives, over_pieces(): return lax.all_gather(value, axis).sum(0)  25.4 us
    all_to_all x2, starting transfers between devices, items_in_groups(): lax.all_to_all(group, axis, split_axis=split_dim, concat_axis=concat_dim,...  17.6 us
    all_to_all x2, starting transfers between devices, supply(): lax.all_to_all(joined[wanted], 'ep', split_axis=0, concat_axis=0, tiled=T...  16.1 us
    scatter x1, local copies, waits for them, and re-layouts, slot_layout(): jnp.full((n_ep * cap,), total, jnp.int32).at[target]  15.5 us
  transfers between devices with their start and end apart: 4, of which 3 were waited for; matrix products, arithmetic and copies ran while one was open for 33% of the time, Pallas kernels for 0%

commit v1 on v0

v1 whole, which is shorter than its diff:
```python
import jax
import jax.numpy as jnp
from jax import lax
from jax.experimental import pallas as pl
from jax.experimental.pallas import tpu as pltpu
from jax.sharding import PartitionSpec as P

D = 2048
LANES = 128
INTERPRET = False


def bucket_kernel(ids_ref, gates_ref, out_ref, a_ref, b_ref, *, n_ep, cap, shift):
    picks, tok = ids_ref.shape
    before = jnp.where(
        lax.broadcasted_iota(jnp.int32, (tok, tok), 0)
        < lax.broadcasted_iota(jnp.int32, (tok, tok), 1),
        1.0,
        0.0,
    ).astype(jnp.bfloat16)
    token_no = (lax.broadcasted_iota(jnp.int32, (1, tok), 1) + 1).astype(jnp.float32)
    owners = lax.broadcasted_iota(jnp.int32, (n_ep, tok), 0)
    slots = lax.broadcasted_iota(jnp.int32, (cap, tok), 0)
    base = jnp.zeros((n_ep, 1), jnp.float32)
    for k in range(picks):
        ids = ids_ref[k : k + 1, :]
        mine = (ids >> shift) == owners
        hot = jnp.where(mine, 1.0, 0.0)
        rank = base + jnp.dot(
            hot.astype(jnp.bfloat16), before, preferred_element_type=jnp.float32
        )
        place = jnp.sum(jnp.where(mine, rank, 0.0), axis=0, keepdims=True).astype(jnp.int32)
        base = base + jnp.sum(hot, axis=1, keepdims=True)
        b_ref[:, k * tok : (k + 1) * tok] = jnp.where(slots == place, 1.0, 0.0).astype(
            jnp.bfloat16
        )
        local = ids & ((1 << shift) - 1)
        gate = gates_ref[k : k + 1, :]
        gate_hi = gate.astype(jnp.bfloat16).astype(jnp.float32)
        gate_mid = (gate - gate_hi).astype(jnp.bfloat16).astype(jnp.float32)
        gate_lo = gate - gate_hi - gate_mid
        values = (
            token_no,
            (local >> 4).astype(jnp.float32),
            (local & 15).astype(jnp.float32),
            gate_hi,
            gate_mid,
            gate_lo,
        )
        for c, value in enumerate(values):
            a_ref[c * n_ep : (c + 1) * n_ep, k * tok : (k + 1) * tok] = jnp.where(
                mine, value, 0.0
            ).astype(jnp.bfloat16)
    res = lax.dot_general(
        a_ref[...], b_ref[...], (((1,), (1,)), ((), ())), preferred_element_type=jnp.float32
    )
    part = [res[c * n_ep : (c + 1) * n_ep] for c in range(6)]
    code = part[0] * float(1 << shift) + (part[1] * 16.0 + part[2])
    gates = part[3] + part[4] + part[5]
    chunks = cap // LANES
    out_ref[...] = jnp.zeros(out_ref.shape, jnp.float32)
    for j in range(chunks):
        out_ref[:, j, :] = code[:, j * LANES : (j + 1) * LANES]
        out_ref[:, chunks + j, :] = gates[:, j * LANES : (j + 1) * LANES]


def widen(table_ref, wide_ref):
    step = 256

    def one(i, carry):
        rows = pl.ds(pl.multiple_of(i * step, step), step)
        wide_ref[rows, :] = table_ref[rows, :].astype(jnp.float32)
        return carry

    lax.fori_loop(0, table_ref.shape[0] // step, one, 0)


def take_rows(rows_ref, line, wide_ref, rows_out):
    for s in range(LANES):
        rows_out[pl.ds(s, 1), :] = wide_ref[pl.ds(rows_ref[line, s], 1), :]


def score_kernel(rows_ref, count_ref, place_ref, tok_ref, key_ref, out_ref, wide, picked):
    n_ep, tok, _ = tok_ref.shape
    chunks = place_ref.shape[0] // n_ep
    widen(key_ref, wide)
    out_ref[...] = jnp.zeros(out_ref.shape, jnp.float32)
    token_of = lax.broadcasted_iota(jnp.int32, (tok, LANES), 0)

    def block(i, carry):
        def chunk(c, inner):
            line = i * chunks + c
            take_rows(rows_ref, line, wide, picked)
            prod = lax.dot_general(
                tok_ref[i],
                picked[...].astype(jnp.bfloat16),
                (((1,), (1,)), ((), ())),
                preferred_element_type=jnp.float32,
            )
            here = place_ref[pl.ds(line, 1), :] == token_of
            out_ref[pl.ds(line, 1), :] = jnp.sum(
                jnp.where(here, prod, 0.0), axis=0, keepdims=True
            )
            return inner

        return lax.fori_loop(0, (count_ref[i] + LANES - 1) // LANES, chunk, carry)

    lax.fori_loop(0, n_ep, block, 0)


def combine_kernel(rows_ref, count_ref, place_ref, hidden_ref, value_ref, out_ref, wide, picked, acc):
    n_ep, tok, _ = out_ref.shape
    chunks = place_ref.shape[0] // n_ep
    widen(value_ref, wide)
    token_of = lax.broadcasted_iota(jnp.int32, (tok, LANES), 0)

    def block(i, carry):
        acc[...] = jnp.zeros(acc.shape, jnp.float32)

        def chunk(c, inner):
            line = i * chunks + c
            take_rows(rows_ref, line, wide, picked)
            here = place_ref[pl.ds(line, 1), :] == token_of
            weight = jnp.where(here, hidden_ref[pl.ds(line, 1), :], 0.0)
            high = weight.astype(jnp.bfloat16)
            low = (weight - high.astype(jnp.float32)).astype(jnp.bfloat16)
            rows = picked[...].astype(jnp.bfloat16)
            acc[...] += jnp.dot(high, rows, preferred_element_type=jnp.float32) + jnp.dot(
                low, rows, preferred_element_type=jnp.float32
            )
            return inner

        lax.fori_loop(0, (count_ref[i] + LANES - 1) // LANES, chunk, 0)
        out_ref[i] = acc[...].astype(out_ref.dtype)
        return carry

    lax.fori_loop(0, n_ep, block, 0)


def vmem():
    return pl.BlockSpec(memory_space=pltpu.VMEM)


def smem():
    return pl.BlockSpec(memory_space=pltpu.SMEM)


def body(tokens, row_ids, row_gates, key_table, value_table, norm_gain):
    tok, width = tokens.shape
    picks = row_ids.shape[1]
    exp_dev = key_table.shape[0]
    n_ep = lax.axis_size("ep")
    cap = 3 * tok * picks // n_ep
    chunks = cap // LANES
    shift = exp_dev.bit_length() - 1
    lines = n_ep * chunks

    spread = lax.all_to_all(
        jnp.broadcast_to(tokens[None], (n_ep, tok, width)), "ep", 0, 0, tiled=True
    )
    listed = pl.pallas_call(
        lambda *refs: bucket_kernel(*refs, n_ep=n_ep, cap=cap, shift=shift),
        out_shape=jax.ShapeDtypeStruct((n_ep, 8, LANES), jnp.float32),
        in_specs=[vmem(), vmem()],
        out_specs=vmem(),
        scratch_shapes=[
            pltpu.VMEM((6 * n_ep, tok * picks), jnp.bfloat16),
            pltpu.VMEM((cap, tok * picks), jnp.bfloat16),
        ],
        interpret=INTERPRET,
        name="bucket",
    )(row_ids.T, row_gates.T)
    listed = lax.all_to_all(listed, "ep", 0, 0, tiled=True)
    codes = listed[:, :chunks].astype(jnp.int32)
    gates = listed[:, chunks : 2 * chunks].reshape(lines, LANES)
    rows = (codes & (exp_dev - 1)).reshape(lines, LANES)
    place = ((codes >> shift) - 1).reshape(lines, LANES)
    count = jnp.sum((codes > 0).astype(jnp.int32), axis=(1, 2))

    partial_score = pl.pallas_call(
        score_kernel,
        out_shape=jax.ShapeDtypeStruct((lines, LANES), jnp.float32),
        in_specs=[smem(), smem(), vmem(), vmem(), vmem()],
        out_specs=vmem(),
        scratch_shapes=[
            pltpu.VMEM((exp_dev, width), jnp.float32),
            pltpu.VMEM((LANES, width), jnp.float32),
        ],
        interpret=INTERPRET,
        name="score",
    )(rows, count, place, spread, key_table)
    score = jnp.sum(lax.all_gather(partial_score, "tp"), axis=0)
    hidden = jnp.where(place >= 0, jax.nn.gelu(score, approximate=False) * gates, 0.0)
    mixed_part = pl.pallas_call(
        combine_kernel,
        out_shape=jax.ShapeDtypeStruct((n_ep, tok, width), jnp.bfloat16),
        in_specs=[smem(), smem(), vmem(), vmem(), vmem()],
        out_specs=vmem(),
        scratch_shapes=[
            pltpu.VMEM((exp_dev, width), jnp.float32),
            pltpu.VMEM((LANES, width), jnp.float32),
            pltpu.VMEM((tok, width), jnp.float32),
        ],
        interpret=INTERPRET,
        name="combine",
    )(rows, count, place, hidden, value_table)
    back = lax.all_to_all(mixed_part, "ep", 0, 0, tiled=True)
    mixed = jnp.sum(back.astype(jnp.float32), axis=0)
    squares = jnp.sum(lax.all_gather(jnp.sum(mixed * mixed, axis=1), "tp"), axis=0)
    strength = squares / D
    return (mixed * lax.rsqrt(strength + 1e-06)[:, None] * norm_gain).astype(jnp.bfloat16)


def solution(mesh):
    in_specs = (P("ep", "tp"), P("ep", None), P("ep", None), P("ep", "tp"), P("ep", "tp"), P("tp"))
    out_specs = P("ep", "tp")
    return jax.shard_map(body, mesh=mesh, in_specs=in_specs, out_specs=out_specs, check_vma=False)
```

time: 361 us -> 207 us (0.57)
  local copies, waits for them, and re-layouts: 208 us -> 5.35 us
  blocking collectives: 37.1 us -> 120 us
  starting transfers between devices: 33.7 us -> 4.01 us
  Pallas kernels: 0 us -> 28.5 us
  matrix products: 17.7 us -> 0 us
  other arithmetic: 13.2 us -> 3.14 us
  waiting for transfers between devices: 51.2 us -> 44.6 us
    gather x4 -> x0, local copies, waits for them, and re-layouts: 186 us -> none  [the longest x1 68 us: slot_layout(): send_local = jnp.where(valid, local[safe], 0).reshape(n_ep, cap)]
    all_to_all x1 -> x2, blocking collectives: 11.6 us -> 78.9 us  [the longest x1 55.9 us: body(): back = lax.all_to_all(mixed_part, 'ep', 0, 0, tiled=True)]
    all_to_all x4 -> x1, starting transfers between devices: 33.7 us -> 4.01 us  [body(): lax.all_to_all(jnp.broadcast_to(tokens[None], (n_ep, tok, width)), 'ep',...]
    pallas_call x0 -> x3, Pallas kernels: none -> 28.5 us  [the longest x1 13.1 us: body(): pl.pallas_call(combine_kernel, out_shape=jax.ShapeDtypeStruct((n_ep, tok,...]
    dot_general x2 -> x0, matrix products: 17.7 us -> none  [the longest x1 10.2 us: body(): jnp.dot(combine, back[:, width:].astype(jnp.float32), precision=lax.Preci...]
    all_gather x1 -> x2, blocking collectives: 25.4 us -> 41.2 us  [the longest x1 24.5 us: body(): score = jnp.sum(lax.all_gather(partial_score, 'tp'), axis=0)]
    scatter x1 -> x0, local copies, waits for them, and re-layouts: 15.5 us -> none  [slot_layout(): jnp.full((n_ep * cap,), total, jnp.int32).at[target]]
    another operation x3 -> x0, other arithmetic: 9.62 us -> none
  transfers between devices with their start and end apart: 4 -> 1, of which waited for: 3 -> 1; matrix products, arithmetic and copies ran while one was open for 33% -> 1% of each run, Pallas kernels for 0% -> 0%
where the time goes in v1:
time: 207 us; the launch traced here: 206 us
  blocking collectives  120 us (58%)
  waiting for transfers between devices  44.6 us (22%)
  Pallas kernels  28.5 us (14%)
  local copies, waits for them, and re-layouts  5.35 us (3%)
  starting transfers between devices  4.01 us (2%)
  other arithmetic  3.14 us (2%)
    all_to_all x1, blocking collectives, body(): back = lax.all_to_all(mixed_part, 'ep', 0, 0, tiled=True)  55.9 us
    all_to_all x1, waiting for transfers between devices, body(): lax.all_to_all(jnp.broadcast_to(tokens[None], (n_ep, tok, width)), 'ep',...  44.6 us
    all_gather x1, blocking collectives, body(): score = jnp.sum(lax.all_gather(partial_score, 'tp'), axis=0)  24.5 us
    all_to_all x1, blocking collectives, body(): listed = lax.all_to_all(listed, 'ep', 0, 0, tiled=True)  23 us
    all_gather x1, blocking collectives, body(): lax.all_gather(jnp.sum(mixed * mixed, axis=1), 'tp')  16.7 us
    pallas_call x1, Pallas kernels, body(): pl.pallas_call(combine_kernel, out_shape=jax.ShapeDtypeStruct((n_ep, tok,...  13.1 us
    pallas_call x1, Pallas kernels, body(): pl.pallas_call(score_kernel, out_shape=jax.ShapeDtypeStruct((lines, LANES...  12.4 us
  transfers between devices with their start and end apart: 1, of which 1 were waited for; matrix products, arithmetic and copies ran while one was open for 1% of the time, Pallas kernels for 0%

profile of v1, /device:TPU:1, one launch (start us, length us, event | category | flops | bytes accessed | tf_op | source)
XLA Modules:
  0.0 205.8 jit_solution(1852077495330928499)
XLA Ops:
  0.0 3.0 %bucket.1 = f32[32,8,128]{2,1,0:T(8,128)} custom-call(s32[16,256]{1,0:T(8,128)} %bitcast.5, f32[16,256]{1,0:T(8,128)} %bitcast.6), custom_call_target="tpu_custom_call" | custom-call | tf_op jit(solution)/shard_map/bucket/pallas_call | solution.py:161
  3.0 23.0 %all_to_all.15 = f32[32,8,128]{2,1,0:T(8,128)S(1)} all-to-all(f32[32,8,128]{2,1,0:T(8,128)} %bucket.1), channel_id=1, replica_groups=mesh['ep'=32,'tp'=16] {'ep'}, dimensions={0} | all-to-all | bytes 262144 | tf_op jit(solution)/shard_map/all_to_all | solution.py:173
  26.0 2.7 %broadcast_in_dim.3 = bf16[32,256,128]{2,1,0:T(8,128)(2,1)} broadcast(bf16[256,128]{1,0:T(8,128)(2,1)} %param.6), dimensions={1,2} | broadcast | bytes 2162688 | tf_op jit(solution)/shard_map/broadcast_in_dim | solution.py:159
  28.7 4.0 %all-to-all-start.1 = ((bf16[32,256,128]{2,1,0:T(8,128)(2,1)}), bf16[32,256,128]{2,1,0:T(8,128)(2,1)S(1)}, u32[]{:S(2)}, u32[]{:S(2)}) async-start(bf16[32,256,128]{2,1,0:T(8,128)(2,1)} %broadcast_in_dim.3), calls=%async_computation.1 | async-start | bytes 4194304 | tf_op jit(solution)/shard_map/all_to_all | solution.py:158
  32.8 1.2 shift-right-arithmetic_add_fusion
  33.9 0.6 reshape.17.place_ref
  34.6 0.6 reshape.16.rows_ref
  35.2 44.6 %all-to-all-done.1.tok_ref = bf16[32,256,128]{2,1,0:T(8,128)(2,1)S(1)} async-done(((bf16[32,256,128]{2,1,0:T(8,128)(2,1)}), bf16[32,256,128]{2,1,0:T(8,128)(2,1)S(1)}, u32[]{:S(2)}, u32[]{:S(2)}) %all-to-all-start.1) | async-done | bytes 2097184 | tf_op jit(solution)/shard_map/all_to_all | solution.py:158
  79.8 0.0 copy-start
  79.8 1.3 copy-done
  81.1 0.0 copy-start.1
  81.1 12.4 %score.1 = f32[96,128]{1,0:T(8,128)} custom-call(s32[96,128]{1,0:T(8,128)} %reshape.16.rows_ref, s32[32]{0:T(128)} %get-tuple-element.6.count_ref, s32[96,128]{1,0:T(8,128)} %reshape.17.place_ref, bf16[32,256,128]{2,1,0:T(8,128)(2,1)} %copy-done, bf16[4096,128]{1,0:T(8,128)(2,1)} %key_ref.1), custom_call_target="tpu_custom_call" | custom-call | tf_op jit(solution)/shard_map/score/pallas_call | solution.py:180
  93.6 24.5 %all-gather = f32[1536,128]{1,0:T(8,128)S(1)} all-gather(f32[96,128]{1,0:T(8,128)} %score.1), channel_id=2, replica_groups=mesh['ep'=32,'tp'=16] {'tp'}, dimensions={0}, use_global_device_ids=true | all-gather | bytes 835584 | tf_op jit(solution)/shard_map/all_gather | solution.py:192
  118.1 0.0 copy-done.1
  118.1 0.7 fusion.4.hidden_ref
  118.9 13.1 %combine.1 = bf16[32,256,128]{2,1,0:T(8,128)(2,1)} custom-call(s32[96,128]{1,0:T(8,128)} %reshape.16.rows_ref, s32[32]{0:T(128)} %get-tuple-element.6.count_ref, s32[96,128]{1,0:T(8,128)} %reshape.17.place_ref, f32[96,128]{1,0:T(8,128)} %fusion.4.hidden_ref, bf16[4096,128]{1,0:T(8,128)(2,1)} %value_ref.1), custom_call_target="tpu_custom_call" | custom-call | tf_op jit(solution)/shard_map/combine/pallas_call | solution.py:194
  132.0 55.9 %all_to_all.16 = bf16[32,256,128]{2,1,0:T(8,128)(2,1)S(1)} all-to-all(bf16[32,256,128]{2,1,0:T(8,128)(2,1)} %combine.1), channel_id=1, replica_groups=mesh['ep'=32,'tp'=16] {'ep'}, dimensions={0} | all-to-all | bytes 4194304 | tf_op jit(solution)/shard_map/all_to_all | solution.py:207
  187.9 0.0 copy-start.2
  187.9 0.3 convert_reduce_fusion
  188.2 0.1 multiply_reduce_fusion
  188.3 16.7 %all-gather.2 = f32[16,1,256]{2,1,0:T(1,128)S(1)} all-gather(f32[1,1,256]{2,1,0:T(1,128)S(1)} %bitcast.7), channel_id=3, replica_groups=mesh['ep'=32,'tp'=16] {'tp'}, dimensions={0}, use_global_device_ids=true | all-gather | bytes 17408 | tf_op jit(solution)/shard_map/all_gather | solution.py:209
  205.0 0.0 copy-done.2
  205.0 0.7 multiply_convert_fusion
  (5 shorter events, 0.1 us)
Async XLA Ops:
  28.7 51.1 %all-to-all-start.1 = ((bf16[32,256,128]{2,1,0:T(8,128)(2,1)}), bf16[32,256,128]{2,1,0:T(8,128)(2,1)S(1)}, u32[]{:S(2)}, u32[]{:S(2)}) async-start(bf16[32,256,128]{2,1,0:T(8,128)(2,1)} %broadcast_in_dim.3), calls=%async_computation.1 | async-start | bytes 4194304 | tf_op jit(solution)/shard_map/all_to_all | solution.py:158
  79.8 1.4 copy-start
  81.1 37.0 %copy-start.1 = (s32[96,128]{1,0:T(8,128)S(1)}, s32[96,128]{1,0:T(8,128)}, u32[]{:S(2)}) copy-start(s32[96,128]{1,0:T(8,128)} %reshape.17.place_ref) | copy-start | bytes 147460
  187.9 17.1 %copy-start.2 = (f32[128]{0:T(128)S(1)}, f32[128]{0:T(128)}, u32[]{:S(2)}) copy-start(f32[128]{0:T(128)} %param.11) | copy-start | bytes 1540

commit v2 on v1

v2 whole, which is shorter than its diff:
```python
import jax
import jax.numpy as jnp
from jax import lax
from jax.experimental import pallas as pl
from jax.experimental.pallas import tpu as pltpu
from jax.sharding import Mesh
from jax.sharding import PartitionSpec as P

D = 2048
LANES = 128
INTERPRET = False
Z = 8
EP = ("z", "x")
TP = ("y", "core")


def bucket_kernel(ids_ref, gates_ref, out_ref, a_ref, b_ref, *, n_ep, cap, shift):
    picks, tok = ids_ref.shape
    before = jnp.where(
        lax.broadcasted_iota(jnp.int32, (tok, tok), 0)
        < lax.broadcasted_iota(jnp.int32, (tok, tok), 1),
        1.0,
        0.0,
    ).astype(jnp.bfloat16)
    token_no = (lax.broadcasted_iota(jnp.int32, (1, tok), 1) + 1).astype(jnp.float32)
    owners = lax.broadcasted_iota(jnp.int32, (n_ep, tok), 0)
    slots = lax.broadcasted_iota(jnp.int32, (cap, tok), 0)
    base = jnp.zeros((n_ep, 1), jnp.float32)
    for k in range(picks):
        ids = ids_ref[k : k + 1, :]
        mine = (ids >> shift) == owners
        hot = jnp.where(mine, 1.0, 0.0)
        rank = base + jnp.dot(
            hot.astype(jnp.bfloat16), before, preferred_element_type=jnp.float32
        )
        place = jnp.sum(jnp.where(mine, rank, 0.0), axis=0, keepdims=True).astype(jnp.int32)
        base = base + jnp.sum(hot, axis=1, keepdims=True)
        b_ref[:, k * tok : (k + 1) * tok] = jnp.where(slots == place, 1.0, 0.0).astype(
            jnp.bfloat16
        )
        local = ids & ((1 << shift) - 1)
        gate = gates_ref[k : k + 1, :]
        gate_hi = gate.astype(jnp.bfloat16).astype(jnp.float32)
        gate_mid = (gate - gate_hi).astype(jnp.bfloat16).astype(jnp.float32)
        gate_lo = gate - gate_hi - gate_mid
        values = (
            token_no,
            (local >> 4).astype(jnp.float32),
            (local & 15).astype(jnp.float32),
            gate_hi,
            gate_mid,
            gate_lo,
        )
        for c, value in enumerate(values):
            a_ref[c * n_ep : (c + 1) * n_ep, k * tok : (k + 1) * tok] = jnp.where(
                mine, value, 0.0
            ).astype(jnp.bfloat16)
    res = lax.dot_general(
        a_ref[...], b_ref[...], (((1,), (1,)), ((), ())), preferred_element_type=jnp.float32
    )
    part = [res[c * n_ep : (c + 1) * n_ep] for c in range(6)]
    code = part[0] * float(1 << shift) + (part[1] * 16.0 + part[2])
    gates = part[3] + part[4] + part[5]
    chunks = cap // LANES
    out_ref[...] = jnp.zeros(out_ref.shape, jnp.float32)
    for j in range(chunks):
        out_ref[:, j, :] = code[:, j * LANES : (j + 1) * LANES]
        out_ref[:, chunks + j, :] = gates[:, j * LANES : (j + 1) * LANES]


def widen(table_ref, wide_ref):
    step = 256

    def one(i, carry):
        rows = pl.ds(pl.multiple_of(i * step, step), step)
        wide_ref[rows, :] = table_ref[rows, :].astype(jnp.float32)
        return carry

    lax.fori_loop(0, table_ref.shape[0] // step, one, 0)


def take_rows(rows_ref, line, wide_ref, picked, out_ref):
    for s in range(LANES):
        picked[pl.ds(s, 1), :] = wide_ref[pl.ds(rows_ref[line, s], 1), :]
    out_ref[line] = picked[...].astype(out_ref.dtype)


def each_line(count_ref, chunks, start, work, finish):
    def block(i, carry):
        start(i)

        def chunk(c, inner):
            work(i, i * chunks + c)
            return inner

        lax.fori_loop(0, (count_ref[i] + LANES - 1) // LANES, chunk, 0)
        finish(i)
        return carry

    lax.fori_loop(0, count_ref.shape[0], block, 0)


def nothing(i):
    del i


def pick_kernel(
    rows_ref, count_ref, key_ref, value_ref, keys_out, values_out, wide_k, wide_v, took_k, took_v
):
    widen(key_ref, wide_k)
    widen(value_ref, wide_v)
    chunks = keys_out.shape[0] // count_ref.shape[0]

    def work(i, line):
        take_rows(rows_ref, line, wide_k, took_k, keys_out)
        take_rows(rows_ref, line, wide_v, took_v, values_out)

    each_line(count_ref, chunks, nothing, work, nothing)


def score_kernel(count_ref, place_ref, tok_ref, keys_ref, out_ref):
    n_x, n_z, tok, _ = tok_ref.shape
    chunks = place_ref.shape[0] // (n_x * n_z)
    out_ref[...] = jnp.zeros(out_ref.shape, jnp.float32)
    token_of = lax.broadcasted_iota(jnp.int32, (tok, LANES), 0)

    def work(i, line):
        prod = lax.dot_general(
            tok_ref[i % n_x, i // n_x],
            keys_ref[line],
            (((1,), (1,)), ((), ())),
            preferred_element_type=jnp.float32,
        )
        here = place_ref[pl.ds(line, 1), :] == token_of
        out_ref[pl.ds(line, 1), :] = jnp.sum(jnp.where(here, prod, 0.0), axis=0, keepdims=True)

    each_line(count_ref, chunks, nothing, work, nothing)


def combine_kernel(count_ref, place_ref, hidden_ref, values_ref, out_ref, acc):
    n_ep, tok, _ = out_ref.shape
    chunks = place_ref.shape[0] // n_ep
    token_of = lax.broadcasted_iota(jnp.int32, (tok, LANES), 0)

    def start(i):
        acc[...] = jnp.zeros(acc.shape, jnp.float32)

    def work(i, line):
        here = place_ref[pl.ds(line, 1), :] == token_of
        weight = jnp.where(here, hidden_ref[pl.ds(line, 1), :], 0.0)
        high = weight.astype(jnp.bfloat16)
        low = (weight - high.astype(jnp.float32)).astype(jnp.bfloat16)
        rows = values_ref[line]
        acc[...] += jnp.dot(high, rows, preferred_element_type=jnp.float32) + jnp.dot(
            low, rows, preferred_element_type=jnp.float32
        )

    def finish(i):
        out_ref[i] = acc[...].astype(out_ref.dtype)

    each_line(count_ref, chunks, start, work, finish)


def vmem():
    return pl.BlockSpec(memory_space=pltpu.VMEM)


def smem():
    return pl.BlockSpec(memory_space=pltpu.SMEM)


def to_each(value, axis):
    return lax.all_to_all(
        jnp.broadcast_to(value[None], (lax.axis_size(axis), *value.shape)), axis, 0, 0, tiled=True
    )


def body(tokens, row_ids, row_gates, key_table, value_table, norm_gain):
    tok, width = tokens.shape
    picks = row_ids.shape[1]
    exp_dev = key_table.shape[0]
    n_ep = lax.axis_size(EP)
    cap = 3 * tok * picks // n_ep
    chunks = cap // LANES
    shift = exp_dev.bit_length() - 1
    lines = n_ep * chunks

    spread = to_each(to_each(tokens, "z"), "x")
    listed = pl.pallas_call(
        lambda *refs: bucket_kernel(*refs, n_ep=n_ep, cap=cap, shift=shift),
        out_shape=jax.ShapeDtypeStruct((n_ep, 8, LANES), jnp.float32),
        in_specs=[vmem(), vmem()],
        out_specs=vmem(),
        scratch_shapes=[
            pltpu.VMEM((6 * n_ep, tok * picks), jnp.bfloat16),
            pltpu.VMEM((cap, tok * picks), jnp.bfloat16),
        ],
        interpret=INTERPRET,
        name="bucket",
    )(row_ids.T, row_gates.T)
    listed = lax.all_to_all(listed, EP, 0, 0, tiled=True)
    codes = listed[:, :chunks].astype(jnp.int32)
    gates = listed[:, chunks : 2 * chunks].reshape(lines, LANES)
    rows = (codes & (exp_dev - 1)).reshape(lines, LANES)
    place = ((codes >> shift) - 1).reshape(lines, LANES)
    count = jnp.sum((codes > 0).astype(jnp.int32), axis=(1, 2))

    picked = jax.ShapeDtypeStruct((lines, LANES, width), jnp.bfloat16)
    keys, values = pl.pallas_call(
        pick_kernel,
        out_shape=(picked, picked),
        in_specs=[smem(), smem(), vmem(), vmem()],
        out_specs=(vmem(), vmem()),
        scratch_shapes=[
            pltpu.VMEM((exp_dev, width), jnp.float32),
            pltpu.VMEM((exp_dev, width), jnp.float32),
            pltpu.VMEM((LANES, width), jnp.float32),
            pltpu.VMEM((LANES, width), jnp.float32),
        ],
        interpret=INTERPRET,
        name="pick",
    )(rows, count, key_table, value_table)
    partial_score = pl.pallas_call(
        score_kernel,
        out_shape=jax.ShapeDtypeStruct((lines, LANES), jnp.float32),
        in_specs=[smem(), vmem(), vmem(), vmem()],
        out_specs=vmem(),
        interpret=INTERPRET,
        name="score",
    )(count, place, spread, keys)
    score = jnp.sum(lax.all_gather(partial_score, TP), axis=0)
    hidden = jnp.where(place >= 0, jax.nn.gelu(score, approximate=False) * gates, 0.0)
    mixed_part = pl.pallas_call(
        combine_kernel,
        out_shape=jax.ShapeDtypeStruct((n_ep, tok, width), jnp.bfloat16),
        in_specs=[smem(), vmem(), vmem(), vmem()],
        out_specs=vmem(),
        scratch_shapes=[pltpu.VMEM((tok, width), jnp.float32)],
        interpret=INTERPRET,
        name="combine",
    )(count, place, hidden, values)
    back = lax.all_to_all(mixed_part, EP, 0, 0, tiled=True)
    mixed = jnp.sum(back.astype(jnp.float32), axis=0)
    part = jnp.sum(mixed * mixed, axis=1).reshape(tok // LANES, LANES)
    squares = jnp.sum(to_each(part, TP), axis=0).reshape(tok)
    strength = squares / D
    return (mixed * lax.rsqrt(strength + 1e-06)[:, None] * norm_gain).astype(jnp.bfloat16)


def solution(mesh):
    ep, tp = mesh.devices.shape
    fine = Mesh(mesh.devices.reshape(Z, ep // Z, tp // 2, 2), ("z", "x", "y", "core"))
    in_specs = (P(EP, TP), P(EP, None), P(EP, None), P(EP, TP), P(EP, TP), P(TP))
    return jax.shard_map(body, mesh=fine, in_specs=in_specs, out_specs=P(EP, TP), check_vma=False)
```

time: 207 us -> 188 us (0.908)
  waiting for transfers between devices: 44.6 us -> 7.54 us
  blocking collectives: 120 us -> 133 us
  Pallas kernels: 28.5 us -> 35.5 us
    all_to_all x1, waiting for transfers between devices: 44.6 us -> 7.54 us  [to_each(): lax.all_to_all(jnp.broadcast_to(value[None], (lax.axis_size(axis), *value...]
    all_to_all x2 -> x4, blocking collectives: 78.9 us -> 108 us  [the longest x1 54.8 us: body(): back = lax.all_to_all(mixed_part, EP, 0, 0, tiled=True)]
    all_gather x2 -> x1, blocking collectives: 41.2 us -> 24.4 us  [body(): score = jnp.sum(lax.all_gather(partial_score, TP), axis=0)]
    pallas_call x0 -> x1, Pallas kernels: none -> 12.6 us  [body(): pl.pallas_call(pick_kernel, out_shape=(picked, picked), in_specs=[smem(),...]
    pallas_call x1, Pallas kernels: 13.1 us -> 9.88 us  [body(): pl.pallas_call(combine_kernel, out_shape=jax.ShapeDtypeStruct((n_ep, tok,...]
    pallas_call x1, Pallas kernels: 12.4 us -> 10 us  [body(): pl.pallas_call(score_kernel, out_shape=jax.ShapeDtypeStruct((lines, LANES...]
  transfers between devices with their start and end apart: 1 -> 1, of which waited for: 1 -> 1; matrix products, arithmetic and copies ran while one was open for 1% -> 1% of each run, Pallas kernels for 0% -> 7%
where the time goes in v2:
time: 188 us
  blocking collectives  133 us (71%)
  Pallas kernels  35.5 us (19%)
  waiting for transfers between devices  7.54 us (4%)
  local copies, waits for them, and re-layouts  5.41 us (3%)
  starting transfers between devices  3.61 us (2%)
  other arithmetic  3.14 us (2%)
    all_to_all x1, blocking collectives, body(): back = lax.all_to_all(mixed_part, EP, 0, 0, tiled=True)  54.8 us
    all_to_all x2, blocking collectives, to_each(): lax.all_to_all(jnp.broadcast_to(value[None], (lax.axis_size(axis), *value...  30.4 us
    all_gather x1, blocking collectives, body(): score = jnp.sum(lax.all_gather(partial_score, TP), axis=0)  24.4 us
    all_to_all x1, blocking collectives, body(): listed = lax.all_to_all(listed, EP, 0, 0, tiled=True)  23 us
    pallas_call x1, Pallas kernels, body(): pl.pallas_call(pick_kernel, out_shape=(picked, picked), in_specs=[smem(),...  12.6 us
    pallas_call x1, Pallas kernels, body(): pl.pallas_call(score_kernel, out_shape=jax.ShapeDtypeStruct((lines, LANES...  10 us
    pallas_call x1, Pallas kernels, body(): pl.pallas_call(combine_kernel, out_shape=jax.ShapeDtypeStruct((n_ep, tok,...  9.88 us
    all_to_all x1, waiting for transfers between devices, to_each(): lax.all_to_all(jnp.broadcast_to(value[None], (lax.axis_size(axis), *value...  7.54 us
  transfers between devices with their start and end apart: 1, of which 1 were waited for; matrix products, arithmetic and copies ran while one was open for 1% of the time, Pallas kernels for 7%

profile of v2, /device:TPU:1, one launch (start us, length us, event | category | flops | bytes accessed | tf_op | source)
XLA Modules:
  0.0 187.9 jit_solution(7456011899723214339)
XLA Ops:
  0.0 3.0 %bucket.1 = f32[32,8,128]{2,1,0:T(8,128)} custom-call(s32[16,256]{1,0:T(8,128)} %bitcast.7, f32[16,256]{1,0:T(8,128)} %bitcast.8), custom_call_target="tpu_custom_call" | custom-call | tf_op jit(solution)/shard_map/bucket/pallas_call | solution.py:189
  3.0 23.0 %all_to_all.25 = f32[32,8,128]{2,1,0:T(8,128)S(1)} all-to-all(f32[32,8,128]{2,1,0:T(8,128)} %bucket.1), channel_id=1, replica_groups=mesh['z'=8,'x'=4,'y'=8,'core'=2] {'z','x'}, dimensions={0} | all-to-all | bytes 262144 | tf_op jit(solution)/shard_map/all_to_all | solution.py:201
  26.0 0.9 broadcast_in_dim.10
  26.9 17.1 %all_to_all.26 = bf16[8,256,128]{2,1,0:T(8,128)(2,1)S(1)} all-to-all(bf16[8,256,128]{2,1,0:T(8,128)(2,1)S(1)} %broadcast_in_dim.10), channel_id=1, replica_groups=mesh['z'=8,'x'=4,'y'=8,'core'=2] {'z'}, dimensions={0} | all-to-all | bytes 1048576 | tf_op jit(solution)/shard_map/all_to_all | solution.py:173
  44.0 1.8 broadcast_in_dim.11
  45.8 3.6 %all-to-all-start.2 = ((bf16[4,8,256,128]{3,2,1,0:T(8,128)(2,1)}), bf16[4,8,256,128]{3,2,1,0:T(8,128)(2,1)S(1)}, u32[]{:S(2)}, u32[]{:S(2)}) async-start(bf16[4,8,256,128]{3,2,1,0:T(8,128)(2,1)} %broadcast_in_dim.11), calls=%async_computation.2 | async-start | bytes 4194304 | tf_op jit(solution)/shard_map/all_to_all | solution.py:173
  49.5 1.2 fusion
  50.7 0.6 reshape.27.rows_ref
  51.3 0.6 reshape.26.place_ref
  52.0 12.6 %pick.1 = (bf16[96,128,128]{2,1,0:T(8,128)(2,1)}, bf16[96,128,128]{2,1,0:T(8,128)(2,1)}) custom-call(s32[96,128]{1,0:T(8,128)} %reshape.27.rows_ref, s32[32]{0:T(128)} %get-tuple-element.11.count_ref, bf16[4096,128]{1,0:T(8,128)(2,1)} %key_ref.1, bf16[4096,128]{1,0:T(8,128)(2,1)} %value_ref.1), custom_call_target="tpu_custom_call" | custom-call | tf_op jit(solution)/shard_map/pick/pallas_call | solution.py:209
  64.6 7.5 %all-to-all-done.2.tok_ref = bf16[4,8,256,128]{3,2,1,0:T(8,128)(2,1)S(1)} async-done(((bf16[4,8,256,128]{3,2,1,0:T(8,128)(2,1)}), bf16[4,8,256,128]{3,2,1,0:T(8,128)(2,1)S(1)}, u32[]{:S(2)}, u32[]{:S(2)}) %all-to-all-start.2) | async-done | bytes 2097184 | tf_op jit(solution)/shard_map/all_to_all | solution.py:173
  72.1 0.0 copy-start
  72.1 1.3 copy-done
  73.4 0.0 copy-start.1
  73.4 10.0 %score.1 = f32[96,128]{1,0:T(8,128)} custom-call(s32[32]{0:T(128)} %get-tuple-element.11.count_ref, s32[96,128]{1,0:T(8,128)} %reshape.26.place_ref, bf16[4,8,256,128]{3,2,1,0:T(8,128)(2,1)} %copy-done, bf16[96,128,128]{2,1,0:T(8,128)(2,1)} %get-tuple-element.7.keys_ref), custom_call_target="tpu_custom_call" | custom-call | tf_op jit(solution)/shard_map/score/pallas_call | solution.py:223
  83.5 24.4 %all-gather = f32[1536,128]{1,0:T(8,128)S(1)} all-gather(f32[96,128]{1,0:T(8,128)} %score.1), channel_id=2, replica_groups=mesh['z'=8,'x'=4,'y'=8,'core'=2] {'y','core'}, dimensions={0}, use_global_device_ids=true | all-gather | bytes 835584 | tf_op jit(solution)/shard_map/all_gather | solution.py:231
  107.9 0.0 copy-done.1
  108.0 0.7 fusion.4.hidden_ref
  108.7 9.9 %combine.1 = bf16[32,256,128]{2,1,0:T(8,128)(2,1)} custom-call(s32[32]{0:T(128)} %get-tuple-element.11.count_ref, s32[96,128]{1,0:T(8,128)} %reshape.26.place_ref, f32[96,128]{1,0:T(8,128)} %fusion.4.hidden_ref, bf16[96,128,128]{2,1,0:T(8,128)(2,1)} %get-tuple-element.8.values_ref), custom_call_target="tpu_custom_call" | custom-call | tf_op jit(solution)/shard_map/combine/pallas_call | solution.py:233
  118.6 54.8 %all_to_all.27 = bf16[32,256,128]{2,1,0:T(8,128)(2,1)S(1)} all-to-all(bf16[32,256,128]{2,1,0:T(8,128)(2,1)} %combine.1), channel_id=1, replica_groups=mesh['z'=8,'x'=4,'y'=8,'core'=2] {'z','x'}, dimensions={0} | all-to-all | bytes 4194304 | tf_op jit(solution)/shard_map/all_to_all | solution.py:242
  173.4 0.0 copy-start.2
  173.4 0.3 convert_reduce_fusion
  173.7 0.1 multiply_reduce_fusion
  173.8 13.3 %all_to_all.28 = f32[16,2,128]{2,1,0:T(2,128)S(1)} all-to-all(f32[16,2,128]{2,1,0:T(2,128)S(1)} %broadcast_in_dim.13), channel_id=1, replica_groups=mesh['z'=8,'x'=4,'y'=8,'core'=2] {'y','core'}, dimensions={0} | all-to-all | bytes 32768 | tf_op jit(solution)/shard_map/all_to_all | solution.py:173
  187.2 0.0 copy-done.2
  187.2 0.7 multiply_convert_fusion
  (6 shorter events, 0.1 us)
Async XLA Ops:
  45.8 26.2 %all-to-all-start.2 = ((bf16[4,8,256,128]{3,2,1,0:T(8,128)(2,1)}), bf16[4,8,256,128]{3,2,1,0:T(8,128)(2,1)S(1)}, u32[]{:S(2)}, u32[]{:S(2)}) async-start(bf16[4,8,256,128]{3,2,1,0:T(8,128)(2,1)} %broadcast_in_dim.11), calls=%async_computation.2 | async-start | bytes 4194304 | tf_op jit(solution)/shard_map/all_to_all | solution.py:173
  72.1 1.3 copy-start
  73.4 34.5 %copy-start.1 = (s32[96,128]{1,0:T(8,128)S(1)}, s32[96,128]{1,0:T(8,128)}, u32[]{:S(2)}) copy-start(s32[96,128]{1,0:T(8,128)} %reshape.26.place_ref) | copy-start | bytes 147460
  173.4 13.8 %copy-start.2 = (f32[128]{0:T(128)S(1)}, f32[128]{0:T(128)}, u32[]{:S(2)}) copy-start(f32[128]{0:T(128)} %param.11) | copy-start | bytes 1540

commit v3 on v2

--- a/solution.py
+++ b/solution.py
@@ -10,6 +10,8 @@
 LANES = 128
 INTERPRET = False
 Z = 8
+X = 4
+SHIFTS = (0, 2, 1, 3)
 EP = ("z", "x")
 TP = ("y", "core")
 
@@ -79,86 +81,133 @@
     lax.fori_loop(0, table_ref.shape[0] // step, one, 0)
 
 
-def take_rows(rows_ref, line, wide_ref, picked, out_ref):
+def take_rows(rows_ref, line, wide_ref, picked, out_ref, to):
     for s in range(LANES):
         picked[pl.ds(s, 1), :] = wide_ref[pl.ds(rows_ref[line, s], 1), :]
-    out_ref[line] = picked[...].astype(out_ref.dtype)
-
-
-def each_line(count_ref, chunks, start, work, finish):
-    def block(i, carry):
-        start(i)
-
-        def chunk(c, inner):
-            work(i, i * chunks + c)
-            return inner
-
-        lax.fori_loop(0, (count_ref[i] + LANES - 1) // LANES, chunk, 0)
-        finish(i)
-        return carry
-
-    lax.fori_loop(0, count_ref.shape[0], block, 0)
-
-
-def nothing(i):
-    del i
+    out_ref[to] = picked[...].astype(out_ref.dtype)
+
+
+def chunks_of(count):
+    return (count + LANES - 1) // LANES
 
 
 def pick_kernel(
-    rows_ref, count_ref, key_ref, value_ref, keys_out, values_out, wide_k, wide_v, took_k, took_v
+    x_ref,
+    rows_ref,
+    count_ref,
+    place_ref,
+    gate_ref,
+    key_ref,
+    value_ref,
+    count_out,
+    place_out,
+    gate_out,
+    keys_out,
+    values_out,
+    wide_k,
+    wide_v,
+    took_k,
+    took_v,
 ):
+    n_ep = count_ref.shape[0]
+    n_z = n_ep // X
+    chunks = place_ref.shape[0] // n_ep
     widen(key_ref, wide_k)
     widen(value_ref, wide_v)
-    chunks = keys_out.shape[0] // count_ref.shape[0]
-
-    def work(i, line):
-        take_rows(rows_ref, line, wide_k, took_k, keys_out)
-        take_rows(rows_ref, line, wide_v, took_v, values_out)
-
-    each_line(count_ref, chunks, nothing, work, nothing)
-
-
-def score_kernel(count_ref, place_ref, tok_ref, keys_ref, out_ref):
-    n_x, n_z, tok, _ = tok_ref.shape
-    chunks = place_ref.shape[0] // (n_x * n_z)
+
+    def block(i, carry):
+        z = i // X
+        shift = (x_ref[0] + X - i % X) % X
+        slot = (shift // 2 + (shift % 2) * 2) * n_z + z
+        count_out[slot] = count_ref[i]
+        for c in range(chunks):
+            place_out[pl.ds(slot * chunks + c, 1), :] = place_ref[pl.ds(i * chunks + c, 1), :]
+            gate_out[pl.ds(slot * chunks + c, 1), :] = gate_ref[pl.ds(i * chunks + c, 1), :]
+
+        def chunk(c, inner):
+            take_rows(rows_ref, i * chunks + c, wide_k, took_k, keys_out, slot * chunks + c)
+            take_rows(rows_ref, i * chunks + c, wide_v, took_v, values_out, slot * chunks + c)
+            return inner
+
+        lax.fori_loop(0, chunks_of(count_ref[i]), chunk, 0)
+        return carry
+
+    lax.fori_loop(0, n_ep, block, 0)
+
+
+def score_kernel(count_ref, place_ref, keys_ref, tok0, tok1, tok2, tok3, out_ref):
+    toks = (tok0, tok1, tok2, tok3)
+    n_z, tok, _ = tok0.shape
+    chunks = place_ref.shape[0] // (X * n_z)
     out_ref[...] = jnp.zeros(out_ref.shape, jnp.float32)
     token_of = lax.broadcasted_iota(jnp.int32, (tok, LANES), 0)
 
-    def work(i, line):
+    def line_scores(tokens, line):
         prod = lax.dot_general(
-            tok_ref[i % n_x, i // n_x],
-            keys_ref[line],
-            (((1,), (1,)), ((), ())),
-            preferred_element_type=jnp.float32,
+            tokens, keys_ref[line], (((1,), (1,)), ((), ())), preferred_element_type=jnp.float32
         )
         here = place_ref[pl.ds(line, 1), :] == token_of
-        out_ref[pl.ds(line, 1), :] = jnp.sum(jnp.where(here, prod, 0.0), axis=0, keepdims=True)
-
-    each_line(count_ref, chunks, nothing, work, nothing)
-
-
-def combine_kernel(count_ref, place_ref, hidden_ref, values_ref, out_ref, acc):
-    n_ep, tok, _ = out_ref.shape
-    chunks = place_ref.shape[0] // n_ep
+        return jnp.sum(jnp.where(here, prod, 0.0), axis=0, keepdims=True)
+
+    def first(z, carry):
+        lines = [(g * n_z + z) * chunks for g in range(X)]
+        found = [line_scores(toks[g][z], lines[g]) for g in range(X)]
+        for line, value in zip(lines, found):
+            out_ref[pl.ds(line, 1), :] = value
+        return carry
+
+    lax.fori_loop(0, n_z, first, 0)
+
+    def more(z, carry):
+        for g in range(X):
+
+            def chunk(c, inner, g=g):
+                line = (g * n_z + z) * chunks + c
+                out_ref[pl.ds(line, 1), :] = line_scores(toks[g][z], line)
+                return inner
+
+            lax.fori_loop(1, chunks_of(count_ref[g * n_z + z]), chunk, 0)
+        return carry
+
+    lax.fori_loop(0, n_z, more, 0)
+
+
+def combine_kernel(count_ref, place_ref, hidden_ref, values_ref, out_ref, acc, *, group):
+    n_z, tok, _ = out_ref.shape
+    chunks = place_ref.shape[0] // n_z
     token_of = lax.broadcasted_iota(jnp.int32, (tok, LANES), 0)
 
-    def start(i):
-        acc[...] = jnp.zeros(acc.shape, jnp.float32)
-
-    def work(i, line):
+    def line_mix(line):
         here = place_ref[pl.ds(line, 1), :] == token_of
         weight = jnp.where(here, hidden_ref[pl.ds(line, 1), :], 0.0)
         high = weight.astype(jnp.bfloat16)
         low = (weight - high.astype(jnp.float32)).astype(jnp.bfloat16)
         rows = values_ref[line]
-        acc[...] += jnp.dot(high, rows, preferred_element_type=jnp.float32) + jnp.dot(
-            low, rows, preferred_element_type=jnp.float32
-        )
-
-    def finish(i):
-        out_ref[i] = acc[...].astype(out_ref.dtype)
-
-    each_line(count_ref, chunks, start, work, finish)
+        return jnp.dot(
+            jnp.concatenate([high, low], axis=1),
+            jnp.concatenate([rows, rows], axis=0),
+            preferred_element_type=jnp.float32,
+        )
+
+    def first(half, carry):
+        zs = [half * 4 + j for j in range(4)]
+        found = [line_mix(z * chunks) for z in zs]
+        for z, value in zip(zs, found):
+            acc[z] = value
+        return carry
+
+    lax.fori_loop(0, n_z // 4, first, 0)
+
+    def more(z, carry):
+        def chunk(c, inner):
+            acc[z] += line_mix(z * chunks + c)
+            return inner
+
+        lax.fori_loop(1, chunks_of(count_ref[group * n_z + z]), chunk, 0)
+        out_ref[z] = acc[z].astype(out_ref.dtype)
+        return carry
+
+    lax.fori_loop(0, n_z, more, 0)
 
 
 def vmem():
@@ -173,6 +222,10 @@
     return lax.all_to_all(
         jnp.broadcast_to(value[None], (lax.axis_size(axis), *value.shape)), axis, 0, 0, tiled=True
     )
+
+
+def around(shift):
+    return [(i, (i + shift) % X) for i in range(X)]
 
 
 def body(tokens, row_ids, row_gates, key_table, value_table, norm_gain):
@@ -185,7 +238,8 @@
     shift = exp_dev.bit_length() - 1
     lines = n_ep * chunks
 
-    spread = to_each(to_each(tokens, "z"), "x")
+    near = to_each(tokens, "z")
+    groups = [near] + [lax.ppermute(near, "x", around(shift)) for shift in SHIFTS[1:]]
     listed = pl.pallas_call(
         lambda *refs: bucket_kernel(*refs, n_ep=n_ep, cap=cap, shift=shift),
         out_shape=jax.ShapeDtypeStruct((n_ep, 8, LANES), jnp.float32),
@@ -205,12 +259,19 @@
     place = ((codes >> shift) - 1).reshape(lines, LANES)
     count = jnp.sum((codes > 0).astype(jnp.int32), axis=(1, 2))
 
+    n_z = n_ep // X
     picked = jax.ShapeDtypeStruct((lines, LANES, width), jnp.bfloat16)
-    keys, values = pl.pallas_call(
+    count, place, gates, keys, values = pl.pallas_call(
         pick_kernel,
-        out_shape=(picked, picked),
-        in_specs=[smem(), smem(), vmem(), vmem()],
-        out_specs=(vmem(), vmem()),
+        out_shape=(
+            jax.ShapeDtypeStruct((n_ep,), jnp.int32),
+            jax.ShapeDtypeStruct((lines, LANES), jnp.int32),
+            jax.ShapeDtypeStruct((lines, LANES), jnp.float32),
+            picked,
+            picked,
+        ),
+        in_specs=[smem(), smem(), smem(), vmem(), vmem(), vmem(), vmem()],
+        out_specs=(smem(), vmem(), vmem(), vmem(), vmem()),
         scratch_shapes=[
             pltpu.VMEM((exp_dev, width), jnp.float32),
             pltpu.VMEM((exp_dev, width), jnp.float32),
@@ -219,27 +280,41 @@
         ],
         interpret=INTERPRET,
         name="pick",
-    )(rows, count, key_table, value_table)
+    )(lax.axis_index("x").reshape(1), rows, count, place, gates, key_table, value_table)
     partial_score = pl.pallas_call(
         score_kernel,
         out_shape=jax.ShapeDtypeStruct((lines, LANES), jnp.float32),
-        in_specs=[smem(), vmem(), vmem(), vmem()],
+        in_specs=[smem()] + [vmem()] * 6,
         out_specs=vmem(),
         interpret=INTERPRET,
         name="score",
-    )(count, place, spread, keys)
+    )(count, place, keys, *groups)
     score = jnp.sum(lax.all_gather(partial_score, TP), axis=0)
     hidden = jnp.where(place >= 0, jax.nn.gelu(score, approximate=False) * gates, 0.0)
-    mixed_part = pl.pallas_call(
-        combine_kernel,
-        out_shape=jax.ShapeDtypeStruct((n_ep, tok, width), jnp.bfloat16),
-        in_specs=[smem(), vmem(), vmem(), vmem()],
-        out_specs=vmem(),
-        scratch_shapes=[pltpu.VMEM((tok, width), jnp.float32)],
-        interpret=INTERPRET,
-        name="combine",
-    )(count, place, hidden, values)
-    back = lax.all_to_all(mixed_part, EP, 0, 0, tiled=True)
+
+    def combine(group):
+        per = n_z * chunks
+        return pl.pallas_call(
+            lambda *refs: combine_kernel(*refs, group=group),
+            out_shape=jax.ShapeDtypeStruct((n_z, tok, width), jnp.bfloat16),
+            grid=(1,),
+            in_specs=[
+                smem(),
+                pl.BlockSpec((per, LANES), lambda i: (group, 0)),
+                pl.BlockSpec((per, LANES), lambda i: (group, 0)),
+                pl.BlockSpec((per, LANES, width), lambda i: (group, 0, 0)),
+            ],
+            out_specs=pl.BlockSpec((n_z, tok, width), lambda i: (0, 0, 0)),
+            scratch_shapes=[pltpu.VMEM((n_z, tok, width), jnp.float32)],
+            interpret=INTERPRET,
+            name="combine",
+        )(count, place, hidden, values)
+
+    parts = [
+        lax.ppermute(combine(g), "x", around(-SHIFTS[g])) if g else combine(g) for g in (1, 2, 3, 0)
+    ]
+    mine = sum(p.astype(jnp.float32) for p in parts).astype(jnp.bfloat16)
+    back = lax.all_to_all(mine, "z", 0, 0, tiled=True)
     mixed = jnp.sum(back.astype(jnp.float32), axis=0)
     part = jnp.sum(mixed * mixed, axis=1).reshape(tok // LANES, LANES)
     squares = jnp.sum(to_each(part, TP), axis=0).reshape(tok)

time: 188 us -> 177 us (0.941)
  blocking collectives: 133 us -> 82.6 us
  starting transfers between devices: 3.61 us -> 25.2 us
  waiting for transfers between devices: 7.54 us -> 27.2 us
  Pallas kernels: 35.5 us -> 32.4 us
    all_to_all x2 -> x1, blocking collectives: 77.9 us -> 20.5 us  [body(): back = lax.all_to_all(mine, 'z', 0, 0, tiled=True)]
    ppermute x0 -> x6, starting transfers between devices: none -> 21.4 us  [the longest x3 11.1 us: body(): lax.ppermute(near, 'x', around(shift))]
    ppermute x0 -> x6, waiting for transfers between devices: none -> 15.5 us  [the longest x3 15.5 us: body(): lax.ppermute(combine(g), 'x', around(-SHIFTS[g]))]
    all_to_all x2, blocking collectives: 30.4 us -> 40.3 us  [to_each(): lax.all_to_all(jnp.broadcast_to(value[None], (lax.axis_size(axis), *value...]
    pallas_call x1, Pallas kernels: 10 us -> 5.54 us  [body(): pl.pallas_call(score_kernel, out_shape=jax.ShapeDtypeStruct((lines, LANES...]
    all_to_all x1, waiting for transfers between devices: 7.54 us -> 11.7 us  [body(): listed = lax.all_to_all(listed, EP, 0, 0, tiled=True)]
    all_gather x1, blocking collectives: 24.4 us -> 21.8 us  [body(): score = jnp.sum(lax.all_gather(partial_score, TP), axis=0)]
    pallas_call x2 -> x5, Pallas kernels: 22.4 us -> 23.8 us  [the longest x1 12.6 us: body(): pl.pallas_call(pick_kernel, out_shape=(jax.ShapeDtypeStruct((n_ep,), jnp....]
  transfers between devices with their start and end apart: 1 -> 7, of which waited for: 1 -> 4; matrix products, arithmetic and copies ran while one was open for 1% -> 2% of each run, Pallas kernels for 7% -> 10%
where the time goes in v3:
time: 177 us; the launch traced here: 176 us
  blocking collectives  82.6 us (47%)
  Pallas kernels  32.4 us (18%)
  waiting for transfers between devices  27.2 us (15%)
  starting transfers between devices  25.2 us (14%)
  other arithmetic  4.2 us (2%)
  local copies, waits for them, and re-layouts  3.97 us (2%)
    all_to_all x2, blocking collectives, to_each(): lax.all_to_all(jnp.broadcast_to(value[None], (lax.axis_size(axis), *value...  40.3 us
    all_gather x1, blocking collectives, body(): score = jnp.sum(lax.all_gather(partial_score, TP), axis=0)  21.8 us
    all_to_all x1, blocking collectives, body(): back = lax.all_to_all(mine, 'z', 0, 0, tiled=True)  20.5 us
    ppermute x3, waiting for transfers between devices, body(): lax.ppermute(combine(g), 'x', around(-SHIFTS[g]))  15.5 us
    pallas_call x1, Pallas kernels, body(): pl.pallas_call(pick_kernel, out_shape=(jax.ShapeDtypeStruct((n_ep,), jnp....  12.6 us
    all_to_all x1, waiting for transfers between devices, body(): listed = lax.all_to_all(listed, EP, 0, 0, tiled=True)  11.7 us
    pallas_call x4, Pallas kernels, combine(): pl.pallas_call(lambda *refs: combine_kernel(*refs, group=group), out_shap...  11.2 us
    ppermute x3, starting transfers between devices, body(): lax.ppermute(near, 'x', around(shift))  11.1 us
  transfers between devices with their start and end apart: 7, of which 4 were waited for; matrix products, arithmetic and copies ran while one was open for 2% of the time, Pallas kernels for 10%

profile of v3, /device:TPU:1, one launch (start us, length us, event | category | flops | bytes accessed | tf_op | source)
XLA Modules:
  0.0 175.8 jit_solution(15496931845950104363)
XLA Ops:
  0.0 0.9 broadcast_in_dim.8
  0.9 26.8 %all_to_all.20.tok0 = bf16[8,256,128]{2,1,0:T(8,128)(2,1)S(1)} all-to-all(bf16[8,256,128]{2,1,0:T(8,128)(2,1)S(1)} %broadcast_in_dim.8), channel_id=1, replica_groups=mesh['z'=8,'x'=4,'y'=8,'core'=2] {'z'}, dimensions={0} | all-to-all | bytes 1048576 | tf_op jit(solution)/shard_map/all_to_all | solution.py:222
  27.7 0.0 copy-start
  27.7 4.6 %collective-permute-start = (bf16[8,256,128]{2,1,0:T(8,128)(2,1)S(1)}, bf16[8,256,128]{2,1,0:T(8,128)(2,1)S(1)}, u32[]{:S(2)}, u32[]{:S(2)}) collective-permute-start(bf16[8,256,128]{2,1,0:T(8,128)(2,1)S(1)} %all_to_all.20.tok0), channel_id=1, source_target_pairs={{0,32},{16,48},{32,0},{48,16},{1,33},{17,49},{33,1},{49,17},{2,34}... | collective-permute-start | bytes 1572872 | tf_op jit(solution)/shard_map/ppermute | solution.py:242
  32.3 2.2 %collective-permute-start.1 = (bf16[8,256,128]{2,1,0:T(8,128)(2,1)S(1)}, bf16[8,256,128]{2,1,0:T(8,128)(2,1)S(1)}, u32[]{:S(2)}, u32[]{:S(2)}) collective-permute-start(bf16[8,256,128]{2,1,0:T(8,128)(2,1)S(1)} %all_to_all.20.tok0), channel_id=1, source_target_pairs={{0,16},{16,32},{32,48},{48,0},{1,17},{17,33},{33,49},{49,1},{2,18}... | collective-permute-start | bytes 1572872 | tf_op jit(solution)/shard_map/ppermute | solution.py:242
  34.6 4.3 %collective-permute-start.2 = (bf16[8,256,128]{2,1,0:T(8,128)(2,1)S(1)}, bf16[8,256,128]{2,1,0:T(8,128)(2,1)S(1)}, u32[]{:S(2)}, u32[]{:S(2)}) collective-permute-start(bf16[8,256,128]{2,1,0:T(8,128)(2,1)S(1)} %all_to_all.20.tok0), channel_id=1, source_target_pairs={{0,48},{16,0},{32,16},{48,32},{1,49},{17,1},{33,17},{49,33},{2,50}... | collective-permute-start | bytes 1572872 | tf_op jit(solution)/shard_map/ppermute | solution.py:242
  38.8 3.0 %bucket.1 = f32[32,8,128]{2,1,0:T(8,128)} custom-call(s32[16,256]{1,0:T(8,128)} %bitcast.8, f32[16,256]{1,0:T(8,128)} %bitcast.9), custom_call_target="tpu_custom_call" | custom-call | tf_op jit(solution)/shard_map/bucket/pallas_call | solution.py:243
  41.8 3.9 %all-to-all-start = ((f32[32,8,128]{2,1,0:T(8,128)}), f32[32,8,128]{2,1,0:T(8,128)S(1)}, u32[]{:S(2)}, u32[]{:S(2)}) async-start(f32[32,8,128]{2,1,0:T(8,128)} %bucket.1), calls=%async_computation | async-start | bytes 262144 | tf_op jit(solution)/shard_map/all_to_all | solution.py:255
  45.7 11.7 %all-to-all-done = f32[32,8,128]{2,1,0:T(8,128)S(1)} async-done(((f32[32,8,128]{2,1,0:T(8,128)}), f32[32,8,128]{2,1,0:T(8,128)S(1)}, u32[]{:S(2)}, u32[]{:S(2)}) %all-to-all-start) | async-done | bytes 131104 | tf_op jit(solution)/shard_map/all_to_all | solution.py:255
  57.4 1.1 shift-right-arithmetic_add_fusion
  58.5 0.6 reshape.29.rows_ref
  59.2 0.6 reshape.30.place_ref
  59.8 0.6 reshape.31.gate_ref
  60.5 12.6 %pick.1 = (s32[32]{0:T(128)}, s32[96,128]{1,0:T(8,128)}, f32[96,128]{1,0:T(8,128)}, bf16[96,128,128]{2,1,0:T(8,128)(2,1)}, bf16[96,128,128]{2,1,0:T(8,128)(2,1)}) custom-call(s32[1]{0:T(128)} %bitcast.x_ref, s32[96,128]{1,0:T(8,128)} %reshape.29.rows_ref, s32[32]{0:T(128)} %get-tuple-element.16.count_ref, s32[96,128]{1,0:T(8,128)} %reshape.30.place_ref, ...), custom_call_target="tpu_custom_call" | custom-call | tf_op jit(solution)/shard_map/pick/pallas_call | solution.py:264
  73.1 0.0 collective-permute-done.tok1
  73.1 0.0 copy-start.4
  73.1 0.0 collective-permute-done.1.tok2
  73.1 0.0 copy-start.5
  73.1 0.0 collective-permute-done.2.tok3
  73.1 0.0 copy-start.6
  73.1 0.0 copy-done
  73.1 0.7 copy-done.4
  73.9 0.2 copy-done.5
  74.0 0.2 copy-done.6
  74.2 5.5 %score.1 = f32[96,128]{1,0:T(8,128)} custom-call(s32[32]{0:T(128)} %get-tuple-element.10.count_ref.refs_0_, s32[96,128]{1,0:T(8,128)} %get-tuple-element.11.place_ref.refs_1_, bf16[96,128,128]{2,1,0:T(8,128)(2,1)} %get-tuple-element.12.keys_ref, bf16[8,256,128]{2,1,0:T(8,128)(2,1)} %copy-done, bf16[8,256,128]{2,1,0:T(8,128)(2,1)} %copy-done.4, ...), custom_call_target="tpu_custom_call" | custom-call | tf_op jit(solution)/shard_map/score/pallas_call | solution.py:284
  79.8 21.8 %all-gather = f32[1536,128]{1,0:T(8,128)S(1)} all-gather(f32[96,128]{1,0:T(8,128)} %score.1), channel_id=2, replica_groups=mesh['z'=8,'x'=4,'y'=8,'core'=2] {'y','core'}, dimensions={0}, use_global_device_ids=true | all-gather | bytes 835584 | tf_op jit(solution)/shard_map/all_gather | solution.py:292
  101.7 0.0 copy-done.1
  101.7 0.0 copy-done.7
  101.7 0.7 fusion.4.refs_2_
  102.4 2.8 %combine.4 = bf16[8,256,128]{2,1,0:T(8,128)(2,1)} custom-call(s32[32]{0:T(128)} %get-tuple-element.10.count_ref.refs_0_, s32[96,128]{1,0:T(8,128)} %get-tuple-element.11.place_ref.refs_1_, f32[96,128]{1,0:T(8,128)} %fusion.4.refs_2_, bf16[96,128,128]{2,1,0:T(8,128)(2,1)} %get-tuple-element.14.refs_3_), custom_call_target="tpu_custom_call" | custom-call | tf_op jit(solution)/shard_map/combine/pallas_call | solution.py:297
  105.2 2.8 %combine.5 = bf16[8,256,128]{2,1,0:T(8,128)(2,1)} custom-call(s32[32]{0:T(128)} %get-tuple-element.10.count_ref.refs_0_, s32[96,128]{1,0:T(8,128)} %get-tuple-element.11.place_ref.refs_1_, f32[96,128]{1,0:T(8,128)} %fusion.4.refs_2_, bf16[96,128,128]{2,1,0:T(8,128)(2,1)} %get-tuple-element.14.refs_3_), custom_call_target="tpu_custom_call" | custom-call | tf_op jit(solution)/shard_map/combine/pallas_call | solution.py:297
  108.1 2.8 %combine.6 = bf16[8,256,128]{2,1,0:T(8,128)(2,1)} custom-call(s32[32]{0:T(128)} %get-tuple-element.10.count_ref.refs_0_, s32[96,128]{1,0:T(8,128)} %get-tuple-element.11.place_ref.refs_1_, f32[96,128]{1,0:T(8,128)} %fusion.4.refs_2_, bf16[96,128,128]{2,1,0:T(8,128)(2,1)} %get-tuple-element.14.refs_3_), custom_call_target="tpu_custom_call" | custom-call | tf_op jit(solution)/shard_map/combine/pallas_call | solution.py:297
  110.9 0.0 copy-done.3
  110.9 4.9 %collective-permute-start.3 = (bf16[8,256,128]{2,1,0:T(8,128)(2,1)S(1)}, bf16[8,256,128]{2,1,0:T(8,128)(2,1)S(1)}, u32[]{:S(2)}, u32[]{:S(2)}) collective-permute-start(bf16[8,256,128]{2,1,0:T(8,128)(2,1)S(1)} %copy-done.3), channel_id=1, source_target_pairs={{0,32},{16,48},{32,0},{48,16},{1,33},{17,49},{33,1},{49,17},{2,34}... | collective-permute-start | bytes 1572872 | tf_op jit(solution)/shard_map/ppermute | solution.py:314
  115.8 0.0 copy-done.2
  115.9 2.3 %collective-permute-start.4 = (bf16[8,256,128]{2,1,0:T(8,128)(2,1)S(1)}, bf16[8,256,128]{2,1,0:T(8,128)(2,1)S(1)}, u32[]{:S(2)}, u32[]{:S(2)}) collective-permute-start(bf16[8,256,128]{2,1,0:T(8,128)(2,1)S(1)} %copy-done.2), channel_id=1, source_target_pairs={{0,48},{16,0},{32,16},{48,32},{1,49},{17,1},{33,17},{49,33},{2,50}... | collective-permute-start | bytes 1572872 | tf_op jit(solution)/shard_map/ppermute | solution.py:314
  118.2 3.0 %collective-permute-start.5 = (bf16[8,256,128]{2,1,0:T(8,128)(2,1)}, bf16[8,256,128]{2,1,0:T(8,128)(2,1)S(1)}, u32[]{:S(2)}, u32[]{:S(2)}) collective-permute-start(bf16[8,256,128]{2,1,0:T(8,128)(2,1)} %combine.6), channel_id=1, source_target_pairs={{0,16},{16,32},{32,48},{48,0},{1,17},{17,33},{33,49},{49,1},{2,18}... | collective-permute-start | bytes 1572872 | tf_op jit(solution)/shard_map/ppermute | solution.py:314
  121.2 2.8 %combine.7 = bf16[8,256,128]{2,1,0:T(8,128)(2,1)} custom-call(s32[32]{0:T(128)} %get-tuple-element.10.count_ref.refs_0_, s32[96,128]{1,0:T(8,128)} %get-tuple-element.11.place_ref.refs_1_, f32[96,128]{1,0:T(8,128)} %fusion.4.refs_2_, bf16[96,128,128]{2,1,0:T(8,128)(2,1)} %get-tuple-element.14.refs_3_), custom_call_target="tpu_custom_call" | custom-call | tf_op jit(solution)/shard_map/combine/pallas_call | solution.py:297
  123.9 3.9 %collective-permute-done.3 = bf16[8,256,128]{2,1,0:T(8,128)(2,1)S(1)} collective-permute-done((bf16[8,256,128]{2,1,0:T(8,128)(2,1)S(1)}, bf16[8,256,128]{2,1,0:T(8,128)(2,1)S(1)}, u32[]{:S(2)}, u32[]{:S(2)}) %collective-permute-start.3) | collective-permute-done | bytes 524320 | tf_op jit(solution)/shard_map/ppermute | solution.py:314
  127.8 10.9 %collective-permute-done.4 = bf16[8,256,128]{2,1,0:T(8,128)(2,1)S(1)} collective-permute-done((bf16[8,256,128]{2,1,0:T(8,128)(2,1)S(1)}, bf16[8,256,128]{2,1,0:T(8,128)(2,1)S(1)}, u32[]{:S(2)}, u32[]{:S(2)}) %collective-permute-start.4) | collective-permute-done | bytes 524320 | tf_op jit(solution)/shard_map/ppermute | solution.py:314
  138.7 0.7 collective-permute-done.5
  139.5 1.3 add_convert_fusion
  140.8 20.5 %all_to_all.21 = bf16[8,256,128]{2,1,0:T(8,128)(2,1)S(1)} all-to-all(bf16[8,256,128]{2,1,0:T(8,128)(2,1)S(1)} %add_convert_fusion), channel_id=1, replica_groups=mesh['z'=8,'x'=4,'y'=8,'core'=2] {'z'}, dimensions={0} | all-to-all | bytes 1048576 | tf_op jit(solution)/shard_map/all_to_all | solution.py:317
  161.3 0.1 convert_reduce_fusion
  161.4 0.1 multiply_reduce_fusion
  161.5 13.5 %all_to_all.22 = f32[16,2,128]{2,1,0:T(2,128)S(1)} all-to-all(f32[16,2,128]{2,1,0:T(2,128)S(1)} %broadcast_in_dim.10), channel_id=1, replica_groups=mesh['z'=8,'x'=4,'y'=8,'core'=2] {'y','core'}, dimensions={0} | all-to-all | bytes 32768 | tf_op jit(solution)/shard_map/all_to_all | solution.py:222
  175.0 0.0 copy-done.8
  175.0 0.7 multiply_convert_fusion
  (10 shorter events, 0.1 us)
Async XLA Ops:
  27.7 45.5 %copy-start = (bf16[8,256,128]{2,1,0:T(8,128)(2,1)}, bf16[8,256,128]{2,1,0:T(8,128)(2,1)S(1)}, u32[]{:S(2)}) copy-start(bf16[8,256,128]{2,1,0:T(8,128)(2,1)S(1)} %all_to_all.20.tok0) | copy-start | bytes 1572868
  27.7 45.4 %collective-permute-start = (bf16[8,256,128]{2,1,0:T(8,128)(2,1)S(1)}, bf16[8,256,128]{2,1,0:T(8,128)(2,1)S(1)}, u32[]{:S(2)}, u32[]{:S(2)}) collective-permute-start(bf16[8,256,128]{2,1,0:T(8,128)(2,1)S(1)} %all_to_all.20.tok0), channel_id=1, source_target_pairs={{0,32},{16,48},{32,0},{48,16},{1,33},{17,49},{33,1},{49,17},{2,34}... | collective-permute-start | bytes 1572872 | tf_op jit(solution)/shard_map/ppermute | solution.py:242
  32.3 40.8 %collective-permute-start.1 = (bf16[8,256,128]{2,1,0:T(8,128)(2,1)S(1)}, bf16[8,256,128]{2,1,0:T(8,128)(2,1)S(1)}, u32[]{:S(2)}, u32[]{:S(2)}) collective-permute-start(bf16[8,256,128]{2,1,0:T(8,128)(2,1)S(1)} %all_to_all.20.tok0), channel_id=1, source_target_pairs={{0,16},{16,32},{32,48},{48,0},{1,17},{17,33},{33,49},{49,1},{2,18}... | collective-permute-start | bytes 1572872 | tf_op jit(solution)/shard_map/ppermute | solution.py:242
  34.6 38.6 %collective-permute-start.2 = (bf16[8,256,128]{2,1,0:T(8,128)(2,1)S(1)}, bf16[8,256,128]{2,1,0:T(8,128)(2,1)S(1)}, u32[]{:S(2)}, u32[]{:S(2)}) collective-permute-start(bf16[8,256,128]{2,1,0:T(8,128)(2,1)S(1)} %all_to_all.20.tok0), channel_id=1, source_target_pairs={{0,48},{16,0},{32,16},{48,32},{1,49},{17,1},{33,17},{49,33},{2,50}... | collective-permute-start | bytes 1572872 | tf_op jit(solution)/shard_map/ppermute | solution.py:242
  41.8 15.5 %all-to-all-start = ((f32[32,8,128]{2,1,0:T(8,128)}), f32[32,8,128]{2,1,0:T(8,128)S(1)}, u32[]{:S(2)}, u32[]{:S(2)}) async-start(f32[32,8,128]{2,1,0:T(8,128)} %bucket.1), calls=%async_computation | async-start | bytes 262144 | tf_op jit(solution)/shard_map/all_to_all | solution.py:255
  73.1 0.8 copy-start.4
  73.1 0.9 copy-start.5
  73.1 1.1 copy-start.6
  74.2 27.4 %copy-start.1 = (s32[96,128]{1,0:T(8,128)S(1)}, s32[96,128]{1,0:T(8,128)}, u32[]{:S(2)}) copy-start(s32[96,128]{1,0:T(8,128)} %get-tuple-element.11.place_ref.refs_1_) | copy-start | bytes 147460
  74.2 27.4 %copy-start.7 = (f32[96,128]{1,0:T(8,128)S(1)}, f32[96,128]{1,0:T(8,128)}, u32[]{:S(2)}) copy-start(f32[96,128]{1,0:T(8,128)} %get-tuple-element.13) | copy-start | bytes 147460
  105.2 5.7 %copy-start.3 = (bf16[8,256,128]{2,1,0:T(8,128)(2,1)S(1)}, bf16[8,256,128]{2,1,0:T(8,128)(2,1)}, u32[]{:S(2)}) copy-start(bf16[8,256,128]{2,1,0:T(8,128)(2,1)} %combine.4) | copy-start | bytes 1572868
  108.1 7.8 %copy-start.2 = (bf16[8,256,128]{2,1,0:T(8,128)(2,1)S(1)}, bf16[8,256,128]{2,1,0:T(8,128)(2,1)}, u32[]{:S(2)}) copy-start(bf16[8,256,128]{2,1,0:T(8,128)(2,1)} %combine.5) | copy-start | bytes 1572868
  110.9 16.9 %collective-permute-start.3 = (bf16[8,256,128]{2,1,0:T(8,128)(2,1)S(1)}, bf16[8,256,128]{2,1,0:T(8,128)(2,1)S(1)}, u32[]{:S(2)}, u32[]{:S(2)}) collective-permute-start(bf16[8,256,128]{2,1,0:T(8,128)(2,1)S(1)} %copy-done.3), channel_id=1, source_target_pairs={{0,32},{16,48},{32,0},{48,16},{1,33},{17,49},{33,1},{49,17},{2,34}... | collective-permute-start | bytes 1572872 | tf_op jit(solution)/shard_map/ppermute | solution.py:314
  115.9 22.9 %collective-permute-start.4 = (bf16[8,256,128]{2,1,0:T(8,128)(2,1)S(1)}, bf16[8,256,128]{2,1,0:T(8,128)(2,1)S(1)}, u32[]{:S(2)}, u32[]{:S(2)}) collective-permute-start(bf16[8,256,128]{2,1,0:T(8,128)(2,1)S(1)} %copy-done.2), channel_id=1, source_target_pairs={{0,48},{16,0},{32,16},{48,32},{1,49},{17,1},{33,17},{49,33},{2,50}... | collective-permute-start | bytes 1572872 | tf_op jit(solution)/shard_map/ppermute | solution.py:314
  118.2 21.3 %collective-permute-start.5 = (bf16[8,256,128]{2,1,0:T(8,128)(2,1)}, bf16[8,256,128]{2,1,0:T(8,128)(2,1)S(1)}, u32[]{:S(2)}, u32[]{:S(2)}) collective-permute-start(bf16[8,256,128]{2,1,0:T(8,128)(2,1)} %combine.6), channel_id=1, source_target_pairs={{0,16},{16,32},{32,48},{48,0},{1,17},{17,33},{33,49},{49,1},{2,18}... | collective-permute-start | bytes 1572872 | tf_op jit(solution)/shard_map/ppermute | solution.py:314
  123.9 51.1 %copy-start.8 = (f32[128]{0:T(128)S(1)}, f32[128]{0:T(128)}, u32[]{:S(2)}) copy-start(f32[128]{0:T(128)} %param.11) | copy-start | bytes 1540

commit v4 on v3

--- a/solution.py
+++ b/solution.py
@@ -135,11 +135,11 @@
     lax.fori_loop(0, n_ep, block, 0)
 
 
-def score_kernel(count_ref, place_ref, keys_ref, tok0, tok1, tok2, tok3, out_ref):
+def score_kernel(count_ref, place_ref, keys_ref, tok0, tok1, tok2, tok3, out_ref, found_ref):
     toks = (tok0, tok1, tok2, tok3)
     n_z, tok, _ = tok0.shape
     chunks = place_ref.shape[0] // (X * n_z)
-    out_ref[...] = jnp.zeros(out_ref.shape, jnp.float32)
+    found_ref[...] = jnp.zeros(found_ref.shape, jnp.float32)
     token_of = lax.broadcasted_iota(jnp.int32, (tok, LANES), 0)
 
     def line_scores(tokens, line):
@@ -153,7 +153,7 @@
         lines = [(g * n_z + z) * chunks for g in range(X)]
         found = [line_scores(toks[g][z], lines[g]) for g in range(X)]
         for line, value in zip(lines, found):
-            out_ref[pl.ds(line, 1), :] = value
+            found_ref[pl.ds(line, 1), :] = value
         return carry
 
     lax.fori_loop(0, n_z, first, 0)
@@ -163,13 +163,14 @@
 
             def chunk(c, inner, g=g):
                 line = (g * n_z + z) * chunks + c
-                out_ref[pl.ds(line, 1), :] = line_scores(toks[g][z], line)
+                found_ref[pl.ds(line, 1), :] = line_scores(toks[g][z], line)
                 return inner
 
             lax.fori_loop(1, chunks_of(count_ref[g * n_z + z]), chunk, 0)
         return carry
 
     lax.fori_loop(0, n_z, more, 0)
+    out_ref[...] = found_ref[...].astype(out_ref.dtype)
 
 
 def combine_kernel(count_ref, place_ref, hidden_ref, values_ref, out_ref, acc, *, group):
@@ -238,7 +239,7 @@
     shift = exp_dev.bit_length() - 1
     lines = n_ep * chunks
 
-    near = to_each(tokens, "z")
+    near = lax.all_gather(tokens, "z")
     groups = [near] + [lax.ppermute(near, "x", around(shift)) for shift in SHIFTS[1:]]
     listed = pl.pallas_call(
         lambda *refs: bucket_kernel(*refs, n_ep=n_ep, cap=cap, shift=shift),
@@ -283,13 +284,14 @@
     )(lax.axis_index("x").reshape(1), rows, count, place, gates, key_table, value_table)
     partial_score = pl.pallas_call(
         score_kernel,
-        out_shape=jax.ShapeDtypeStruct((lines, LANES), jnp.float32),
+        out_shape=jax.ShapeDtypeStruct((lines, LANES), jnp.bfloat16),
         in_specs=[smem()] + [vmem()] * 6,
         out_specs=vmem(),
+        scratch_shapes=[pltpu.VMEM((lines, LANES), jnp.float32)],
         interpret=INTERPRET,
         name="score",
     )(count, place, keys, *groups)
-    score = jnp.sum(lax.all_gather(partial_score, TP), axis=0)
+    score = jnp.sum(lax.all_gather(partial_score, TP).astype(jnp.float32), axis=0)
     hidden = jnp.where(place >= 0, jax.nn.gelu(score, approximate=False) * gates, 0.0)
 
     def combine(group):
@@ -310,9 +312,12 @@
             name="combine",
         )(count, place, hidden, values)
 
-    parts = [
-        lax.ppermute(combine(g), "x", around(-SHIFTS[g])) if g else combine(g) for g in (1, 2, 3, 0)
-    ]
+    parts = []
+    for g in (1, 2, 3, 0):
+        part = combine(g)
+        if g:
+            part = lax.ppermute(part, "x", around(-SHIFTS[g]))
+        parts.append(part)
     mine = sum(p.astype(jnp.float32) for p in parts).astype(jnp.bfloat16)
     back = lax.all_to_all(mine, "z", 0, 0, tiled=True)
     mixed = jnp.sum(back.astype(jnp.float32), axis=0)
@@ -326,4 +331,5 @@
     ep, tp = mesh.devices.shape
     fine = Mesh(mesh.devices.reshape(Z, ep // Z, tp // 2, 2), ("z", "x", "y", "core"))
     in_specs = (P(EP, TP), P(EP, None), P(EP, None), P(EP, TP), P(EP, TP), P(TP))
+
     return jax.shard_map(body, mesh=fine, in_specs=in_specs, out_specs=P(EP, TP), check_vma=False)

time: 177 us -> 181 us (1.023)
  blocking collectives: 82.6 us -> 90.6 us
  waiting for transfers between devices: 27.2 us -> 24.8 us
    all_gather x1 -> x2, blocking collectives: 21.8 us -> 54.8 us  [the longest x1 27.7 us: body(): lax.all_gather(partial_score, TP).astype(jnp.float32)]
    all_to_all x2 -> x1, blocking collectives: 40.3 us -> 13.5 us  [to_each(): lax.all_to_all(jnp.broadcast_to(value[None], (lax.axis_size(axis), *value...]
    all_to_all x1, waiting for transfers between devices: 11.7 us -> 9.4 us  [body(): listed = lax.all_to_all(listed, EP, 0, 0, tiled=True)]
where the time goes in v4:
time: 181 us; the launch traced here: 180 us
  blocking collectives  90.6 us (50%)
  Pallas kernels  32.3 us (18%)
  starting transfers between devices  25.3 us (14%)
  waiting for transfers between devices  24.8 us (14%)
  other arithmetic  4.22 us (2%)
  local copies, waits for them, and re-layouts  3.06 us (2%)
    all_gather x1, blocking collectives, body(): lax.all_gather(partial_score, TP).astype(jnp.float32)  27.7 us
    all_gather x1, blocking collectives, body(): near = lax.all_gather(tokens, 'z')  27.1 us
    all_to_all x1, blocking collectives, body(): back = lax.all_to_all(mine, 'z', 0, 0, tiled=True)  22.3 us
    ppermute x3, waiting for transfers between devices, body(): part = lax.ppermute(part, 'x', around(-SHIFTS[g]))  15.4 us
    all_to_all x1, blocking collectives, to_each(): lax.all_to_all(jnp.broadcast_to(value[None], (lax.axis_size(axis), *value...  13.5 us
    pallas_call x1, Pallas kernels, body(): pl.pallas_call(pick_kernel, out_shape=(jax.ShapeDtypeStruct((n_ep,), jnp....  12.6 us
    pallas_call x4, Pallas kernels, combine(): pl.pallas_call(lambda *refs: combine_kernel(*refs, group=group), out_shap...  11.2 us
    ppermute x3, starting transfers between devices, body(): lax.ppermute(near, 'x', around(shift))  11.1 us
  transfers between devices with their start and end apart: 7, of which 4 were waited for; matrix products, arithmetic and copies ran while one was open for 2% of the time, Pallas kernels for 10%

profile of v4, /device:TPU:1, one launch (start us, length us, event | category | flops | bytes accessed | tf_op | source)
XLA Modules:
  0.0 180.5 jit_solution(13417625999225064153)
XLA Ops:
  0.0 27.1 %all-gather = bf16[2048,128]{1,0:T(8,128)(2,1)S(1)} all-gather(bf16[256,128]{1,0:T(8,128)(2,1)} %param.6), channel_id=2, replica_groups=mesh['z'=8,'x'=4,'y'=8,'core'=2] {'z'}, dimensions={0}, use_global_device_ids=true | all-gather | bytes 589824 | tf_op jit(solution)/shard_map/all_gather | solution.py:242
  27.1 4.6 %collective-permute-start = (bf16[8,256,128]{2,1,0:T(8,128)(2,1)S(1)}, bf16[8,256,128]{2,1,0:T(8,128)(2,1)S(1)}, u32[]{:S(2)}, u32[]{:S(2)}) collective-permute-start(bf16[8,256,128]{2,1,0:T(8,128)(2,1)S(1)} %bitcast.9), channel_id=1, source_target_pairs={{0,32},{16,48},{32,0},{48,16},{1,33},{17,49},{33,1},{49,17},{2,34}... | collective-permute-start | bytes 1572872 | tf_op jit(solution)/shard_map/ppermute | solution.py:243
  31.8 2.2 %collective-permute-start.1 = (bf16[8,256,128]{2,1,0:T(8,128)(2,1)S(1)}, bf16[8,256,128]{2,1,0:T(8,128)(2,1)S(1)}, u32[]{:S(2)}, u32[]{:S(2)}) collective-permute-start(bf16[8,256,128]{2,1,0:T(8,128)(2,1)S(1)} %bitcast.10), channel_id=1, source_target_pairs={{0,16},{16,32},{32,48},{48,0},{1,17},{17,33},{33,49},{49,1},{2,18}... | collective-permute-start | bytes 1572872 | tf_op jit(solution)/shard_map/ppermute | solution.py:243
  34.0 4.3 %collective-permute-start.2 = (bf16[8,256,128]{2,1,0:T(8,128)(2,1)S(1)}, bf16[8,256,128]{2,1,0:T(8,128)(2,1)S(1)}, u32[]{:S(2)}, u32[]{:S(2)}) collective-permute-start(bf16[8,256,128]{2,1,0:T(8,128)(2,1)S(1)} %bitcast.11), channel_id=1, source_target_pairs={{0,48},{16,0},{32,16},{48,32},{1,49},{17,1},{33,17},{49,33},{2,50}... | collective-permute-start | bytes 1572872 | tf_op jit(solution)/shard_map/ppermute | solution.py:243
  38.3 3.0 %bucket.1 = f32[32,8,128]{2,1,0:T(8,128)} custom-call(s32[16,256]{1,0:T(8,128)} %bitcast.14, f32[16,256]{1,0:T(8,128)} %bitcast.15), custom_call_target="tpu_custom_call" | custom-call | tf_op jit(solution)/shard_map/bucket/pallas_call | solution.py:244
  41.3 3.9 %all-to-all-start = ((f32[32,8,128]{2,1,0:T(8,128)}), f32[32,8,128]{2,1,0:T(8,128)S(1)}, u32[]{:S(2)}, u32[]{:S(2)}) async-start(f32[32,8,128]{2,1,0:T(8,128)} %bucket.1), calls=%async_computation | async-start | bytes 262144 | tf_op jit(solution)/shard_map/all_to_all | solution.py:256
  45.1 9.4 %all-to-all-done = f32[32,8,128]{2,1,0:T(8,128)S(1)} async-done(((f32[32,8,128]{2,1,0:T(8,128)}), f32[32,8,128]{2,1,0:T(8,128)S(1)}, u32[]{:S(2)}, u32[]{:S(2)}) %all-to-all-start) | async-done | bytes 131104 | tf_op jit(solution)/shard_map/all_to_all | solution.py:256
  54.5 1.1 shift-right-arithmetic_add_fusion
  55.7 0.6 reshape.28.rows_ref
  56.3 0.6 reshape.29.place_ref
  57.0 0.6 reshape.30.gate_ref
  57.6 12.6 %pick.1 = (s32[32]{0:T(128)}, s32[96,128]{1,0:T(8,128)}, f32[96,128]{1,0:T(8,128)}, bf16[96,128,128]{2,1,0:T(8,128)(2,1)}, bf16[96,128,128]{2,1,0:T(8,128)(2,1)}) custom-call(s32[1]{0:T(128)} %bitcast.x_ref, s32[96,128]{1,0:T(8,128)} %reshape.28.rows_ref, s32[32]{0:T(128)} %get-tuple-element.16.count_ref, s32[96,128]{1,0:T(8,128)} %reshape.29.place_ref, ...), custom_call_target="tpu_custom_call" | custom-call | tf_op jit(solution)/shard_map/pick/pallas_call | solution.py:265
  70.2 0.0 copy-start.1
  70.2 0.0 copy-start.7
  70.3 0.0 collective-permute-done.tok1
  70.3 0.0 copy-start.4
  70.3 0.0 collective-permute-done.1.tok2
  70.3 0.0 copy-start.5
  70.3 0.0 collective-permute-done.2.tok3
  70.3 0.0 copy-start.6
  70.3 0.0 copy-done
  70.3 0.7 copy-done.4
  71.1 0.2 copy-done.5
  71.2 0.2 copy-done.6
  71.4 5.5 %score.1 = bf16[96,128]{1,0:T(8,128)(2,1)} custom-call(s32[32]{0:T(128)} %get-tuple-element.10.count_ref.refs_0_, s32[96,128]{1,0:T(8,128)} %get-tuple-element.11.place_ref.refs_1_, bf16[96,128,128]{2,1,0:T(8,128)(2,1)} %get-tuple-element.12.keys_ref, bf16[8,256,128]{2,1,0:T(8,128)(2,1)} %bitcast.12, bf16[8,256,128]{2,1,0:T(8,128)(2,1)} %copy-done.4, ...), custom_call_target="tpu_custom_call" | custom-call | tf_op jit(solution)/shard_map/score/pallas_call | solution.py:285
  76.9 27.7 %all-gather.1 = bf16[1536,128]{1,0:T(8,128)(2,1)S(1)} all-gather(bf16[96,128]{1,0:T(8,128)(2,1)} %score.1), channel_id=3, replica_groups=mesh['z'=8,'x'=4,'y'=8,'core'=2] {'y','core'}, dimensions={0}, use_global_device_ids=true | all-gather | bytes 417792 | tf_op jit(solution)/shard_map/all_gather | solution.py:294
  104.6 0.1 convert_reduce_fusion.1
  104.7 0.0 copy-done.1
  104.7 0.0 copy-done.7
  104.7 0.7 fusion.4.refs_2_
  105.4 2.8 %combine.4 = bf16[8,256,128]{2,1,0:T(8,128)(2,1)} custom-call(s32[32]{0:T(128)} %get-tuple-element.10.count_ref.refs_0_, s32[96,128]{1,0:T(8,128)} %get-tuple-element.11.place_ref.refs_1_, f32[96,128]{1,0:T(8,128)} %fusion.4.refs_2_, bf16[96,128,128]{2,1,0:T(8,128)(2,1)} %get-tuple-element.14.refs_3_), custom_call_target="tpu_custom_call" | custom-call | tf_op jit(solution)/shard_map/combine/pallas_call | solution.py:299
  108.2 2.8 %combine.5 = bf16[8,256,128]{2,1,0:T(8,128)(2,1)} custom-call(s32[32]{0:T(128)} %get-tuple-element.10.count_ref.refs_0_, s32[96,128]{1,0:T(8,128)} %get-tuple-element.11.place_ref.refs_1_, f32[96,128]{1,0:T(8,128)} %fusion.4.refs_2_, bf16[96,128,128]{2,1,0:T(8,128)(2,1)} %get-tuple-element.14.refs_3_), custom_call_target="tpu_custom_call" | custom-call | tf_op jit(solution)/shard_map/combine/pallas_call | solution.py:299
  111.1 2.8 %combine.6 = bf16[8,256,128]{2,1,0:T(8,128)(2,1)} custom-call(s32[32]{0:T(128)} %get-tuple-element.10.count_ref.refs_0_, s32[96,128]{1,0:T(8,128)} %get-tuple-element.11.place_ref.refs_1_, f32[96,128]{1,0:T(8,128)} %fusion.4.refs_2_, bf16[96,128,128]{2,1,0:T(8,128)(2,1)} %get-tuple-element.14.refs_3_), custom_call_target="tpu_custom_call" | custom-call | tf_op jit(solution)/shard_map/combine/pallas_call | solution.py:299
  113.9 0.0 copy-done.3
  113.9 2.8 %collective-permute-start.3 = (bf16[8,256,128]{2,1,0:T(8,128)(2,1)S(1)}, bf16[8,256,128]{2,1,0:T(8,128)(2,1)S(1)}, u32[]{:S(2)}, u32[]{:S(2)}) collective-permute-start(bf16[8,256,128]{2,1,0:T(8,128)(2,1)S(1)} %copy-done.3), channel_id=1, source_target_pairs={{0,32},{16,48},{32,0},{48,16},{1,33},{17,49},{33,1},{49,17},{2,34}... | collective-permute-start | bytes 1572872 | tf_op jit(solution)/shard_map/ppermute | solution.py:319
  116.7 0.0 copy-done.2
  116.7 5.5 %collective-permute-start.4 = (bf16[8,256,128]{2,1,0:T(8,128)(2,1)S(1)}, bf16[8,256,128]{2,1,0:T(8,128)(2,1)S(1)}, u32[]{:S(2)}, u32[]{:S(2)}) collective-permute-start(bf16[8,256,128]{2,1,0:T(8,128)(2,1)S(1)} %copy-done.2), channel_id=1, source_target_pairs={{0,48},{16,0},{32,16},{48,32},{1,49},{17,1},{33,17},{49,33},{2,50}... | collective-permute-start | bytes 1572872 | tf_op jit(solution)/shard_map/ppermute | solution.py:319
  122.3 1.9 %collective-permute-start.5 = (bf16[8,256,128]{2,1,0:T(8,128)(2,1)}, bf16[8,256,128]{2,1,0:T(8,128)(2,1)S(1)}, u32[]{:S(2)}, u32[]{:S(2)}) collective-permute-start(bf16[8,256,128]{2,1,0:T(8,128)(2,1)} %combine.6), channel_id=1, source_target_pairs={{0,16},{16,32},{32,48},{48,0},{1,17},{17,33},{33,49},{49,1},{2,18}... | collective-permute-start | bytes 1572872 | tf_op jit(solution)/shard_map/ppermute | solution.py:319
  124.2 2.8 %combine.7 = bf16[8,256,128]{2,1,0:T(8,128)(2,1)} custom-call(s32[32]{0:T(128)} %get-tuple-element.10.count_ref.refs_0_, s32[96,128]{1,0:T(8,128)} %get-tuple-element.11.place_ref.refs_1_, f32[96,128]{1,0:T(8,128)} %fusion.4.refs_2_, bf16[96,128,128]{2,1,0:T(8,128)(2,1)} %get-tuple-element.14.refs_3_), custom_call_target="tpu_custom_call" | custom-call | tf_op jit(solution)/shard_map/combine/pallas_call | solution.py:299
  127.0 3.6 %collective-permute-done.3 = bf16[8,256,128]{2,1,0:T(8,128)(2,1)S(1)} collective-permute-done((bf16[8,256,128]{2,1,0:T(8,128)(2,1)S(1)}, bf16[8,256,128]{2,1,0:T(8,128)(2,1)S(1)}, u32[]{:S(2)}, u32[]{:S(2)}) %collective-permute-start.3) | collective-permute-done | bytes 524320 | tf_op jit(solution)/shard_map/ppermute | solution.py:319
  130.6 11.1 %collective-permute-done.4 = bf16[8,256,128]{2,1,0:T(8,128)(2,1)S(1)} collective-permute-done((bf16[8,256,128]{2,1,0:T(8,128)(2,1)S(1)}, bf16[8,256,128]{2,1,0:T(8,128)(2,1)S(1)}, u32[]{:S(2)}, u32[]{:S(2)}) %collective-permute-start.4) | collective-permute-done | bytes 524320 | tf_op jit(solution)/shard_map/ppermute | solution.py:319
  141.7 0.6 collective-permute-done.5
  142.4 1.3 add_convert_fusion
  143.7 22.3 %all_to_all.15 = bf16[8,256,128]{2,1,0:T(8,128)(2,1)S(1)} all-to-all(bf16[8,256,128]{2,1,0:T(8,128)(2,1)S(1)} %add_convert_fusion), channel_id=1, replica_groups=mesh['z'=8,'x'=4,'y'=8,'core'=2] {'z'}, dimensions={0} | all-to-all | bytes 1048576 | tf_op jit(solution)/shard_map/all_to_all | solution.py:322
  166.0 0.1 convert_reduce_fusion
  166.0 0.1 multiply_reduce_fusion
  166.2 13.5 %all_to_all.16 = f32[16,2,128]{2,1,0:T(2,128)S(1)} all-to-all(f32[16,2,128]{2,1,0:T(2,128)S(1)} %broadcast_in_dim.12), channel_id=1, replica_groups=mesh['z'=8,'x'=4,'y'=8,'core'=2] {'y','core'}, dimensions={0} | all-to-all | bytes 32768 | tf_op jit(solution)/shard_map/all_to_all | solution.py:223
  179.7 0.7 multiply_convert_fusion
  (9 shorter events, 0.1 us)
Async XLA Ops:
  27.1 43.2 %copy-start = (bf16[2048,128]{1,0:T(8,128)(2,1)}, bf16[2048,128]{1,0:T(8,128)(2,1)S(1)}, u32[]{:S(2)}) copy-start(bf16[2048,128]{1,0:T(8,128)(2,1)S(1)} %all-gather) | copy-start | bytes 1572868
  27.1 43.1 %collective-permute-start = (bf16[8,256,128]{2,1,0:T(8,128)(2,1)S(1)}, bf16[8,256,128]{2,1,0:T(8,128)(2,1)S(1)}, u32[]{:S(2)}, u32[]{:S(2)}) collective-permute-start(bf16[8,256,128]{2,1,0:T(8,128)(2,1)S(1)} %bitcast.9), channel_id=1, source_target_pairs={{0,32},{16,48},{32,0},{48,16},{1,33},{17,49},{33,1},{49,17},{2,34}... | collective-permute-start | bytes 1572872 | tf_op jit(solution)/shard_map/ppermute | solution.py:243
  31.8 38.5 %collective-permute-start.1 = (bf16[8,256,128]{2,1,0:T(8,128)(2,1)S(1)}, bf16[8,256,128]{2,1,0:T(8,128)(2,1)S(1)}, u32[]{:S(2)}, u32[]{:S(2)}) collective-permute-start(bf16[8,256,128]{2,1,0:T(8,128)(2,1)S(1)} %bitcast.10), channel_id=1, source_target_pairs={{0,16},{16,32},{32,48},{48,0},{1,17},{17,33},{33,49},{49,1},{2,18}... | collective-permute-start | bytes 1572872 | tf_op jit(solution)/shard_map/ppermute | solution.py:243
  34.0 36.3 %collective-permute-start.2 = (bf16[8,256,128]{2,1,0:T(8,128)(2,1)S(1)}, bf16[8,256,128]{2,1,0:T(8,128)(2,1)S(1)}, u32[]{:S(2)}, u32[]{:S(2)}) collective-permute-start(bf16[8,256,128]{2,1,0:T(8,128)(2,1)S(1)} %bitcast.11), channel_id=1, source_target_pairs={{0,48},{16,0},{32,16},{48,32},{1,49},{17,1},{33,17},{49,33},{2,50}... | collective-permute-start | bytes 1572872 | tf_op jit(solution)/shard_map/ppermute | solution.py:243
  41.3 13.3 %all-to-all-start = ((f32[32,8,128]{2,1,0:T(8,128)}), f32[32,8,128]{2,1,0:T(8,128)S(1)}, u32[]{:S(2)}, u32[]{:S(2)}) async-start(f32[32,8,128]{2,1,0:T(8,128)} %bucket.1), calls=%async_computation | async-start | bytes 262144 | tf_op jit(solution)/shard_map/all_to_all | solution.py:256
  70.2 34.4 %copy-start.1 = (s32[96,128]{1,0:T(8,128)S(1)}, s32[96,128]{1,0:T(8,128)}, u32[]{:S(2)}) copy-start(s32[96,128]{1,0:T(8,128)} %get-tuple-element.11.place_ref.refs_1_) | copy-start | bytes 147460
  70.2 34.4 %copy-start.7 = (f32[96,128]{1,0:T(8,128)S(1)}, f32[96,128]{1,0:T(8,128)}, u32[]{:S(2)}) copy-start(f32[96,128]{1,0:T(8,128)} %get-tuple-element.13) | copy-start | bytes 147460
  70.3 0.8 copy-start.4
  70.3 0.9 copy-start.5
  70.3 1.1 copy-start.6
  108.2 5.7 %copy-start.3 = (bf16[8,256,128]{2,1,0:T(8,128)(2,1)S(1)}, bf16[8,256,128]{2,1,0:T(8,128)(2,1)}, u32[]{:S(2)}) copy-start(bf16[8,256,128]{2,1,0:T(8,128)(2,1)} %combine.4) | copy-start | bytes 1572868
  111.1 5.7 %copy-start.2 = (bf16[8,256,128]{2,1,0:T(8,128)(2,1)S(1)}, bf16[8,256,128]{2,1,0:T(8,128)(2,1)}, u32[]{:S(2)}) copy-start(bf16[8,256,128]{2,1,0:T(8,128)(2,1)} %combine.5) | copy-start | bytes 1572868
  113.9 16.7 %collective-permute-start.3 = (bf16[8,256,128]{2,1,0:T(8,128)(2,1)S(1)}, bf16[8,256,128]{2,1,0:T(8,128)(2,1)S(1)}, u32[]{:S(2)}, u32[]{:S(2)}) collective-permute-start(bf16[8,256,128]{2,1,0:T(8,128)(2,1)S(1)} %copy-done.3), channel_id=1, source_target_pairs={{0,32},{16,48},{32,0},{48,16},{1,33},{17,49},{33,1},{49,17},{2,34}... | collective-permute-start | bytes 1572872 | tf_op jit(solution)/shard_map/ppermute | solution.py:319
  116.7 25.0 %collective-permute-start.4 = (bf16[8,256,128]{2,1,0:T(8,128)(2,1)S(1)}, bf16[8,256,128]{2,1,0:T(8,128)(2,1)S(1)}, u32[]{:S(2)}, u32[]{:S(2)}) collective-permute-start(bf16[8,256,128]{2,1,0:T(8,128)(2,1)S(1)} %copy-done.2), channel_id=1, source_target_pairs={{0,48},{16,0},{32,16},{48,32},{1,49},{17,1},{33,17},{49,33},{2,50}... | collective-permute-start | bytes 1572872 | tf_op jit(solution)/shard_map/ppermute | solution.py:319
  122.3 20.1 %collective-permute-start.5 = (bf16[8,256,128]{2,1,0:T(8,128)(2,1)}, bf16[8,256,128]{2,1,0:T(8,128)(2,1)S(1)}, u32[]{:S(2)}, u32[]{:S(2)}) collective-permute-start(bf16[8,256,128]{2,1,0:T(8,128)(2,1)} %combine.6), channel_id=1, source_target_pairs={{0,16},{16,32},{32,48},{48,0},{1,17},{17,33},{33,49},{49,1},{2,18}... | collective-permute-start | bytes 1572872 | tf_op jit(solution)/shard_map/ppermute | solution.py:319
  127.0 52.7 %copy-start.8 = (f32[128]{0:T(128)S(1)}, f32[128]{0:T(128)}, u32[]{:S(2)}) copy-start(f32[128]{0:T(128)} %param.11) | copy-start | bytes 1540

commit v5 on v3

--- a/solution.py
+++ b/solution.py
@@ -11,6 +11,7 @@
 INTERPRET = False
 Z = 8
 X = 4
+ROOM = 24 * 1024 * 1024
 SHIFTS = (0, 2, 1, 3)
 EP = ("z", "x")
 TP = ("y", "core")
@@ -174,10 +175,11 @@
 
 def combine_kernel(count_ref, place_ref, hidden_ref, values_ref, out_ref, acc, *, group):
     n_z, tok, _ = out_ref.shape
-    chunks = place_ref.shape[0] // n_z
+    chunks = place_ref.shape[0] // (X * n_z)
     token_of = lax.broadcasted_iota(jnp.int32, (tok, LANES), 0)
 
-    def line_mix(line):
+    def line_mix(z, c):
+        line = (group * n_z + z) * chunks + c
         here = place_ref[pl.ds(line, 1), :] == token_of
         weight = jnp.where(here, hidden_ref[pl.ds(line, 1), :], 0.0)
         high = weight.astype(jnp.bfloat16)
@@ -191,7 +193,7 @@
 
     def first(half, carry):
         zs = [half * 4 + j for j in range(4)]
-        found = [line_mix(z * chunks) for z in zs]
+        found = [line_mix(z, 0) for z in zs]
         for z, value in zip(zs, found):
             acc[z] = value
         return carry
@@ -200,7 +202,7 @@
 
     def more(z, carry):
         def chunk(c, inner):
-            acc[z] += line_mix(z * chunks + c)
+            acc[z] += line_mix(z, c)
             return inner
 
         lax.fori_loop(1, chunks_of(count_ref[group * n_z + z]), chunk, 0)
@@ -212,6 +214,14 @@
 
 def vmem():
     return pl.BlockSpec(memory_space=pltpu.VMEM)
+
+
+def made(shape, dtype):
+    return jax.ShapeDtypeStruct(shape, dtype) if INTERPRET else pltpu.VMEM(shape, dtype)
+
+
+def held(value):
+    return value if INTERPRET else pltpu.with_memory_space_constraint(value, pltpu.VMEM)
 
 
 def smem():
@@ -238,7 +248,7 @@
     shift = exp_dev.bit_length() - 1
     lines = n_ep * chunks
 
-    near = to_each(tokens, "z")
+    near = lax.all_gather(tokens, "z")
     groups = [near] + [lax.ppermute(near, "x", around(shift)) for shift in SHIFTS[1:]]
     listed = pl.pallas_call(
         lambda *refs: bucket_kernel(*refs, n_ep=n_ep, cap=cap, shift=shift),
@@ -250,6 +260,7 @@
             pltpu.VMEM((cap, tok * picks), jnp.bfloat16),
         ],
         interpret=INTERPRET,
+        compiler_params=pltpu.CompilerParams(vmem_limit_bytes=ROOM),
         name="bucket",
     )(row_ids.T, row_gates.T)
     listed = lax.all_to_all(listed, EP, 0, 0, tiled=True)
@@ -260,7 +271,7 @@
     count = jnp.sum((codes > 0).astype(jnp.int32), axis=(1, 2))
 
     n_z = n_ep // X
-    picked = jax.ShapeDtypeStruct((lines, LANES, width), jnp.bfloat16)
+    picked = made((lines, LANES, width), jnp.bfloat16)
     count, place, gates, keys, values = pl.pallas_call(
         pick_kernel,
         out_shape=(
@@ -279,6 +290,7 @@
             pltpu.VMEM((LANES, width), jnp.float32),
         ],
         interpret=INTERPRET,
+        compiler_params=pltpu.CompilerParams(vmem_limit_bytes=ROOM),
         name="pick",
     )(lax.axis_index("x").reshape(1), rows, count, place, gates, key_table, value_table)
     partial_score = pl.pallas_call(
@@ -287,32 +299,30 @@
         in_specs=[smem()] + [vmem()] * 6,
         out_specs=vmem(),
         interpret=INTERPRET,
+        compiler_params=pltpu.CompilerParams(vmem_limit_bytes=ROOM),
         name="score",
-    )(count, place, keys, *groups)
+    )(count, place, held(keys), *[held(g) for g in groups])
     score = jnp.sum(lax.all_gather(partial_score, TP), axis=0)
     hidden = jnp.where(place >= 0, jax.nn.gelu(score, approximate=False) * gates, 0.0)
 
     def combine(group):
-        per = n_z * chunks
         return pl.pallas_call(
             lambda *refs: combine_kernel(*refs, group=group),
-            out_shape=jax.ShapeDtypeStruct((n_z, tok, width), jnp.bfloat16),
-            grid=(1,),
-            in_specs=[
-                smem(),
-                pl.BlockSpec((per, LANES), lambda i: (group, 0)),
-                pl.BlockSpec((per, LANES), lambda i: (group, 0)),
-                pl.BlockSpec((per, LANES, width), lambda i: (group, 0, 0)),
-            ],
-            out_specs=pl.BlockSpec((n_z, tok, width), lambda i: (0, 0, 0)),
+            out_shape=made((n_z, tok, width), jnp.bfloat16),
+            in_specs=[smem(), vmem(), vmem(), vmem()],
+            out_specs=vmem(),
             scratch_shapes=[pltpu.VMEM((n_z, tok, width), jnp.float32)],
             interpret=INTERPRET,
+            compiler_params=pltpu.CompilerParams(vmem_limit_bytes=ROOM),
             name="combine",
-        )(count, place, hidden, values)
-
-    parts = [
-        lax.ppermute(combine(g), "x", around(-SHIFTS[g])) if g else combine(g) for g in (1, 2, 3, 0)
-    ]
+        )(count, held(place), held(hidden), held(values))
+
+    parts = []
+    for g in (1, 2, 3, 0):
+        part = combine(g)
+        if g:
+            part = lax.ppermute(part, "x", around(-SHIFTS[g]))
+        parts.append(part)
     mine = sum(p.astype(jnp.float32) for p in parts).astype(jnp.bfloat16)
     back = lax.all_to_all(mine, "z", 0, 0, tiled=True)
     mixed = jnp.sum(back.astype(jnp.float32), axis=0)
@@ -326,4 +336,5 @@
     ep, tp = mesh.devices.shape
     fine = Mesh(mesh.devices.reshape(Z, ep // Z, tp // 2, 2), ("z", "x", "y", "core"))
     in_specs = (P(EP, TP), P(EP, None), P(EP, None), P(EP, TP), P(EP, TP), P(TP))
+
     return jax.shard_map(body, mesh=fine, in_specs=in_specs, out_specs=P(EP, TP), check_vma=False)

time: 177 us -> 176 us (level)
  blocking collectives: 82.6 us -> 93.8 us
  Pallas kernels: 32.4 us -> 21.9 us
    all_gather x0 -> x1, blocking collectives: none -> 28.6 us  [body(): near = lax.all_gather(tokens, 'z')]
    all_to_all x2 -> x1, blocking collectives: 40.3 us -> 13.5 us  [to_each(): lax.all_to_all(jnp.broadcast_to(value[None], (lax.axis_size(axis), *value...]
    all_gather x1, blocking collectives: 21.8 us -> 29.4 us  [body(): score = jnp.sum(lax.all_gather(partial_score, TP), axis=0)]
    pallas_call x4, Pallas kernels: 11.2 us -> 5.33 us  [combine(): pl.pallas_call(lambda *refs: combine_kernel(*refs, group=group), out_shap...]
    unnamed x18 -> x10, local copies, waits for them, and re-layouts: 1.12 us -> 3.88 us
    all_to_all x1, waiting for transfers between devices: 11.7 us -> 9.34 us  [body(): listed = lax.all_to_all(listed, EP, 0, 0, tiled=True)]
    pallas_call x1, Pallas kernels: 12.6 us -> 10.3 us  [body(): pl.pallas_call(pick_kernel, out_shape=(jax.ShapeDtypeStruct((n_ep,), jnp....]
    all_to_all x1, blocking collectives: 20.5 us -> 22.3 us  [body(): back = lax.all_to_all(mine, 'z', 0, 0, tiled=True)]
  transfers between devices with their start and end apart: 7 -> 7, of which waited for: 4 -> 4; matrix products, arithmetic and copies ran while one was open for 2% -> 0% of each run, Pallas kernels for 10% -> 8%
where the time goes in v5:
time: 176 us; the launch traced here: 175 us
  blocking collectives  93.8 us (53%)
  starting transfers between devices  26.1 us (15%)
  waiting for transfers between devices  26.1 us (15%)
  Pallas kernels  21.9 us (12%)
  local copies, waits for them, and re-layouts  3.97 us (2%)
  other arithmetic  3.2 us (2%)
    all_gather x1, blocking collectives, body(): score = jnp.sum(lax.all_gather(partial_score, TP), axis=0)  29.4 us
    all_gather x1, blocking collectives, body(): near = lax.all_gather(tokens, 'z')  28.6 us
    all_to_all x1, blocking collectives, body(): back = lax.all_to_all(mine, 'z', 0, 0, tiled=True)  22.3 us
    ppermute x3, waiting for transfers between devices, body(): part = lax.ppermute(part, 'x', around(-SHIFTS[g]))  16.8 us
    all_to_all x1, blocking collectives, to_each(): lax.all_to_all(jnp.broadcast_to(value[None], (lax.axis_size(axis), *value...  13.5 us
    ppermute x3, starting transfers between devices, body(): lax.ppermute(near, 'x', around(shift))  11.1 us
    pallas_call x1, Pallas kernels, body(): pl.pallas_call(pick_kernel, out_shape=(jax.ShapeDtypeStruct((n_ep,), jnp....  10.3 us
    ppermute x3, starting transfers between devices, body(): part = lax.ppermute(part, 'x', around(-SHIFTS[g]))  10.3 us
  transfers between devices with their start and end apart: 7, of which 4 were waited for; matrix products, arithmetic and copies ran while one was open for 0% of the time, Pallas kernels for 8%

profile of v5, /device:TPU:1, one launch (start us, length us, event | category | flops | bytes accessed | tf_op | source)
XLA Modules:
  0.0 175.3 jit_solution(6148365846546432476)
XLA Ops:
  0.0 28.6 %all-gather = bf16[2048,128]{1,0:T(8,128)(2,1)} all-gather(bf16[256,128]{1,0:T(8,128)(2,1)} %param.6), channel_id=2, replica_groups=mesh['z'=8,'x'=4,'y'=8,'core'=2] {'z'}, dimensions={0}, use_global_device_ids=true | all-gather | bytes 589824 | tf_op jit(solution)/shard_map/all_gather | solution.py:251
  28.6 4.6 %collective-permute-start = (bf16[8,256,128]{2,1,0:T(8,128)(2,1)}, bf16[8,256,128]{2,1,0:T(8,128)(2,1)}, u32[]{:S(2)}, u32[]{:S(2)}) collective-permute-start(bf16[8,256,128]{2,1,0:T(8,128)(2,1)} %bitcast.3.tok0), channel_id=1, source_target_pairs={{0,32},{16,48},{32,0},{48,16},{1,33},{17,49},{33,1},{49,17},{2,34}... | collective-permute-start | bytes 1572872 | tf_op jit(solution)/shard_map/ppermute | solution.py:252
  33.3 2.2 %collective-permute-start.1 = (bf16[8,256,128]{2,1,0:T(8,128)(2,1)}, bf16[8,256,128]{2,1,0:T(8,128)(2,1)}, u32[]{:S(2)}, u32[]{:S(2)}) collective-permute-start(bf16[8,256,128]{2,1,0:T(8,128)(2,1)} %bitcast.3.tok0), channel_id=1, source_target_pairs={{0,16},{16,32},{32,48},{48,0},{1,17},{17,33},{33,49},{49,1},{2,18}... | collective-permute-start | bytes 1572872 | tf_op jit(solution)/shard_map/ppermute | solution.py:252
  35.5 4.3 %collective-permute-start.2 = (bf16[8,256,128]{2,1,0:T(8,128)(2,1)}, bf16[8,256,128]{2,1,0:T(8,128)(2,1)}, u32[]{:S(2)}, u32[]{:S(2)}) collective-permute-start(bf16[8,256,128]{2,1,0:T(8,128)(2,1)} %bitcast.3.tok0), channel_id=1, source_target_pairs={{0,48},{16,0},{32,16},{48,32},{1,49},{17,1},{33,17},{49,33},{2,50}... | collective-permute-start | bytes 1572872 | tf_op jit(solution)/shard_map/ppermute | solution.py:252
  39.8 0.0 copy-start.2
  39.8 0.7 copy-done.2
  40.5 0.0 copy-start.3
  40.5 0.7 copy-done.3
  41.2 2.3 %bucket.1 = f32[32,8,128]{2,1,0:T(8,128)} custom-call(s32[16,256]{1,0:T(8,128)S(1)} %bitcast.8, f32[16,256]{1,0:T(8,128)S(1)} %bitcast.9), custom_call_target="tpu_custom_call" | custom-call | tf_op jit(solution)/shard_map/bucket/pallas_call | solution.py:253
  43.5 4.6 %all-to-all-start = ((f32[32,8,128]{2,1,0:T(8,128)}), f32[32,8,128]{2,1,0:T(8,128)S(1)}, u32[]{:S(2)}, u32[]{:S(2)}) async-start(f32[32,8,128]{2,1,0:T(8,128)} %bucket.1), calls=%async_computation | async-start | bytes 262144 | tf_op jit(solution)/shard_map/all_to_all | solution.py:266
  48.1 9.3 %all-to-all-done = f32[32,8,128]{2,1,0:T(8,128)S(1)} async-done(((f32[32,8,128]{2,1,0:T(8,128)}), f32[32,8,128]{2,1,0:T(8,128)S(1)}, u32[]{:S(2)}, u32[]{:S(2)}) %all-to-all-start) | async-done | bytes 131104 | tf_op jit(solution)/shard_map/all_to_all | solution.py:266
  57.5 0.7 shift-right-arithmetic_add_fusion
  58.3 0.0 copy-start
  58.3 1.2 copy-done
  59.5 0.0 copy-start.1
  59.5 1.2 copy-done.1
  60.7 10.3 %pick.1 = (s32[32]{0:T(128)S(1)}, s32[96,128]{1,0:T(8,128)S(1)}, f32[96,128]{1,0:T(8,128)S(1)}, bf16[96,128,128]{2,1,0:T(8,128)(2,1)S(1)}, bf16[96,128,128]{2,1,0:T(8,128)(2,1)S(1)}) custom-call(s32[1]{0:T(128)} %bitcast.x_ref, s32[96,128]{1,0:T(8,128)S(1)} %reshape.28.rows_ref, s32[32]{0:T(128)S(1)} %get-tuple-element.16.count_ref, ...), custom_call_target="tpu_custom_call" | custom-call | tf_op jit(solution)/shard_map/pick/pallas_call | solution.py:275
  71.1 0.0 collective-permute-done.tok1
  71.1 0.0 collective-permute-done.1.tok2
  71.1 0.0 collective-permute-done.2.tok3
  71.1 3.9 %score.1 = f32[96,128]{1,0:T(8,128)S(1)} custom-call(s32[32]{0:T(128)S(1)} %get-tuple-element.10.count_ref.refs_0_, s32[96,128]{1,0:T(8,128)S(1)} %get-tuple-element.11.place_ref.refs_1_, bf16[96,128,128]{2,1,0:T(8,128)(2,1)S(1)} %get-tuple-element.12.keys_ref, bf16[8,256,128]{2,1,0:T(8,128)(2,1)} %bitcast.3.tok0, ...), custom_call_target="tpu_custom_call" | custom-call | tf_op jit(solution)/shard_map/score/pallas_call | solution.py:296
  75.1 29.4 %all-gather.1 = f32[1536,128]{1,0:T(8,128)} all-gather(f32[96,128]{1,0:T(8,128)S(1)} %score.1), channel_id=3, replica_groups=mesh['z'=8,'x'=4,'y'=8,'core'=2] {'y','core'}, dimensions={0}, use_global_device_ids=true | all-gather | bytes 835584 | tf_op jit(solution)/shard_map/all_gather | solution.py:305
  104.4 1.2 reduce_sum.46
  105.6 0.1 fusion.4.refs_2_
  105.7 1.3 combine.4
  107.1 1.3 combine.5
  108.4 1.3 combine.6
  109.8 2.8 %collective-permute-start.3 = (bf16[8,256,128]{2,1,0:T(8,128)(2,1)S(1)}, bf16[8,256,128]{2,1,0:T(8,128)(2,1)S(1)}, u32[]{:S(2)}, u32[]{:S(2)}) collective-permute-start(bf16[8,256,128]{2,1,0:T(8,128)(2,1)S(1)} %combine.4), channel_id=1, source_target_pairs={{0,32},{16,48},{32,0},{48,16},{1,33},{17,49},{33,1},{49,17},{2,34}... | collective-permute-start | bytes 1572872 | tf_op jit(solution)/shard_map/ppermute | solution.py:324
  112.6 5.6 %collective-permute-start.4 = (bf16[8,256,128]{2,1,0:T(8,128)(2,1)S(1)}, bf16[8,256,128]{2,1,0:T(8,128)(2,1)S(1)}, u32[]{:S(2)}, u32[]{:S(2)}) collective-permute-start(bf16[8,256,128]{2,1,0:T(8,128)(2,1)S(1)} %combine.5), channel_id=1, source_target_pairs={{0,48},{16,0},{32,16},{48,32},{1,49},{17,1},{33,17},{49,33},{2,50}... | collective-permute-start | bytes 1572872 | tf_op jit(solution)/shard_map/ppermute | solution.py:324
  118.2 1.9 %collective-permute-start.5 = (bf16[8,256,128]{2,1,0:T(8,128)(2,1)S(1)}, bf16[8,256,128]{2,1,0:T(8,128)(2,1)S(1)}, u32[]{:S(2)}, u32[]{:S(2)}) collective-permute-start(bf16[8,256,128]{2,1,0:T(8,128)(2,1)S(1)} %combine.6), channel_id=1, source_target_pairs={{0,16},{16,32},{32,48},{48,0},{1,17},{17,33},{33,49},{49,1},{2,18}... | collective-permute-start | bytes 1572872 | tf_op jit(solution)/shard_map/ppermute | solution.py:324
  120.1 1.3 combine.7
  121.5 0.0 copy-start.4
  121.5 5.0 %collective-permute-done.3 = bf16[8,256,128]{2,1,0:T(8,128)(2,1)S(1)} collective-permute-done((bf16[8,256,128]{2,1,0:T(8,128)(2,1)S(1)}, bf16[8,256,128]{2,1,0:T(8,128)(2,1)S(1)}, u32[]{:S(2)}, u32[]{:S(2)}) %collective-permute-start.3) | collective-permute-done | bytes 524320 | tf_op jit(solution)/shard_map/ppermute | solution.py:324
  126.5 11.1 %collective-permute-done.4 = bf16[8,256,128]{2,1,0:T(8,128)(2,1)S(1)} collective-permute-done((bf16[8,256,128]{2,1,0:T(8,128)(2,1)S(1)}, bf16[8,256,128]{2,1,0:T(8,128)(2,1)S(1)}, u32[]{:S(2)}, u32[]{:S(2)}) %collective-permute-start.4) | collective-permute-done | bytes 524320 | tf_op jit(solution)/shard_map/ppermute | solution.py:324
  137.6 0.6 collective-permute-done.5
  138.2 0.3 add_convert_fusion
  138.5 22.3 %all_to_all.15 = bf16[8,256,128]{2,1,0:T(8,128)(2,1)S(1)} all-to-all(bf16[8,256,128]{2,1,0:T(8,128)(2,1)S(1)} %add_convert_fusion), channel_id=1, replica_groups=mesh['z'=8,'x'=4,'y'=8,'core'=2] {'z'}, dimensions={0} | all-to-all | bytes 1048576 | tf_op jit(solution)/shard_map/all_to_all | solution.py:327
  160.8 0.1 convert_reduce_fusion
  160.9 0.1 multiply_reduce_fusion
  161.0 13.5 %all_to_all.16 = f32[16,2,128]{2,1,0:T(2,128)S(1)} all-to-all(f32[16,2,128]{2,1,0:T(2,128)S(1)} %broadcast_in_dim.12), channel_id=1, replica_groups=mesh['z'=8,'x'=4,'y'=8,'core'=2] {'y','core'}, dimensions={0} | all-to-all | bytes 32768 | tf_op jit(solution)/shard_map/all_to_all | solution.py:232
  174.6 0.0 copy-done.4
  174.6 0.7 multiply_convert_fusion
  (7 shorter events, 0.1 us)
Async XLA Ops:
  28.6 42.4 %collective-permute-start = (bf16[8,256,128]{2,1,0:T(8,128)(2,1)}, bf16[8,256,128]{2,1,0:T(8,128)(2,1)}, u32[]{:S(2)}, u32[]{:S(2)}) collective-permute-start(bf16[8,256,128]{2,1,0:T(8,128)(2,1)} %bitcast.3.tok0), channel_id=1, source_target_pairs={{0,32},{16,48},{32,0},{48,16},{1,33},{17,49},{33,1},{49,17},{2,34}... | collective-permute-start | bytes 1572872 | tf_op jit(solution)/shard_map/ppermute | solution.py:252
  33.3 37.8 %collective-permute-start.1 = (bf16[8,256,128]{2,1,0:T(8,128)(2,1)}, bf16[8,256,128]{2,1,0:T(8,128)(2,1)}, u32[]{:S(2)}, u32[]{:S(2)}) collective-permute-start(bf16[8,256,128]{2,1,0:T(8,128)(2,1)} %bitcast.3.tok0), channel_id=1, source_target_pairs={{0,16},{16,32},{32,48},{48,0},{1,17},{17,33},{33,49},{49,1},{2,18}... | collective-permute-start | bytes 1572872 | tf_op jit(solution)/shard_map/ppermute | solution.py:252
  35.5 35.6 %collective-permute-start.2 = (bf16[8,256,128]{2,1,0:T(8,128)(2,1)}, bf16[8,256,128]{2,1,0:T(8,128)(2,1)}, u32[]{:S(2)}, u32[]{:S(2)}) collective-permute-start(bf16[8,256,128]{2,1,0:T(8,128)(2,1)} %bitcast.3.tok0), channel_id=1, source_target_pairs={{0,48},{16,0},{32,16},{48,32},{1,49},{17,1},{33,17},{49,33},{2,50}... | collective-permute-start | bytes 1572872 | tf_op jit(solution)/shard_map/ppermute | solution.py:252
  39.8 0.7 copy-start.2
  40.5 0.7 copy-start.3
  43.5 14.0 %all-to-all-start = ((f32[32,8,128]{2,1,0:T(8,128)}), f32[32,8,128]{2,1,0:T(8,128)S(1)}, u32[]{:S(2)}, u32[]{:S(2)}) async-start(f32[32,8,128]{2,1,0:T(8,128)} %bucket.1), calls=%async_computation | async-start | bytes 262144 | tf_op jit(solution)/shard_map/all_to_all | solution.py:266
  58.3 1.2 copy-start
  59.5 1.2 copy-start.1
  109.8 16.8 %collective-permute-start.3 = (bf16[8,256,128]{2,1,0:T(8,128)(2,1)S(1)}, bf16[8,256,128]{2,1,0:T(8,128)(2,1)S(1)}, u32[]{:S(2)}, u32[]{:S(2)}) collective-permute-start(bf16[8,256,128]{2,1,0:T(8,128)(2,1)S(1)} %combine.4), channel_id=1, source_target_pairs={{0,32},{16,48},{32,0},{48,16},{1,33},{17,49},{33,1},{49,17},{2,34}... | collective-permute-start | bytes 1572872 | tf_op jit(solution)/shard_map/ppermute | solution.py:324
  112.6 25.0 %collective-permute-start.4 = (bf16[8,256,128]{2,1,0:T(8,128)(2,1)S(1)}, bf16[8,256,128]{2,1,0:T(8,128)(2,1)S(1)}, u32[]{:S(2)}, u32[]{:S(2)}) collective-permute-start(bf16[8,256,128]{2,1,0:T(8,128)(2,1)S(1)} %combine.5), channel_id=1, source_target_pairs={{0,48},{16,0},{32,16},{48,32},{1,49},{17,1},{33,17},{49,33},{2,50}... | collective-permute-start | bytes 1572872 | tf_op jit(solution)/shard_map/ppermute | solution.py:324
  118.2 20.0 %collective-permute-start.5 = (bf16[8,256,128]{2,1,0:T(8,128)(2,1)S(1)}, bf16[8,256,128]{2,1,0:T(8,128)(2,1)S(1)}, u32[]{:S(2)}, u32[]{:S(2)}) collective-permute-start(bf16[8,256,128]{2,1,0:T(8,128)(2,1)S(1)} %combine.6), channel_id=1, source_target_pairs={{0,16},{16,32},{32,48},{48,0},{1,17},{17,33},{33,49},{49,1},{2,18}... | collective-permute-start | bytes 1572872 | tf_op jit(solution)/shard_map/ppermute | solution.py:324
  121.5 53.1 %copy-start.4 = (f32[128]{0:T(128)S(1)}, f32[128]{0:T(128)}, u32[]{:S(2)}) copy-start(f32[128]{0:T(128)} %param.11) | copy-start | bytes 1540

commit v6 on v5

--- a/solution.py
+++ b/solution.py
@@ -220,8 +220,8 @@
     return jax.ShapeDtypeStruct(shape, dtype) if INTERPRET else pltpu.VMEM(shape, dtype)
 
 
-def held(value):
-    return value if INTERPRET else pltpu.with_memory_space_constraint(value, pltpu.VMEM)
+def held(value, where=pltpu.VMEM):
+    return value if INTERPRET else pltpu.with_memory_space_constraint(value, where)
 
 
 def smem():
@@ -248,7 +248,7 @@
     shift = exp_dev.bit_length() - 1
     lines = n_ep * chunks
 
-    near = lax.all_gather(tokens, "z")
+    near = to_each(tokens, "z")
     groups = [near] + [lax.ppermute(near, "x", around(shift)) for shift in SHIFTS[1:]]
     listed = pl.pallas_call(
         lambda *refs: bucket_kernel(*refs, n_ep=n_ep, cap=cap, shift=shift),
@@ -292,7 +292,15 @@
         interpret=INTERPRET,
         compiler_params=pltpu.CompilerParams(vmem_limit_bytes=ROOM),
         name="pick",
-    )(lax.axis_index("x").reshape(1), rows, count, place, gates, key_table, value_table)
+    )(
+        lax.axis_index("x").reshape(1),
+        rows,
+        count,
+        place,
+        gates,
+        held(key_table, pltpu.HBM),
+        held(value_table, pltpu.HBM),
+    )
     partial_score = pl.pallas_call(
         score_kernel,
         out_shape=jax.ShapeDtypeStruct((lines, LANES), jnp.float32),

time: 176 us -> 168 us (0.955)
  blocking collectives: 93.8 us -> 86.1 us
  waiting for transfers between devices: 26.1 us -> 28 us
    all_gather x1 -> x0, blocking collectives: 28.6 us -> none  [body(): near = lax.all_gather(tokens, 'z')]
    all_to_all x1 -> x2, blocking collectives: 13.5 us -> 40.4 us  [to_each(): lax.all_to_all(jnp.broadcast_to(value[None], (lax.axis_size(axis), *value...]
    all_gather x1, blocking collectives: 29.4 us -> 23.5 us  [body(): score = jnp.sum(lax.all_gather(partial_score, TP), axis=0)]
    unnamed x10 -> x6, local copies, waits for them, and re-layouts: 3.88 us -> 1.44 us
    all_to_all x1, waiting for transfers between devices: 9.34 us -> 11.2 us  [body(): listed = lax.all_to_all(listed, EP, 0, 0, tiled=True)]
where the time goes in v6:
time: 168 us; the launch traced here: 167 us
  blocking collectives  86.1 us (51%)
  waiting for transfers between devices  28 us (17%)
  starting transfers between devices  25.3 us (15%)
  Pallas kernels  22.1 us (13%)
  other arithmetic  3.2 us (2%)
  local copies, waits for them, and re-layouts  2.44 us (1%)
    all_to_all x2, blocking collectives, to_each(): lax.all_to_all(jnp.broadcast_to(value[None], (lax.axis_size(axis), *value...  40.4 us
    all_gather x1, blocking collectives, body(): score = jnp.sum(lax.all_gather(partial_score, TP), axis=0)  23.5 us
    all_to_all x1, blocking collectives, body(): back = lax.all_to_all(mine, 'z', 0, 0, tiled=True)  22.2 us
    ppermute x3, waiting for transfers between devices, body(): part = lax.ppermute(part, 'x', around(-SHIFTS[g]))  16.8 us
    all_to_all x1, waiting for transfers between devices, body(): listed = lax.all_to_all(listed, EP, 0, 0, tiled=True)  11.2 us
    ppermute x3, starting transfers between devices, body(): lax.ppermute(near, 'x', around(shift))  11.1 us
    pallas_call x1, Pallas kernels, body(): pl.pallas_call(pick_kernel, out_shape=(jax.ShapeDtypeStruct((n_ep,), jnp....  10.6 us
    ppermute x3, starting transfers between devices, body(): part = lax.ppermute(part, 'x', around(-SHIFTS[g]))  10.3 us
  transfers between devices with their start and end apart: 7, of which 4 were waited for; matrix products, arithmetic and copies ran while one was open for 0% of the time, Pallas kernels for 8%

profile of v6, /device:TPU:1, one launch (start us, length us, event | category | flops | bytes accessed | tf_op | source)
XLA Modules:
  0.0 167.4 jit_solution(4088908325532979615)
XLA Ops:
  0.0 0.9 broadcast_in_dim.8
  0.9 26.9 %all_to_all.20.tok0 = bf16[8,256,128]{2,1,0:T(8,128)(2,1)} all-to-all(bf16[8,256,128]{2,1,0:T(8,128)(2,1)S(1)} %broadcast_in_dim.8), channel_id=1, replica_groups=mesh['z'=8,'x'=4,'y'=8,'core'=2] {'z'}, dimensions={0} | all-to-all | bytes 1048576 | tf_op jit(solution)/shard_map/all_to_all | solution.py:232
  27.8 4.6 %collective-permute-start = (bf16[8,256,128]{2,1,0:T(8,128)(2,1)}, bf16[8,256,128]{2,1,0:T(8,128)(2,1)}, u32[]{:S(2)}, u32[]{:S(2)}) collective-permute-start(bf16[8,256,128]{2,1,0:T(8,128)(2,1)} %all_to_all.20.tok0), channel_id=1, source_target_pairs={{0,32},{16,48},{32,0},{48,16},{1,33},{17,49},{33,1},{49,17},{2,34}... | collective-permute-start | bytes 1572872 | tf_op jit(solution)/shard_map/ppermute | solution.py:252
  32.4 2.2 %collective-permute-start.1 = (bf16[8,256,128]{2,1,0:T(8,128)(2,1)}, bf16[8,256,128]{2,1,0:T(8,128)(2,1)}, u32[]{:S(2)}, u32[]{:S(2)}) collective-permute-start(bf16[8,256,128]{2,1,0:T(8,128)(2,1)} %all_to_all.20.tok0), channel_id=1, source_target_pairs={{0,16},{16,32},{32,48},{48,0},{1,17},{17,33},{33,49},{49,1},{2,18}... | collective-permute-start | bytes 1572872 | tf_op jit(solution)/shard_map/ppermute | solution.py:252
  34.7 4.3 %collective-permute-start.2 = (bf16[8,256,128]{2,1,0:T(8,128)(2,1)}, bf16[8,256,128]{2,1,0:T(8,128)(2,1)}, u32[]{:S(2)}, u32[]{:S(2)}) collective-permute-start(bf16[8,256,128]{2,1,0:T(8,128)(2,1)} %all_to_all.20.tok0), channel_id=1, source_target_pairs={{0,48},{16,0},{32,16},{48,32},{1,49},{17,1},{33,17},{49,33},{2,50}... | collective-permute-start | bytes 1572872 | tf_op jit(solution)/shard_map/ppermute | solution.py:252
  38.9 0.0 copy-start
  39.0 0.7 copy-done
  39.7 0.0 copy-start.1
  39.7 0.7 copy-done.1
  40.4 2.3 %bucket.1 = f32[32,8,128]{2,1,0:T(8,128)} custom-call(s32[16,256]{1,0:T(8,128)S(1)} %bitcast.7, f32[16,256]{1,0:T(8,128)S(1)} %bitcast.8), custom_call_target="tpu_custom_call" | custom-call | tf_op jit(solution)/shard_map/bucket/pallas_call | solution.py:253
  42.6 3.9 %all-to-all-start = ((f32[32,8,128]{2,1,0:T(8,128)}), f32[32,8,128]{2,1,0:T(8,128)S(1)}, u32[]{:S(2)}, u32[]{:S(2)}) async-start(f32[32,8,128]{2,1,0:T(8,128)} %bucket.1), calls=%async_computation | async-start | bytes 262144 | tf_op jit(solution)/shard_map/all_to_all | solution.py:266
  46.5 11.2 %all-to-all-done = f32[32,8,128]{2,1,0:T(8,128)S(1)} async-done(((f32[32,8,128]{2,1,0:T(8,128)}), f32[32,8,128]{2,1,0:T(8,128)S(1)}, u32[]{:S(2)}, u32[]{:S(2)}) %all-to-all-start) | async-done | bytes 131104 | tf_op jit(solution)/shard_map/all_to_all | solution.py:266
  57.8 0.7 shift-right-arithmetic_add_fusion
  58.5 10.6 %pick.1 = (s32[32]{0:T(128)S(1)}, s32[96,128]{1,0:T(8,128)S(1)}, f32[96,128]{1,0:T(8,128)S(1)}, bf16[96,128,128]{2,1,0:T(8,128)(2,1)S(1)}, bf16[96,128,128]{2,1,0:T(8,128)(2,1)S(1)}) custom-call(s32[1]{0:T(128)} %bitcast.x_ref, s32[96,128]{1,0:T(8,128)S(1)} %reshape.29.rows_ref, s32[32]{0:T(128)S(1)} %get-tuple-element.16.count_ref, ...), custom_call_target="tpu_custom_call" | custom-call | tf_op jit(solution)/shard_map/pick/pallas_call | solution.py:275
  69.1 0.0 collective-permute-done.tok1
  69.1 0.0 collective-permute-done.1.tok2
  69.1 0.0 collective-permute-done.2.tok3
  69.1 4.0 %score.1 = f32[96,128]{1,0:T(8,128)S(1)} custom-call(s32[32]{0:T(128)S(1)} %get-tuple-element.10.count_ref.refs_0_, s32[96,128]{1,0:T(8,128)S(1)} %get-tuple-element.11.place_ref.refs_1_, bf16[96,128,128]{2,1,0:T(8,128)(2,1)S(1)} %get-tuple-element.12.keys_ref, bf16[8,256,128]{2,1,0:T(8,128)(2,1)} %all_to_all.20.tok0, ...), custom_call_target="tpu_custom_call" | custom-call | tf_op jit(solution)/shard_map/score/pallas_call | solution.py:304
  73.1 23.5 %all-gather = f32[1536,128]{1,0:T(8,128)} all-gather(f32[96,128]{1,0:T(8,128)S(1)} %score.1), channel_id=2, replica_groups=mesh['z'=8,'x'=4,'y'=8,'core'=2] {'y','core'}, dimensions={0}, use_global_device_ids=true | all-gather | bytes 835584 | tf_op jit(solution)/shard_map/all_gather | solution.py:313
  96.6 1.2 reduce_sum.46
  97.7 0.1 fusion.4.refs_2_
  97.9 1.3 combine.4
  99.2 1.3 combine.5
  100.5 1.3 combine.6
  101.9 2.8 %collective-permute-start.3 = (bf16[8,256,128]{2,1,0:T(8,128)(2,1)S(1)}, bf16[8,256,128]{2,1,0:T(8,128)(2,1)S(1)}, u32[]{:S(2)}, u32[]{:S(2)}) collective-permute-start(bf16[8,256,128]{2,1,0:T(8,128)(2,1)S(1)} %combine.4), channel_id=1, source_target_pairs={{0,32},{16,48},{32,0},{48,16},{1,33},{17,49},{33,1},{49,17},{2,34}... | collective-permute-start | bytes 1572872 | tf_op jit(solution)/shard_map/ppermute | solution.py:332
  104.7 5.6 %collective-permute-start.4 = (bf16[8,256,128]{2,1,0:T(8,128)(2,1)S(1)}, bf16[8,256,128]{2,1,0:T(8,128)(2,1)S(1)}, u32[]{:S(2)}, u32[]{:S(2)}) collective-permute-start(bf16[8,256,128]{2,1,0:T(8,128)(2,1)S(1)} %combine.5), channel_id=1, source_target_pairs={{0,48},{16,0},{32,16},{48,32},{1,49},{17,1},{33,17},{49,33},{2,50}... | collective-permute-start | bytes 1572872 | tf_op jit(solution)/shard_map/ppermute | solution.py:332
  110.3 1.9 %collective-permute-start.5 = (bf16[8,256,128]{2,1,0:T(8,128)(2,1)S(1)}, bf16[8,256,128]{2,1,0:T(8,128)(2,1)S(1)}, u32[]{:S(2)}, u32[]{:S(2)}) collective-permute-start(bf16[8,256,128]{2,1,0:T(8,128)(2,1)S(1)} %combine.6), channel_id=1, source_target_pairs={{0,16},{16,32},{32,48},{48,0},{1,17},{17,33},{33,49},{49,1},{2,18}... | collective-permute-start | bytes 1572872 | tf_op jit(solution)/shard_map/ppermute | solution.py:332
  112.2 1.3 combine.7
  113.6 0.0 copy-start.2
  113.6 5.0 %collective-permute-done.3 = bf16[8,256,128]{2,1,0:T(8,128)(2,1)S(1)} collective-permute-done((bf16[8,256,128]{2,1,0:T(8,128)(2,1)S(1)}, bf16[8,256,128]{2,1,0:T(8,128)(2,1)S(1)}, u32[]{:S(2)}, u32[]{:S(2)}) %collective-permute-start.3) | collective-permute-done | bytes 524320 | tf_op jit(solution)/shard_map/ppermute | solution.py:332
  118.6 11.1 %collective-permute-done.4 = bf16[8,256,128]{2,1,0:T(8,128)(2,1)S(1)} collective-permute-done((bf16[8,256,128]{2,1,0:T(8,128)(2,1)S(1)}, bf16[8,256,128]{2,1,0:T(8,128)(2,1)S(1)}, u32[]{:S(2)}, u32[]{:S(2)}) %collective-permute-start.4) | collective-permute-done | bytes 524320 | tf_op jit(solution)/shard_map/ppermute | solution.py:332
  129.7 0.7 collective-permute-done.5
  130.4 0.3 add_convert_fusion
  130.6 22.2 %all_to_all.21 = bf16[8,256,128]{2,1,0:T(8,128)(2,1)S(1)} all-to-all(bf16[8,256,128]{2,1,0:T(8,128)(2,1)S(1)} %add_convert_fusion), channel_id=1, replica_groups=mesh['z'=8,'x'=4,'y'=8,'core'=2] {'z'}, dimensions={0} | all-to-all | bytes 1048576 | tf_op jit(solution)/shard_map/all_to_all | solution.py:335
  152.9 0.1 convert_reduce_fusion
  153.0 0.1 multiply_reduce_fusion
  153.1 13.5 %all_to_all.22 = f32[16,2,128]{2,1,0:T(2,128)S(1)} all-to-all(f32[16,2,128]{2,1,0:T(2,128)S(1)} %broadcast_in_dim.10), channel_id=1, replica_groups=mesh['z'=8,'x'=4,'y'=8,'core'=2] {'y','core'}, dimensions={0} | all-to-all | bytes 32768 | tf_op jit(solution)/shard_map/all_to_all | solution.py:232
  166.6 0.0 copy-done.2
  166.6 0.7 multiply_convert_fusion
  (7 shorter events, 0.1 us)
Async XLA Ops:
  27.8 41.3 %collective-permute-start = (bf16[8,256,128]{2,1,0:T(8,128)(2,1)}, bf16[8,256,128]{2,1,0:T(8,128)(2,1)}, u32[]{:S(2)}, u32[]{:S(2)}) collective-permute-start(bf16[8,256,128]{2,1,0:T(8,128)(2,1)} %all_to_all.20.tok0), channel_id=1, source_target_pairs={{0,32},{16,48},{32,0},{48,16},{1,33},{17,49},{33,1},{49,17},{2,34}... | collective-permute-start | bytes 1572872 | tf_op jit(solution)/shard_map/ppermute | solution.py:252
  32.4 36.7 %collective-permute-start.1 = (bf16[8,256,128]{2,1,0:T(8,128)(2,1)}, bf16[8,256,128]{2,1,0:T(8,128)(2,1)}, u32[]{:S(2)}, u32[]{:S(2)}) collective-permute-start(bf16[8,256,128]{2,1,0:T(8,128)(2,1)} %all_to_all.20.tok0), channel_id=1, source_target_pairs={{0,16},{16,32},{32,48},{48,0},{1,17},{17,33},{33,49},{49,1},{2,18}... | collective-permute-start | bytes 1572872 | tf_op jit(solution)/shard_map/ppermute | solution.py:252
  34.7 34.5 %collective-permute-start.2 = (bf16[8,256,128]{2,1,0:T(8,128)(2,1)}, bf16[8,256,128]{2,1,0:T(8,128)(2,1)}, u32[]{:S(2)}, u32[]{:S(2)}) collective-permute-start(bf16[8,256,128]{2,1,0:T(8,128)(2,1)} %all_to_all.20.tok0), channel_id=1, source_target_pairs={{0,48},{16,0},{32,16},{48,32},{1,49},{17,1},{33,17},{49,33},{2,50}... | collective-permute-start | bytes 1572872 | tf_op jit(solution)/shard_map/ppermute | solution.py:252
  38.9 0.7 copy-start
  39.7 0.7 copy-start.1
  42.6 15.1 %all-to-all-start = ((f32[32,8,128]{2,1,0:T(8,128)}), f32[32,8,128]{2,1,0:T(8,128)S(1)}, u32[]{:S(2)}, u32[]{:S(2)}) async-start(f32[32,8,128]{2,1,0:T(8,128)} %bucket.1), calls=%async_computation | async-start | bytes 262144 | tf_op jit(solution)/shard_map/all_to_all | solution.py:266
  101.9 16.8 %collective-permute-start.3 = (bf16[8,256,128]{2,1,0:T(8,128)(2,1)S(1)}, bf16[8,256,128]{2,1,0:T(8,128)(2,1)S(1)}, u32[]{:S(2)}, u32[]{:S(2)}) collective-permute-start(bf16[8,256,128]{2,1,0:T(8,128)(2,1)S(1)} %combine.4), channel_id=1, source_target_pairs={{0,32},{16,48},{32,0},{48,16},{1,33},{17,49},{33,1},{49,17},{2,34}... | collective-permute-start | bytes 1572872 | tf_op jit(solution)/shard_map/ppermute | solution.py:332
  104.7 25.0 %collective-permute-start.4 = (bf16[8,256,128]{2,1,0:T(8,128)(2,1)S(1)}, bf16[8,256,128]{2,1,0:T(8,128)(2,1)S(1)}, u32[]{:S(2)}, u32[]{:S(2)}) collective-permute-start(bf16[8,256,128]{2,1,0:T(8,128)(2,1)S(1)} %combine.5), channel_id=1, source_target_pairs={{0,48},{16,0},{32,16},{48,32},{1,49},{17,1},{33,17},{49,33},{2,50}... | collective-permute-start | bytes 1572872 | tf_op jit(solution)/shard_map/ppermute | solution.py:332
  110.3 20.0 %collective-permute-start.5 = (bf16[8,256,128]{2,1,0:T(8,128)(2,1)S(1)}, bf16[8,256,128]{2,1,0:T(8,128)(2,1)S(1)}, u32[]{:S(2)}, u32[]{:S(2)}) collective-permute-start(bf16[8,256,128]{2,1,0:T(8,128)(2,1)S(1)} %combine.6), channel_id=1, source_target_pairs={{0,16},{16,32},{32,48},{48,0},{1,17},{17,33},{33,49},{49,1},{2,18}... | collective-permute-start | bytes 1572872 | tf_op jit(solution)/shard_map/ppermute | solution.py:332
  113.6 53.0 %copy-start.2 = (f32[128]{0:T(128)S(1)}, f32[128]{0:T(128)}, u32[]{:S(2)}) copy-start(f32[128]{0:T(128)} %param.11) | copy-start | bytes 1540

commit v7 on v6

--- a/solution.py
+++ b/solution.py
@@ -136,11 +136,15 @@
     lax.fori_loop(0, n_ep, block, 0)
 
 
-def score_kernel(count_ref, place_ref, keys_ref, tok0, tok1, tok2, tok3, out_ref):
-    toks = (tok0, tok1, tok2, tok3)
-    n_z, tok, _ = tok0.shape
+def score_kernel(count_ref, place_ref, keys_ref, *refs, members):
+    toks = dict(zip(members, refs))
+    out_ref = refs[-1]
+    n_z, tok, _ = refs[0].shape
     chunks = place_ref.shape[0] // (X * n_z)
-    out_ref[...] = jnp.zeros(out_ref.shape, jnp.float32)
+    if len(refs) > len(members) + 1:
+        out_ref[...] = refs[-2][...]
+    else:
+        out_ref[...] = jnp.zeros(out_ref.shape, jnp.float32)
     token_of = lax.broadcasted_iota(jnp.int32, (tok, LANES), 0)
 
     def line_scores(tokens, line):
@@ -150,17 +154,19 @@
         here = place_ref[pl.ds(line, 1), :] == token_of
         return jnp.sum(jnp.where(here, prod, 0.0), axis=0, keepdims=True)
 
-    def first(z, carry):
-        lines = [(g * n_z + z) * chunks for g in range(X)]
-        found = [line_scores(toks[g][z], lines[g]) for g in range(X)]
-        for line, value in zip(lines, found):
-            out_ref[pl.ds(line, 1), :] = value
-        return carry
-
-    lax.fori_loop(0, n_z, first, 0)
+    per = 4 // len(members) if 4 % len(members) == 0 else 1
+
+    def first(step, carry):
+        jobs = [(g, step * per + j) for j in range(per) for g in members]
+        found = [line_scores(toks[g][z], (g * n_z + z) * chunks) for g, z in jobs]
+        for (g, z), value in zip(jobs, found):
+            out_ref[pl.ds((g * n_z + z) * chunks, 1), :] = value
+        return carry
+
+    lax.fori_loop(0, n_z // per, first, 0)
 
     def more(z, carry):
-        for g in range(X):
+        for g in members:
 
             def chunk(c, inner, g=g):
                 line = (g * n_z + z) * chunks + c
@@ -249,7 +255,9 @@
     lines = n_ep * chunks
 
     near = to_each(tokens, "z")
-    groups = [near] + [lax.ppermute(near, "x", around(shift)) for shift in SHIFTS[1:]]
+    groups = [near]
+    for g in (1, 2, 3):
+        groups.append(lax.ppermute(near, "x", around(SHIFTS[g])))
     listed = pl.pallas_call(
         lambda *refs: bucket_kernel(*refs, n_ep=n_ep, cap=cap, shift=shift),
         out_shape=jax.ShapeDtypeStruct((n_ep, 8, LANES), jnp.float32),
@@ -301,15 +309,21 @@
         held(key_table, pltpu.HBM),
         held(value_table, pltpu.HBM),
     )
-    partial_score = pl.pallas_call(
-        score_kernel,
-        out_shape=jax.ShapeDtypeStruct((lines, LANES), jnp.float32),
-        in_specs=[smem()] + [vmem()] * 6,
-        out_specs=vmem(),
-        interpret=INTERPRET,
-        compiler_params=pltpu.CompilerParams(vmem_limit_bytes=ROOM),
-        name="score",
-    )(count, place, held(keys), *[held(g) for g in groups])
+
+    def scored(members, *before):
+        toks = [held(groups[g]) for g in members]
+        return pl.pallas_call(
+            lambda *refs: score_kernel(*refs, members=members),
+            out_shape=made((lines, LANES), jnp.float32),
+            in_specs=[smem()] + [vmem()] * (2 + len(toks) + len(before)),
+            out_specs=vmem(),
+            interpret=INTERPRET,
+            compiler_params=pltpu.CompilerParams(vmem_limit_bytes=ROOM),
+            name="score",
+        )(count, held(place), held(keys), *toks, *before)
+
+    partial_score = scored((0, 1, 3))
+    partial_score = scored((2,), held(partial_score))
     score = jnp.sum(lax.all_gather(partial_score, TP), axis=0)
     hidden = jnp.where(place >= 0, jax.nn.gelu(score, approximate=False) * gates, 0.0)
 

time: 168 us -> 169 us (level)
    pallas_call x1 -> x2, Pallas kernels: 3.95 us -> 5.4 us  [scored(): pl.pallas_call(lambda *refs: score_kernel(*refs, members=members), out_sh...]
  transfers between devices with their start and end apart: 7 -> 7, of which waited for: 4 -> 3; matrix products, arithmetic and copies ran while one was open for 0% -> 0% of each run, Pallas kernels for 8% -> 11%
where the time goes in v7:
time: 169 us; the launch traced here: 168 us
  blocking collectives  86.2 us (51%)
  waiting for transfers between devices  26.8 us (16%)
  starting transfers between devices  25.6 us (15%)
  Pallas kernels  23.6 us (14%)
  other arithmetic  3.2 us (2%)
  local copies, waits for them, and re-layouts  2.44 us (1%)
    all_to_all x2, blocking collectives, to_each(): lax.all_to_all(jnp.broadcast_to(value[None], (lax.axis_size(axis), *value...  40.4 us
    all_gather x1, blocking collectives, body(): score = jnp.sum(lax.all_gather(partial_score, TP), axis=0)  23.4 us
    all_to_all x1, blocking collectives, body(): back = lax.all_to_all(mine, 'z', 0, 0, tiled=True)  22.4 us
    ppermute x3, waiting for transfers between devices, body(): part = lax.ppermute(part, 'x', around(-SHIFTS[g]))  16.2 us
    ppermute x3, starting transfers between devices, body(): part = lax.ppermute(part, 'x', around(-SHIFTS[g]))  10.9 us
    all_to_all x1, waiting for transfers between devices, body(): listed = lax.all_to_all(listed, EP, 0, 0, tiled=True)  10.6 us
    pallas_call x1, Pallas kernels, body(): pl.pallas_call(pick_kernel, out_shape=(jax.ShapeDtypeStruct((n_ep,), jnp....  10.6 us
    ppermute x3, starting transfers between devices, body(): groups.append(lax.ppermute(near, 'x', around(SHIFTS[g])))  9.93 us
  transfers between devices with their start and end apart: 7, of which 3 were waited for; matrix products, arithmetic and copies ran while one was open for 0% of the time, Pallas kernels for 11%

profile of v7, /device:TPU:1, one launch (start us, length us, event | category | flops | bytes accessed | tf_op | source)
XLA Modules:
  0.0 168.0 jit_solution(15022936025562506962)
XLA Ops:
  0.0 0.9 broadcast_in_dim.8
  0.9 26.9 %all_to_all.20.refs_3_ = bf16[8,256,128]{2,1,0:T(8,128)(2,1)} all-to-all(bf16[8,256,128]{2,1,0:T(8,128)(2,1)S(1)} %broadcast_in_dim.8), channel_id=1, replica_groups=mesh['z'=8,'x'=4,'y'=8,'core'=2] {'z'}, dimensions={0} | all-to-all | bytes 1048576 | tf_op jit(solution)/shard_map/all_to_all | solution.py:238
  27.8 4.6 %collective-permute-start.1 = (bf16[8,256,128]{2,1,0:T(8,128)(2,1)}, bf16[8,256,128]{2,1,0:T(8,128)(2,1)}, u32[]{:S(2)}, u32[]{:S(2)}) collective-permute-start(bf16[8,256,128]{2,1,0:T(8,128)(2,1)} %all_to_all.20.refs_3_), channel_id=1, source_target_pairs={{0,32},{16,48},{32,0},{48,16},{1,33},{17,49},{33,1},{49,17},{2,34}... | collective-permute-start | bytes 1572872 | tf_op jit(solution)/shard_map/ppermute | solution.py:260
  32.4 2.8 %collective-permute-start.2 = (bf16[8,256,128]{2,1,0:T(8,128)(2,1)}, bf16[8,256,128]{2,1,0:T(8,128)(2,1)}, u32[]{:S(2)}, u32[]{:S(2)}) collective-permute-start(bf16[8,256,128]{2,1,0:T(8,128)(2,1)} %all_to_all.20.refs_3_), channel_id=1, source_target_pairs={{0,48},{16,0},{32,16},{48,32},{1,49},{17,1},{33,17},{49,33},{2,50}... | collective-permute-start | bytes 1572872 | tf_op jit(solution)/shard_map/ppermute | solution.py:260
  35.2 2.5 %collective-permute-start = (bf16[8,256,128]{2,1,0:T(8,128)(2,1)}, bf16[8,256,128]{2,1,0:T(8,128)(2,1)}, u32[]{:S(2)}, u32[]{:S(2)}) collective-permute-start(bf16[8,256,128]{2,1,0:T(8,128)(2,1)} %all_to_all.20.refs_3_), channel_id=1, source_target_pairs={{0,16},{16,32},{32,48},{48,0},{1,17},{17,33},{33,49},{49,1},{2,18}... | collective-permute-start | bytes 1572872 | tf_op jit(solution)/shard_map/ppermute | solution.py:260
  37.7 0.0 copy-start
  37.7 0.7 copy-done
  38.5 0.0 copy-start.1
  38.5 0.7 copy-done.1
  39.2 2.3 %bucket.1 = f32[32,8,128]{2,1,0:T(8,128)} custom-call(s32[16,256]{1,0:T(8,128)S(1)} %bitcast.7, f32[16,256]{1,0:T(8,128)S(1)} %bitcast.8), custom_call_target="tpu_custom_call" | custom-call | tf_op jit(solution)/shard_map/bucket/pallas_call | solution.py:261
  41.4 4.8 %all-to-all-start = ((f32[32,8,128]{2,1,0:T(8,128)}), f32[32,8,128]{2,1,0:T(8,128)S(1)}, u32[]{:S(2)}, u32[]{:S(2)}) async-start(f32[32,8,128]{2,1,0:T(8,128)} %bucket.1), calls=%async_computation | async-start | bytes 262144 | tf_op jit(solution)/shard_map/all_to_all | solution.py:274
  46.2 10.6 %all-to-all-done = f32[32,8,128]{2,1,0:T(8,128)S(1)} async-done(((f32[32,8,128]{2,1,0:T(8,128)}), f32[32,8,128]{2,1,0:T(8,128)S(1)}, u32[]{:S(2)}, u32[]{:S(2)}) %all-to-all-start) | async-done | bytes 131104 | tf_op jit(solution)/shard_map/all_to_all | solution.py:274
  56.8 0.7 shift-right-arithmetic_add_fusion
  57.6 10.6 %pick.1 = (s32[32]{0:T(128)S(1)}, s32[96,128]{1,0:T(8,128)S(1)}, f32[96,128]{1,0:T(8,128)S(1)}, bf16[96,128,128]{2,1,0:T(8,128)(2,1)S(1)}, bf16[96,128,128]{2,1,0:T(8,128)(2,1)S(1)}) custom-call(s32[1]{0:T(128)} %bitcast.x_ref, s32[96,128]{1,0:T(8,128)S(1)} %reshape.29.rows_ref, s32[32]{0:T(128)S(1)} %get-tuple-element.16.count_ref, ...), custom_call_target="tpu_custom_call" | custom-call | tf_op jit(solution)/shard_map/pick/pallas_call | solution.py:283
  68.1 0.0 collective-permute-done.1.refs_4_
  68.1 0.0 collective-permute-done.2.refs_5_
  68.2 3.7 %score.2.refs_4_ = f32[96,128]{1,0:T(8,128)S(1)} custom-call(s32[32]{0:T(128)S(1)} %get-tuple-element.10.refs_0_, s32[96,128]{1,0:T(8,128)S(1)} %get-tuple-element.11.refs_1_, bf16[96,128,128]{2,1,0:T(8,128)(2,1)S(1)} %get-tuple-element.12.refs_2_, bf16[8,256,128]{2,1,0:T(8,128)(2,1)} %all_to_all.20.refs_3_, ...), custom_call_target="tpu_custom_call" | custom-call | tf_op jit(solution)/shard_map/score/pallas_call | solution.py:315
  71.9 0.0 collective-permute-done.refs_3_
  71.9 1.7 %score.3 = f32[96,128]{1,0:T(8,128)S(1)} custom-call(s32[32]{0:T(128)S(1)} %get-tuple-element.10.refs_0_, s32[96,128]{1,0:T(8,128)S(1)} %get-tuple-element.11.refs_1_, bf16[96,128,128]{2,1,0:T(8,128)(2,1)S(1)} %get-tuple-element.12.refs_2_, bf16[8,256,128]{2,1,0:T(8,128)(2,1)} %collective-permute-done.refs_3_, f32[96,128]{1,0:T(8,128)S(1)} %score.2.refs_4_), custom_call_target="tpu_custom_call" | custom-call | tf_op jit(solution)/shard_map/score/pallas_call | solution.py:315
  73.6 23.4 %all-gather = f32[1536,128]{1,0:T(8,128)} all-gather(f32[96,128]{1,0:T(8,128)S(1)} %score.3), channel_id=2, replica_groups=mesh['z'=8,'x'=4,'y'=8,'core'=2] {'y','core'}, dimensions={0}, use_global_device_ids=true | all-gather | bytes 835584 | tf_op jit(solution)/shard_map/all_gather | solution.py:327
  97.0 1.2 reduce_sum.46
  98.1 0.1 fusion.4.refs_2_
  98.3 1.3 combine.4
  99.6 1.3 combine.5
  100.9 1.3 combine.6
  102.3 3.9 %collective-permute-start.3 = (bf16[8,256,128]{2,1,0:T(8,128)(2,1)S(1)}, bf16[8,256,128]{2,1,0:T(8,128)(2,1)S(1)}, u32[]{:S(2)}, u32[]{:S(2)}) collective-permute-start(bf16[8,256,128]{2,1,0:T(8,128)(2,1)S(1)} %combine.4), channel_id=1, source_target_pairs={{0,32},{16,48},{32,0},{48,16},{1,33},{17,49},{33,1},{49,17},{2,34}... | collective-permute-start | bytes 1572872 | tf_op jit(solution)/shard_map/ppermute | solution.py:346
  106.2 5.1 %collective-permute-start.4 = (bf16[8,256,128]{2,1,0:T(8,128)(2,1)S(1)}, bf16[8,256,128]{2,1,0:T(8,128)(2,1)S(1)}, u32[]{:S(2)}, u32[]{:S(2)}) collective-permute-start(bf16[8,256,128]{2,1,0:T(8,128)(2,1)S(1)} %combine.5), channel_id=1, source_target_pairs={{0,48},{16,0},{32,16},{48,32},{1,49},{17,1},{33,17},{49,33},{2,50}... | collective-permute-start | bytes 1572872 | tf_op jit(solution)/shard_map/ppermute | solution.py:346
  111.3 1.9 %collective-permute-start.5 = (bf16[8,256,128]{2,1,0:T(8,128)(2,1)S(1)}, bf16[8,256,128]{2,1,0:T(8,128)(2,1)S(1)}, u32[]{:S(2)}, u32[]{:S(2)}) collective-permute-start(bf16[8,256,128]{2,1,0:T(8,128)(2,1)S(1)} %combine.6), channel_id=1, source_target_pairs={{0,16},{16,32},{32,48},{48,0},{1,17},{17,33},{33,49},{49,1},{2,18}... | collective-permute-start | bytes 1572872 | tf_op jit(solution)/shard_map/ppermute | solution.py:346
  113.2 1.3 combine.7
  114.6 0.0 copy-start.2
  114.6 4.5 %collective-permute-done.3 = bf16[8,256,128]{2,1,0:T(8,128)(2,1)S(1)} collective-permute-done((bf16[8,256,128]{2,1,0:T(8,128)(2,1)S(1)}, bf16[8,256,128]{2,1,0:T(8,128)(2,1)S(1)}, u32[]{:S(2)}, u32[]{:S(2)}) %collective-permute-start.3) | collective-permute-done | bytes 524320 | tf_op jit(solution)/shard_map/ppermute | solution.py:346
  119.1 11.7 %collective-permute-done.4 = bf16[8,256,128]{2,1,0:T(8,128)(2,1)S(1)} collective-permute-done((bf16[8,256,128]{2,1,0:T(8,128)(2,1)S(1)}, bf16[8,256,128]{2,1,0:T(8,128)(2,1)S(1)}, u32[]{:S(2)}, u32[]{:S(2)}) %collective-permute-start.4) | collective-permute-done | bytes 524320 | tf_op jit(solution)/shard_map/ppermute | solution.py:346
  130.7 0.0 collective-permute-done.5
  130.8 0.3 add_convert_fusion
  131.1 22.4 %all_to_all.21 = bf16[8,256,128]{2,1,0:T(8,128)(2,1)S(1)} all-to-all(bf16[8,256,128]{2,1,0:T(8,128)(2,1)S(1)} %add_convert_fusion), channel_id=1, replica_groups=mesh['z'=8,'x'=4,'y'=8,'core'=2] {'z'}, dimensions={0} | all-to-all | bytes 1048576 | tf_op jit(solution)/shard_map/all_to_all | solution.py:349
  153.5 0.1 convert_reduce_fusion
  153.6 0.1 multiply_reduce_fusion
  153.7 13.5 %all_to_all.22 = f32[16,2,128]{2,1,0:T(2,128)S(1)} all-to-all(f32[16,2,128]{2,1,0:T(2,128)S(1)} %broadcast_in_dim.10), channel_id=1, replica_groups=mesh['z'=8,'x'=4,'y'=8,'core'=2] {'y','core'}, dimensions={0} | all-to-all | bytes 32768 | tf_op jit(solution)/shard_map/all_to_all | solution.py:238
  167.2 0.0 copy-done.2
  167.2 0.7 multiply_convert_fusion
  (7 shorter events, 0.1 us)
Async XLA Ops:
  27.8 40.3 %collective-permute-start.1 = (bf16[8,256,128]{2,1,0:T(8,128)(2,1)}, bf16[8,256,128]{2,1,0:T(8,128)(2,1)}, u32[]{:S(2)}, u32[]{:S(2)}) collective-permute-start(bf16[8,256,128]{2,1,0:T(8,128)(2,1)} %all_to_all.20.refs_3_), channel_id=1, source_target_pairs={{0,32},{16,48},{32,0},{48,16},{1,33},{17,49},{33,1},{49,17},{2,34}... | collective-permute-start | bytes 1572872 | tf_op jit(solution)/shard_map/ppermute | solution.py:260
  32.4 35.7 %collective-permute-start.2 = (bf16[8,256,128]{2,1,0:T(8,128)(2,1)}, bf16[8,256,128]{2,1,0:T(8,128)(2,1)}, u32[]{:S(2)}, u32[]{:S(2)}) collective-permute-start(bf16[8,256,128]{2,1,0:T(8,128)(2,1)} %all_to_all.20.refs_3_), channel_id=1, source_target_pairs={{0,48},{16,0},{32,16},{48,32},{1,49},{17,1},{33,17},{49,33},{2,50}... | collective-permute-start | bytes 1572872 | tf_op jit(solution)/shard_map/ppermute | solution.py:260
  35.2 36.6 %collective-permute-start = (bf16[8,256,128]{2,1,0:T(8,128)(2,1)}, bf16[8,256,128]{2,1,0:T(8,128)(2,1)}, u32[]{:S(2)}, u32[]{:S(2)}) collective-permute-start(bf16[8,256,128]{2,1,0:T(8,128)(2,1)} %all_to_all.20.refs_3_), channel_id=1, source_target_pairs={{0,16},{16,32},{32,48},{48,0},{1,17},{17,33},{33,49},{49,1},{2,18}... | collective-permute-start | bytes 1572872 | tf_op jit(solution)/shard_map/ppermute | solution.py:260
  37.7 0.7 copy-start
  38.5 0.7 copy-start.1
  41.4 15.3 %all-to-all-start = ((f32[32,8,128]{2,1,0:T(8,128)}), f32[32,8,128]{2,1,0:T(8,128)S(1)}, u32[]{:S(2)}, u32[]{:S(2)}) async-start(f32[32,8,128]{2,1,0:T(8,128)} %bucket.1), calls=%async_computation | async-start | bytes 262144 | tf_op jit(solution)/shard_map/all_to_all | solution.py:274
  102.3 16.8 %collective-permute-start.3 = (bf16[8,256,128]{2,1,0:T(8,128)(2,1)S(1)}, bf16[8,256,128]{2,1,0:T(8,128)(2,1)S(1)}, u32[]{:S(2)}, u32[]{:S(2)}) collective-permute-start(bf16[8,256,128]{2,1,0:T(8,128)(2,1)S(1)} %combine.4), channel_id=1, source_target_pairs={{0,32},{16,48},{32,0},{48,16},{1,33},{17,49},{33,1},{49,17},{2,34}... | collective-permute-start | bytes 1572872 | tf_op jit(solution)/shard_map/ppermute | solution.py:346
  106.2 24.5 %collective-permute-start.4 = (bf16[8,256,128]{2,1,0:T(8,128)(2,1)S(1)}, bf16[8,256,128]{2,1,0:T(8,128)(2,1)S(1)}, u32[]{:S(2)}, u32[]{:S(2)}) collective-permute-start(bf16[8,256,128]{2,1,0:T(8,128)(2,1)S(1)} %combine.5), channel_id=1, source_target_pairs={{0,48},{16,0},{32,16},{48,32},{1,49},{17,1},{33,17},{49,33},{2,50}... | collective-permute-start | bytes 1572872 | tf_op jit(solution)/shard_map/ppermute | solution.py:346
  111.3 19.4 %collective-permute-start.5 = (bf16[8,256,128]{2,1,0:T(8,128)(2,1)S(1)}, bf16[8,256,128]{2,1,0:T(8,128)(2,1)S(1)}, u32[]{:S(2)}, u32[]{:S(2)}) collective-permute-start(bf16[8,256,128]{2,1,0:T(8,128)(2,1)S(1)} %combine.6), channel_id=1, source_target_pairs={{0,16},{16,32},{32,48},{48,0},{1,17},{17,33},{33,49},{49,1},{2,18}... | collective-permute-start | bytes 1572872 | tf_op jit(solution)/shard_map/ppermute | solution.py:346
  114.6 52.6 %copy-start.2 = (f32[128]{0:T(128)S(1)}, f32[128]{0:T(128)}, u32[]{:S(2)}) copy-start(f32[128]{0:T(128)} %param.11) | copy-start | bytes 1540

commit v8 on v7

--- a/solution.py
+++ b/solution.py
@@ -71,21 +71,24 @@
         out_ref[:, chunks + j, :] = gates[:, j * LANES : (j + 1) * LANES]
 
 
-def widen(table_ref, wide_ref):
+def widen(table_ref, wide_ref, which):
     step = 256
 
     def one(i, carry):
         rows = pl.ds(pl.multiple_of(i * step, step), step)
-        wide_ref[rows, :] = table_ref[rows, :].astype(jnp.float32)
+        into = pl.ds(pl.multiple_of(i * 2 * step, 2 * step) + which, step, stride=2)
+        wide_ref[into, :] = table_ref[rows, :].astype(jnp.float32)
         return carry
 
     lax.fori_loop(0, table_ref.shape[0] // step, one, 0)
 
 
-def take_rows(rows_ref, line, wide_ref, picked, out_ref, to):
+def take_rows(rows_ref, line, wide_ref, picked, keys_out, values_out, to):
     for s in range(LANES):
-        picked[pl.ds(s, 1), :] = wide_ref[pl.ds(rows_ref[line, s], 1), :]
-    out_ref[to] = picked[...].astype(out_ref.dtype)
+        at = pl.multiple_of(rows_ref[line, s] * 2, 2)
+        picked[pl.ds(2 * s, 2), :] = wide_ref[pl.ds(at, 2), :]
+    keys_out[to] = picked[pl.ds(0, LANES, stride=2), :].astype(keys_out.dtype)
+    values_out[to] = picked[pl.ds(1, LANES, stride=2), :].astype(values_out.dtype)
 
 
 def chunks_of(count):
@@ -105,16 +108,14 @@
     gate_out,
     keys_out,
     values_out,
-    wide_k,
-    wide_v,
-    took_k,
-    took_v,
+    wide,
+    took,
 ):
     n_ep = count_ref.shape[0]
     n_z = n_ep // X
     chunks = place_ref.shape[0] // n_ep
-    widen(key_ref, wide_k)
-    widen(value_ref, wide_v)
+    widen(key_ref, wide, 0)
+    widen(value_ref, wide, 1)
 
     def block(i, carry):
         z = i // X
@@ -126,8 +127,9 @@
             gate_out[pl.ds(slot * chunks + c, 1), :] = gate_ref[pl.ds(i * chunks + c, 1), :]
 
         def chunk(c, inner):
-            take_rows(rows_ref, i * chunks + c, wide_k, took_k, keys_out, slot * chunks + c)
-            take_rows(rows_ref, i * chunks + c, wide_v, took_v, values_out, slot * chunks + c)
+            take_rows(
+                rows_ref, i * chunks + c, wide, took, keys_out, values_out, slot * chunks + c
+            )
             return inner
 
         lax.fori_loop(0, chunks_of(count_ref[i]), chunk, 0)
@@ -292,10 +294,8 @@
         in_specs=[smem(), smem(), smem(), vmem(), vmem(), vmem(), vmem()],
         out_specs=(smem(), vmem(), vmem(), vmem(), vmem()),
         scratch_shapes=[
-            pltpu.VMEM((exp_dev, width), jnp.float32),
-            pltpu.VMEM((exp_dev, width), jnp.float32),
-            pltpu.VMEM((LANES, width), jnp.float32),
-            pltpu.VMEM((LANES, width), jnp.float32),
+            pltpu.VMEM((2 * exp_dev, width), jnp.float32),
+            pltpu.VMEM((2 * LANES, width), jnp.float32),
         ],
         interpret=INTERPRET,
         compiler_params=pltpu.CompilerParams(vmem_limit_bytes=ROOM),

time: 169 us -> 166 us (0.982)
  Pallas kernels: 23.6 us -> 21.2 us
    pallas_call x1, Pallas kernels: 10.6 us -> 8.17 us  [body(): pl.pallas_call(pick_kernel, out_shape=(jax.ShapeDtypeStruct((n_ep,), jnp....]
  transfers between devices with their start and end apart: 7 -> 7, of which waited for: 3 -> 4; matrix products, arithmetic and copies ran while one was open for 0% -> 0% of each run, Pallas kernels for 11% -> 9%
where the time goes in v8:
time: 166 us; the launch traced here: 165 us
  blocking collectives  85.6 us (52%)
  waiting for transfers between devices  27.1 us (16%)
  starting transfers between devices  25.3 us (15%)
  Pallas kernels  21.2 us (13%)
  other arithmetic  3.2 us (2%)
  local copies, waits for them, and re-layouts  2.44 us (1%)
    all_to_all x2, blocking collectives, to_each(): lax.all_to_all(jnp.broadcast_to(value[None], (lax.axis_size(axis), *value...  40.4 us
    all_gather x1, blocking collectives, body(): score = jnp.sum(lax.all_gather(partial_score, TP), axis=0)  23.4 us
    all_to_all x1, blocking collectives, body(): back = lax.all_to_all(mine, 'z', 0, 0, tiled=True)  21.8 us
    ppermute x3, waiting for transfers between devices, body(): part = lax.ppermute(part, 'x', around(-SHIFTS[g]))  16.5 us
    ppermute x3, starting transfers between devices, body(): part = lax.ppermute(part, 'x', around(-SHIFTS[g]))  10.6 us
    all_to_all x1, waiting for transfers between devices, body(): listed = lax.all_to_all(listed, EP, 0, 0, tiled=True)  10.6 us
    ppermute x3, starting transfers between devices, body(): groups.append(lax.ppermute(near, 'x', around(SHIFTS[g])))  9.93 us
    pallas_call x1, Pallas kernels, body(): pl.pallas_call(pick_kernel, out_shape=(jax.ShapeDtypeStruct((n_ep,), jnp....  8.17 us
  transfers between devices with their start and end apart: 7, of which 4 were waited for; matrix products, arithmetic and copies ran while one was open for 0% of the time, Pallas kernels for 9%

profile of v8, /device:TPU:1, one launch (start us, length us, event | category | flops | bytes accessed | tf_op | source)
XLA Modules:
  0.0 164.9 jit_solution(628770267172783418)
XLA Ops:
  0.0 0.9 broadcast_in_dim.8
  0.9 26.9 %all_to_all.20.refs_3_ = bf16[8,256,128]{2,1,0:T(8,128)(2,1)} all-to-all(bf16[8,256,128]{2,1,0:T(8,128)(2,1)S(1)} %broadcast_in_dim.8), channel_id=1, replica_groups=mesh['z'=8,'x'=4,'y'=8,'core'=2] {'z'}, dimensions={0} | all-to-all | bytes 1048576 | tf_op jit(solution)/shard_map/all_to_all | solution.py:240
  27.8 4.6 %collective-permute-start.1 = (bf16[8,256,128]{2,1,0:T(8,128)(2,1)}, bf16[8,256,128]{2,1,0:T(8,128)(2,1)}, u32[]{:S(2)}, u32[]{:S(2)}) collective-permute-start(bf16[8,256,128]{2,1,0:T(8,128)(2,1)} %all_to_all.20.refs_3_), channel_id=1, source_target_pairs={{0,32},{16,48},{32,0},{48,16},{1,33},{17,49},{33,1},{49,17},{2,34}... | collective-permute-start | bytes 1572872 | tf_op jit(solution)/shard_map/ppermute | solution.py:262
  32.4 2.8 %collective-permute-start.2 = (bf16[8,256,128]{2,1,0:T(8,128)(2,1)}, bf16[8,256,128]{2,1,0:T(8,128)(2,1)}, u32[]{:S(2)}, u32[]{:S(2)}) collective-permute-start(bf16[8,256,128]{2,1,0:T(8,128)(2,1)} %all_to_all.20.refs_3_), channel_id=1, source_target_pairs={{0,48},{16,0},{32,16},{48,32},{1,49},{17,1},{33,17},{49,33},{2,50}... | collective-permute-start | bytes 1572872 | tf_op jit(solution)/shard_map/ppermute | solution.py:262
  35.2 2.5 %collective-permute-start = (bf16[8,256,128]{2,1,0:T(8,128)(2,1)}, bf16[8,256,128]{2,1,0:T(8,128)(2,1)}, u32[]{:S(2)}, u32[]{:S(2)}) collective-permute-start(bf16[8,256,128]{2,1,0:T(8,128)(2,1)} %all_to_all.20.refs_3_), channel_id=1, source_target_pairs={{0,16},{16,32},{32,48},{48,0},{1,17},{17,33},{33,49},{49,1},{2,18}... | collective-permute-start | bytes 1572872 | tf_op jit(solution)/shard_map/ppermute | solution.py:262
  37.7 0.0 copy-start
  37.7 0.7 copy-done
  38.5 0.0 copy-start.1
  38.5 0.7 copy-done.1
  39.2 2.3 %bucket.1 = f32[32,8,128]{2,1,0:T(8,128)} custom-call(s32[16,256]{1,0:T(8,128)S(1)} %bitcast.7, f32[16,256]{1,0:T(8,128)S(1)} %bitcast.8), custom_call_target="tpu_custom_call" | custom-call | tf_op jit(solution)/shard_map/bucket/pallas_call | solution.py:263
  41.4 4.8 %all-to-all-start = ((f32[32,8,128]{2,1,0:T(8,128)}), f32[32,8,128]{2,1,0:T(8,128)S(1)}, u32[]{:S(2)}, u32[]{:S(2)}) async-start(f32[32,8,128]{2,1,0:T(8,128)} %bucket.1), calls=%async_computation | async-start | bytes 262144 | tf_op jit(solution)/shard_map/all_to_all | solution.py:276
  46.2 10.6 %all-to-all-done = f32[32,8,128]{2,1,0:T(8,128)S(1)} async-done(((f32[32,8,128]{2,1,0:T(8,128)}), f32[32,8,128]{2,1,0:T(8,128)S(1)}, u32[]{:S(2)}, u32[]{:S(2)}) %all-to-all-start) | async-done | bytes 131104 | tf_op jit(solution)/shard_map/all_to_all | solution.py:276
  56.8 0.7 shift-right-arithmetic_add_fusion
  57.6 8.2 %pick.1 = (s32[32]{0:T(128)S(1)}, s32[96,128]{1,0:T(8,128)S(1)}, f32[96,128]{1,0:T(8,128)S(1)}, bf16[96,128,128]{2,1,0:T(8,128)(2,1)S(1)}, bf16[96,128,128]{2,1,0:T(8,128)(2,1)S(1)}) custom-call(s32[1]{0:T(128)} %bitcast.x_ref, s32[96,128]{1,0:T(8,128)S(1)} %reshape.29.rows_ref, s32[32]{0:T(128)S(1)} %get-tuple-element.16.count_ref, ...), custom_call_target="tpu_custom_call" | custom-call | tf_op jit(solution)/shard_map/pick/pallas_call | solution.py:285
  65.7 0.0 collective-permute-done.1.refs_4_
  65.7 0.0 collective-permute-done.2.refs_5_
  65.8 3.7 %score.2.refs_4_ = f32[96,128]{1,0:T(8,128)S(1)} custom-call(s32[32]{0:T(128)S(1)} %get-tuple-element.10.refs_0_, s32[96,128]{1,0:T(8,128)S(1)} %get-tuple-element.11.refs_1_, bf16[96,128,128]{2,1,0:T(8,128)(2,1)S(1)} %get-tuple-element.12.refs_2_, bf16[8,256,128]{2,1,0:T(8,128)(2,1)} %all_to_all.20.refs_3_, ...), custom_call_target="tpu_custom_call" | custom-call | tf_op jit(solution)/shard_map/score/pallas_call | solution.py:315
  69.5 0.0 collective-permute-done.refs_3_
  69.5 1.7 %score.3 = f32[96,128]{1,0:T(8,128)S(1)} custom-call(s32[32]{0:T(128)S(1)} %get-tuple-element.10.refs_0_, s32[96,128]{1,0:T(8,128)S(1)} %get-tuple-element.11.refs_1_, bf16[96,128,128]{2,1,0:T(8,128)(2,1)S(1)} %get-tuple-element.12.refs_2_, bf16[8,256,128]{2,1,0:T(8,128)(2,1)} %collective-permute-done.refs_3_, f32[96,128]{1,0:T(8,128)S(1)} %score.2.refs_4_), custom_call_target="tpu_custom_call" | custom-call | tf_op jit(solution)/shard_map/score/pallas_call | solution.py:315
  71.2 23.4 %all-gather = f32[1536,128]{1,0:T(8,128)} all-gather(f32[96,128]{1,0:T(8,128)S(1)} %score.3), channel_id=2, replica_groups=mesh['z'=8,'x'=4,'y'=8,'core'=2] {'y','core'}, dimensions={0}, use_global_device_ids=true | all-gather | bytes 835584 | tf_op jit(solution)/shard_map/all_gather | solution.py:327
  94.5 1.2 reduce_sum.46
  95.7 0.1 fusion.4.refs_2_
  95.9 1.3 combine.4
  97.2 1.3 combine.5
  98.5 1.3 combine.6
  99.9 3.9 %collective-permute-start.3 = (bf16[8,256,128]{2,1,0:T(8,128)(2,1)S(1)}, bf16[8,256,128]{2,1,0:T(8,128)(2,1)S(1)}, u32[]{:S(2)}, u32[]{:S(2)}) collective-permute-start(bf16[8,256,128]{2,1,0:T(8,128)(2,1)S(1)} %combine.4), channel_id=1, source_target_pairs={{0,32},{16,48},{32,0},{48,16},{1,33},{17,49},{33,1},{49,17},{2,34}... | collective-permute-start | bytes 1572872 | tf_op jit(solution)/shard_map/ppermute | solution.py:346
  103.8 4.8 %collective-permute-start.4 = (bf16[8,256,128]{2,1,0:T(8,128)(2,1)S(1)}, bf16[8,256,128]{2,1,0:T(8,128)(2,1)S(1)}, u32[]{:S(2)}, u32[]{:S(2)}) collective-permute-start(bf16[8,256,128]{2,1,0:T(8,128)(2,1)S(1)} %combine.5), channel_id=1, source_target_pairs={{0,48},{16,0},{32,16},{48,32},{1,49},{17,1},{33,17},{49,33},{2,50}... | collective-permute-start | bytes 1572872 | tf_op jit(solution)/shard_map/ppermute | solution.py:346
  108.6 1.9 %collective-permute-start.5 = (bf16[8,256,128]{2,1,0:T(8,128)(2,1)S(1)}, bf16[8,256,128]{2,1,0:T(8,128)(2,1)S(1)}, u32[]{:S(2)}, u32[]{:S(2)}) collective-permute-start(bf16[8,256,128]{2,1,0:T(8,128)(2,1)S(1)} %combine.6), channel_id=1, source_target_pairs={{0,16},{16,32},{32,48},{48,0},{1,17},{17,33},{33,49},{49,1},{2,18}... | collective-permute-start | bytes 1572872 | tf_op jit(solution)/shard_map/ppermute | solution.py:346
  110.5 1.3 combine.7
  111.9 0.0 copy-start.2
  111.9 4.8 %collective-permute-done.3 = bf16[8,256,128]{2,1,0:T(8,128)(2,1)S(1)} collective-permute-done((bf16[8,256,128]{2,1,0:T(8,128)(2,1)S(1)}, bf16[8,256,128]{2,1,0:T(8,128)(2,1)S(1)}, u32[]{:S(2)}, u32[]{:S(2)}) %collective-permute-start.3) | collective-permute-done | bytes 524320 | tf_op jit(solution)/shard_map/ppermute | solution.py:346
  116.6 11.5 %collective-permute-done.4 = bf16[8,256,128]{2,1,0:T(8,128)(2,1)S(1)} collective-permute-done((bf16[8,256,128]{2,1,0:T(8,128)(2,1)S(1)}, bf16[8,256,128]{2,1,0:T(8,128)(2,1)S(1)}, u32[]{:S(2)}, u32[]{:S(2)}) %collective-permute-start.4) | collective-permute-done | bytes 524320 | tf_op jit(solution)/shard_map/ppermute | solution.py:346
  128.2 0.2 collective-permute-done.5
  128.4 0.3 add_convert_fusion
  128.6 21.8 %all_to_all.21 = bf16[8,256,128]{2,1,0:T(8,128)(2,1)S(1)} all-to-all(bf16[8,256,128]{2,1,0:T(8,128)(2,1)S(1)} %add_convert_fusion), channel_id=1, replica_groups=mesh['z'=8,'x'=4,'y'=8,'core'=2] {'z'}, dimensions={0} | all-to-all | bytes 1048576 | tf_op jit(solution)/shard_map/all_to_all | solution.py:349
  150.5 0.1 convert_reduce_fusion
  150.5 0.1 multiply_reduce_fusion
  150.7 13.5 %all_to_all.22 = f32[16,2,128]{2,1,0:T(2,128)S(1)} all-to-all(f32[16,2,128]{2,1,0:T(2,128)S(1)} %broadcast_in_dim.10), channel_id=1, replica_groups=mesh['z'=8,'x'=4,'y'=8,'core'=2] {'y','core'}, dimensions={0} | all-to-all | bytes 32768 | tf_op jit(solution)/shard_map/all_to_all | solution.py:240
  164.2 0.0 copy-done.2
  164.2 0.7 multiply_convert_fusion
  (7 shorter events, 0.1 us)
Async XLA Ops:
  27.8 38.0 %collective-permute-start.1 = (bf16[8,256,128]{2,1,0:T(8,128)(2,1)}, bf16[8,256,128]{2,1,0:T(8,128)(2,1)}, u32[]{:S(2)}, u32[]{:S(2)}) collective-permute-start(bf16[8,256,128]{2,1,0:T(8,128)(2,1)} %all_to_all.20.refs_3_), channel_id=1, source_target_pairs={{0,32},{16,48},{32,0},{48,16},{1,33},{17,49},{33,1},{49,17},{2,34}... | collective-permute-start | bytes 1572872 | tf_op jit(solution)/shard_map/ppermute | solution.py:262
  32.4 33.3 %collective-permute-start.2 = (bf16[8,256,128]{2,1,0:T(8,128)(2,1)}, bf16[8,256,128]{2,1,0:T(8,128)(2,1)}, u32[]{:S(2)}, u32[]{:S(2)}) collective-permute-start(bf16[8,256,128]{2,1,0:T(8,128)(2,1)} %all_to_all.20.refs_3_), channel_id=1, source_target_pairs={{0,48},{16,0},{32,16},{48,32},{1,49},{17,1},{33,17},{49,33},{2,50}... | collective-permute-start | bytes 1572872 | tf_op jit(solution)/shard_map/ppermute | solution.py:262
  35.2 34.3 %collective-permute-start = (bf16[8,256,128]{2,1,0:T(8,128)(2,1)}, bf16[8,256,128]{2,1,0:T(8,128)(2,1)}, u32[]{:S(2)}, u32[]{:S(2)}) collective-permute-start(bf16[8,256,128]{2,1,0:T(8,128)(2,1)} %all_to_all.20.refs_3_), channel_id=1, source_target_pairs={{0,16},{16,32},{32,48},{48,0},{1,17},{17,33},{33,49},{49,1},{2,18}... | collective-permute-start | bytes 1572872 | tf_op jit(solution)/shard_map/ppermute | solution.py:262
  37.7 0.7 copy-start
  38.5 0.7 copy-start.1
  41.4 15.3 %all-to-all-start = ((f32[32,8,128]{2,1,0:T(8,128)}), f32[32,8,128]{2,1,0:T(8,128)S(1)}, u32[]{:S(2)}, u32[]{:S(2)}) async-start(f32[32,8,128]{2,1,0:T(8,128)} %bucket.1), calls=%async_computation | async-start | bytes 262144 | tf_op jit(solution)/shard_map/all_to_all | solution.py:276
  99.9 16.8 %collective-permute-start.3 = (bf16[8,256,128]{2,1,0:T(8,128)(2,1)S(1)}, bf16[8,256,128]{2,1,0:T(8,128)(2,1)S(1)}, u32[]{:S(2)}, u32[]{:S(2)}) collective-permute-start(bf16[8,256,128]{2,1,0:T(8,128)(2,1)S(1)} %combine.4), channel_id=1, source_target_pairs={{0,32},{16,48},{32,0},{48,16},{1,33},{17,49},{33,1},{49,17},{2,34}... | collective-permute-start | bytes 1572872 | tf_op jit(solution)/shard_map/ppermute | solution.py:346
  103.8 24.4 %collective-permute-start.4 = (bf16[8,256,128]{2,1,0:T(8,128)(2,1)S(1)}, bf16[8,256,128]{2,1,0:T(8,128)(2,1)S(1)}, u32[]{:S(2)}, u32[]{:S(2)}) collective-permute-start(bf16[8,256,128]{2,1,0:T(8,128)(2,1)S(1)} %combine.5), channel_id=1, source_target_pairs={{0,48},{16,0},{32,16},{48,32},{1,49},{17,1},{33,17},{49,33},{2,50}... | collective-permute-start | bytes 1572872 | tf_op jit(solution)/shard_map/ppermute | solution.py:346
  108.6 19.7 %collective-permute-start.5 = (bf16[8,256,128]{2,1,0:T(8,128)(2,1)S(1)}, bf16[8,256,128]{2,1,0:T(8,128)(2,1)S(1)}, u32[]{:S(2)}, u32[]{:S(2)}) collective-permute-start(bf16[8,256,128]{2,1,0:T(8,128)(2,1)S(1)} %combine.6), channel_id=1, source_target_pairs={{0,16},{16,32},{32,48},{48,0},{1,17},{17,33},{33,49},{49,1},{2,18}... | collective-permute-start | bytes 1572872 | tf_op jit(solution)/shard_map/ppermute | solution.py:346
  111.9 52.3 %copy-start.2 = (f32[128]{0:T(128)S(1)}, f32[128]{0:T(128)}, u32[]{:S(2)}) copy-start(f32[128]{0:T(128)} %param.11) | copy-start | bytes 1540

commit v9 on v8

--- a/solution.py
+++ b/solution.py
@@ -85,10 +85,15 @@
 
 def take_rows(rows_ref, line, wide_ref, picked, keys_out, values_out, to):
     for s in range(LANES):
-        at = pl.multiple_of(rows_ref[line, s] * 2, 2)
+        at = pl.multiple_of(rows_ref[line, s], 2)
         picked[pl.ds(2 * s, 2), :] = wide_ref[pl.ds(at, 2), :]
     keys_out[to] = picked[pl.ds(0, LANES, stride=2), :].astype(keys_out.dtype)
     values_out[to] = picked[pl.ds(1, LANES, stride=2), :].astype(values_out.dtype)
+
+
+def repeat_kernel(tok_ref, out_ref):
+    for i in range(out_ref.shape[0]):
+        out_ref[i] = tok_ref[...]
 
 
 def chunks_of(count):
@@ -156,7 +161,7 @@
         here = place_ref[pl.ds(line, 1), :] == token_of
         return jnp.sum(jnp.where(here, prod, 0.0), axis=0, keepdims=True)
 
-    per = 4 // len(members) if 4 % len(members) == 0 else 1
+    per = 4 if len(members) == 1 else 2
 
     def first(step, carry):
         jobs = [(g, step * per + j) for j in range(per) for g in members]
@@ -256,7 +261,16 @@
     shift = exp_dev.bit_length() - 1
     lines = n_ep * chunks
 
-    near = to_each(tokens, "z")
+    copies = pl.pallas_call(
+        repeat_kernel,
+        out_shape=made((lax.axis_size("z"), tok, width), tokens.dtype),
+        in_specs=[vmem()],
+        out_specs=vmem(),
+        interpret=INTERPRET,
+        compiler_params=pltpu.CompilerParams(vmem_limit_bytes=ROOM),
+        name="repeat",
+    )(held(tokens, pltpu.HBM))
+    near = lax.all_to_all(copies, "z", 0, 0, tiled=True)
     groups = [near]
     for g in (1, 2, 3):
         groups.append(lax.ppermute(near, "x", around(SHIFTS[g])))
@@ -276,7 +290,7 @@
     listed = lax.all_to_all(listed, EP, 0, 0, tiled=True)
     codes = listed[:, :chunks].astype(jnp.int32)
     gates = listed[:, chunks : 2 * chunks].reshape(lines, LANES)
-    rows = (codes & (exp_dev - 1)).reshape(lines, LANES)
+    rows = ((codes & (exp_dev - 1)) * 2).reshape(lines, LANES)
     place = ((codes >> shift) - 1).reshape(lines, LANES)
     count = jnp.sum((codes > 0).astype(jnp.int32), axis=(1, 2))
 

time: 166 us -> 164 us (0.988)
    all_to_all x0 -> x1, blocking collectives: none -> 26.9 us  [body(): near = lax.all_to_all(copies, 'z', 0, 0, tiled=True)]
    all_to_all x2 -> x1, blocking collectives: 40.4 us -> 13.5 us  [to_each(): lax.all_to_all(jnp.broadcast_to(value[None], (lax.axis_size(axis), *value...]
  transfers between devices with their start and end apart: 7 -> 7, of which waited for: 4 -> 4; matrix products, arithmetic and copies ran while one was open for 0% -> 0% of each run, Pallas kernels for 9% -> 8%
where the time goes in v9:
time: 164 us; the launch traced here: 163 us
  blocking collectives  85.4 us (52%)
  waiting for transfers between devices  27.2 us (17%)
  starting transfers between devices  25.2 us (15%)
  Pallas kernels  20.5 us (12%)
  other arithmetic  3.2 us (2%)
    all_to_all x1, blocking collectives, body(): near = lax.all_to_all(copies, 'z', 0, 0, tiled=True)  26.9 us
    all_gather x1, blocking collectives, body(): score = jnp.sum(lax.all_gather(partial_score, TP), axis=0)  23.4 us
    all_to_all x1, blocking collectives, body(): back = lax.all_to_all(mine, 'z', 0, 0, tiled=True)  21.6 us
    ppermute x3, waiting for transfers between devices, body(): part = lax.ppermute(part, 'x', around(-SHIFTS[g]))  16.6 us
    all_to_all x1, blocking collectives, to_each(): lax.all_to_all(jnp.broadcast_to(value[None], (lax.axis_size(axis), *value...  13.5 us
    all_to_all x1, waiting for transfers between devices, body(): listed = lax.all_to_all(listed, EP, 0, 0, tiled=True)  10.6 us
    ppermute x3, starting transfers between devices, body(): part = lax.ppermute(part, 'x', around(-SHIFTS[g]))  10.5 us
    ppermute x3, starting transfers between devices, body(): groups.append(lax.ppermute(near, 'x', around(SHIFTS[g])))  9.93 us
  transfers between devices with their start and end apart: 7, of which 4 were waited for; matrix products, arithmetic and copies ran while one was open for 0% of the time, Pallas kernels for 8%

profile of v9, /device:TPU:1, one launch (start us, length us, event | category | flops | bytes accessed | tf_op | source)
XLA Modules:
  0.0 163.2 jit_solution(12719160131762019514)
XLA Ops:
  0.0 0.9 repeat.1
  0.9 26.9 %all_to_all.20.refs_3_ = bf16[8,256,128]{2,1,0:T(8,128)(2,1)} all-to-all(bf16[8,256,128]{2,1,0:T(8,128)(2,1)S(1)} %repeat.1), channel_id=1, replica_groups=mesh['z'=8,'x'=4,'y'=8,'core'=2] {'z'}, dimensions={0} | all-to-all | bytes 1048576 | tf_op jit(solution)/shard_map/all_to_all | solution.py:273
  27.8 4.6 %collective-permute-start.1 = (bf16[8,256,128]{2,1,0:T(8,128)(2,1)}, bf16[8,256,128]{2,1,0:T(8,128)(2,1)}, u32[]{:S(2)}, u32[]{:S(2)}) collective-permute-start(bf16[8,256,128]{2,1,0:T(8,128)(2,1)} %all_to_all.20.refs_3_), channel_id=1, source_target_pairs={{0,32},{16,48},{32,0},{48,16},{1,33},{17,49},{33,1},{49,17},{2,34}... | collective-permute-start | bytes 1572872 | tf_op jit(solution)/shard_map/ppermute | solution.py:276
  32.4 2.8 %collective-permute-start.2 = (bf16[8,256,128]{2,1,0:T(8,128)(2,1)}, bf16[8,256,128]{2,1,0:T(8,128)(2,1)}, u32[]{:S(2)}, u32[]{:S(2)}) collective-permute-start(bf16[8,256,128]{2,1,0:T(8,128)(2,1)} %all_to_all.20.refs_3_), channel_id=1, source_target_pairs={{0,48},{16,0},{32,16},{48,32},{1,49},{17,1},{33,17},{49,33},{2,50}... | collective-permute-start | bytes 1572872 | tf_op jit(solution)/shard_map/ppermute | solution.py:276
  35.2 2.5 %collective-permute-start = (bf16[8,256,128]{2,1,0:T(8,128)(2,1)}, bf16[8,256,128]{2,1,0:T(8,128)(2,1)}, u32[]{:S(2)}, u32[]{:S(2)}) collective-permute-start(bf16[8,256,128]{2,1,0:T(8,128)(2,1)} %all_to_all.20.refs_3_), channel_id=1, source_target_pairs={{0,16},{16,32},{32,48},{48,0},{1,17},{17,33},{33,49},{49,1},{2,18}... | collective-permute-start | bytes 1572872 | tf_op jit(solution)/shard_map/ppermute | solution.py:276
  37.7 0.0 copy-start
  37.7 0.7 copy-done
  38.5 0.0 copy-start.1
  38.5 0.7 copy-done.1
  39.2 2.3 %bucket.1 = f32[32,8,128]{2,1,0:T(8,128)} custom-call(s32[16,256]{1,0:T(8,128)S(1)} %bitcast.7, f32[16,256]{1,0:T(8,128)S(1)} %bitcast.8), custom_call_target="tpu_custom_call" | custom-call | tf_op jit(solution)/shard_map/bucket/pallas_call | solution.py:277
  41.4 4.8 %all-to-all-start = ((f32[32,8,128]{2,1,0:T(8,128)}), f32[32,8,128]{2,1,0:T(8,128)S(1)}, u32[]{:S(2)}, u32[]{:S(2)}) async-start(f32[32,8,128]{2,1,0:T(8,128)} %bucket.1), calls=%async_computation | async-start | bytes 262144 | tf_op jit(solution)/shard_map/all_to_all | solution.py:290
  46.2 10.6 %all-to-all-done = f32[32,8,128]{2,1,0:T(8,128)S(1)} async-done(((f32[32,8,128]{2,1,0:T(8,128)}), f32[32,8,128]{2,1,0:T(8,128)S(1)}, u32[]{:S(2)}, u32[]{:S(2)}) %all-to-all-start) | async-done | bytes 131104 | tf_op jit(solution)/shard_map/all_to_all | solution.py:290
  56.8 0.7 shift-right-arithmetic_add_fusion
  57.6 7.4 %pick.1 = (s32[32]{0:T(128)S(1)}, s32[96,128]{1,0:T(8,128)S(1)}, f32[96,128]{1,0:T(8,128)S(1)}, bf16[96,128,128]{2,1,0:T(8,128)(2,1)S(1)}, bf16[96,128,128]{2,1,0:T(8,128)(2,1)S(1)}) custom-call(s32[1]{0:T(128)} %bitcast.x_ref, s32[96,128]{1,0:T(8,128)S(1)} %reshape.28.rows_ref, s32[32]{0:T(128)S(1)} %get-tuple-element.16.count_ref, ...), custom_call_target="tpu_custom_call" | custom-call | tf_op jit(solution)/shard_map/pick/pallas_call | solution.py:299
  64.9 0.0 collective-permute-done.1.refs_4_
  65.0 0.0 collective-permute-done.2.refs_5_
  65.0 2.9 %score.2.refs_4_ = f32[96,128]{1,0:T(8,128)S(1)} custom-call(s32[32]{0:T(128)S(1)} %get-tuple-element.10.refs_0_, s32[96,128]{1,0:T(8,128)S(1)} %get-tuple-element.11.refs_1_, bf16[96,128,128]{2,1,0:T(8,128)(2,1)S(1)} %get-tuple-element.12.refs_2_, bf16[8,256,128]{2,1,0:T(8,128)(2,1)} %all_to_all.20.refs_3_, ...), custom_call_target="tpu_custom_call" | custom-call | tf_op jit(solution)/shard_map/score/pallas_call | solution.py:329
  67.9 0.0 collective-permute-done.refs_3_
  67.9 1.7 %score.3 = f32[96,128]{1,0:T(8,128)S(1)} custom-call(s32[32]{0:T(128)S(1)} %get-tuple-element.10.refs_0_, s32[96,128]{1,0:T(8,128)S(1)} %get-tuple-element.11.refs_1_, bf16[96,128,128]{2,1,0:T(8,128)(2,1)S(1)} %get-tuple-element.12.refs_2_, bf16[8,256,128]{2,1,0:T(8,128)(2,1)} %collective-permute-done.refs_3_, f32[96,128]{1,0:T(8,128)S(1)} %score.2.refs_4_), custom_call_target="tpu_custom_call" | custom-call | tf_op jit(solution)/shard_map/score/pallas_call | solution.py:329
  69.6 23.4 %all-gather = f32[1536,128]{1,0:T(8,128)} all-gather(f32[96,128]{1,0:T(8,128)S(1)} %score.3), channel_id=2, replica_groups=mesh['z'=8,'x'=4,'y'=8,'core'=2] {'y','core'}, dimensions={0}, use_global_device_ids=true | all-gather | bytes 835584 | tf_op jit(solution)/shard_map/all_gather | solution.py:341
  92.9 1.2 reduce_sum.46
  94.1 0.1 fusion.3.refs_2_
  94.2 1.3 combine.4
  95.6 1.3 combine.5
  96.9 1.3 combine.6
  98.3 3.9 %collective-permute-start.3 = (bf16[8,256,128]{2,1,0:T(8,128)(2,1)S(1)}, bf16[8,256,128]{2,1,0:T(8,128)(2,1)S(1)}, u32[]{:S(2)}, u32[]{:S(2)}) collective-permute-start(bf16[8,256,128]{2,1,0:T(8,128)(2,1)S(1)} %combine.4), channel_id=1, source_target_pairs={{0,32},{16,48},{32,0},{48,16},{1,33},{17,49},{33,1},{49,17},{2,34}... | collective-permute-start | bytes 1572872 | tf_op jit(solution)/shard_map/ppermute | solution.py:360
  102.2 4.7 %collective-permute-start.4 = (bf16[8,256,128]{2,1,0:T(8,128)(2,1)S(1)}, bf16[8,256,128]{2,1,0:T(8,128)(2,1)S(1)}, u32[]{:S(2)}, u32[]{:S(2)}) collective-permute-start(bf16[8,256,128]{2,1,0:T(8,128)(2,1)S(1)} %combine.5), channel_id=1, source_target_pairs={{0,48},{16,0},{32,16},{48,32},{1,49},{17,1},{33,17},{49,33},{2,50}... | collective-permute-start | bytes 1572872 | tf_op jit(solution)/shard_map/ppermute | solution.py:360
  106.9 1.9 %collective-permute-start.5 = (bf16[8,256,128]{2,1,0:T(8,128)(2,1)S(1)}, bf16[8,256,128]{2,1,0:T(8,128)(2,1)S(1)}, u32[]{:S(2)}, u32[]{:S(2)}) collective-permute-start(bf16[8,256,128]{2,1,0:T(8,128)(2,1)S(1)} %combine.6), channel_id=1, source_target_pairs={{0,16},{16,32},{32,48},{48,0},{1,17},{17,33},{33,49},{49,1},{2,18}... | collective-permute-start | bytes 1572872 | tf_op jit(solution)/shard_map/ppermute | solution.py:360
  108.8 1.3 combine.7
  110.2 0.0 copy-start.2
  110.2 4.8 %collective-permute-done.3 = bf16[8,256,128]{2,1,0:T(8,128)(2,1)S(1)} collective-permute-done((bf16[8,256,128]{2,1,0:T(8,128)(2,1)S(1)}, bf16[8,256,128]{2,1,0:T(8,128)(2,1)S(1)}, u32[]{:S(2)}, u32[]{:S(2)}) %collective-permute-start.3) | collective-permute-done | bytes 524320 | tf_op jit(solution)/shard_map/ppermute | solution.py:360
  115.0 11.5 %collective-permute-done.4 = bf16[8,256,128]{2,1,0:T(8,128)(2,1)S(1)} collective-permute-done((bf16[8,256,128]{2,1,0:T(8,128)(2,1)S(1)}, bf16[8,256,128]{2,1,0:T(8,128)(2,1)S(1)}, u32[]{:S(2)}, u32[]{:S(2)}) %collective-permute-start.4) | collective-permute-done | bytes 524320 | tf_op jit(solution)/shard_map/ppermute | solution.py:360
  126.5 0.2 collective-permute-done.5
  126.8 0.3 add_convert_fusion
  127.0 21.6 %all_to_all.21 = bf16[8,256,128]{2,1,0:T(8,128)(2,1)S(1)} all-to-all(bf16[8,256,128]{2,1,0:T(8,128)(2,1)S(1)} %add_convert_fusion), channel_id=1, replica_groups=mesh['z'=8,'x'=4,'y'=8,'core'=2] {'z'}, dimensions={0} | all-to-all | bytes 1048576 | tf_op jit(solution)/shard_map/all_to_all | solution.py:363
  148.7 0.1 convert_reduce_fusion
  148.7 0.1 multiply_reduce_fusion
  148.9 13.5 %all_to_all.22 = f32[16,2,128]{2,1,0:T(2,128)S(1)} all-to-all(f32[16,2,128]{2,1,0:T(2,128)S(1)} %broadcast_in_dim.12), channel_id=1, replica_groups=mesh['z'=8,'x'=4,'y'=8,'core'=2] {'y','core'}, dimensions={0} | all-to-all | bytes 32768 | tf_op jit(solution)/shard_map/all_to_all | solution.py:245
  162.4 0.0 copy-done.2
  162.4 0.7 multiply_convert_fusion
  (7 shorter events, 0.1 us)
Async XLA Ops:
  27.8 37.2 %collective-permute-start.1 = (bf16[8,256,128]{2,1,0:T(8,128)(2,1)}, bf16[8,256,128]{2,1,0:T(8,128)(2,1)}, u32[]{:S(2)}, u32[]{:S(2)}) collective-permute-start(bf16[8,256,128]{2,1,0:T(8,128)(2,1)} %all_to_all.20.refs_3_), channel_id=1, source_target_pairs={{0,32},{16,48},{32,0},{48,16},{1,33},{17,49},{33,1},{49,17},{2,34}... | collective-permute-start | bytes 1572872 | tf_op jit(solution)/shard_map/ppermute | solution.py:276
  32.4 32.5 %collective-permute-start.2 = (bf16[8,256,128]{2,1,0:T(8,128)(2,1)}, bf16[8,256,128]{2,1,0:T(8,128)(2,1)}, u32[]{:S(2)}, u32[]{:S(2)}) collective-permute-start(bf16[8,256,128]{2,1,0:T(8,128)(2,1)} %all_to_all.20.refs_3_), channel_id=1, source_target_pairs={{0,48},{16,0},{32,16},{48,32},{1,49},{17,1},{33,17},{49,33},{2,50}... | collective-permute-start | bytes 1572872 | tf_op jit(solution)/shard_map/ppermute | solution.py:276
  35.2 32.6 %collective-permute-start = (bf16[8,256,128]{2,1,0:T(8,128)(2,1)}, bf16[8,256,128]{2,1,0:T(8,128)(2,1)}, u32[]{:S(2)}, u32[]{:S(2)}) collective-permute-start(bf16[8,256,128]{2,1,0:T(8,128)(2,1)} %all_to_all.20.refs_3_), channel_id=1, source_target_pairs={{0,16},{16,32},{32,48},{48,0},{1,17},{17,33},{33,49},{49,1},{2,18}... | collective-permute-start | bytes 1572872 | tf_op jit(solution)/shard_map/ppermute | solution.py:276
  37.7 0.7 copy-start
  38.5 0.7 copy-start.1
  41.4 15.3 %all-to-all-start = ((f32[32,8,128]{2,1,0:T(8,128)}), f32[32,8,128]{2,1,0:T(8,128)S(1)}, u32[]{:S(2)}, u32[]{:S(2)}) async-start(f32[32,8,128]{2,1,0:T(8,128)} %bucket.1), calls=%async_computation | async-start | bytes 262144 | tf_op jit(solution)/shard_map/all_to_all | solution.py:290
  98.3 16.8 %collective-permute-start.3 = (bf16[8,256,128]{2,1,0:T(8,128)(2,1)S(1)}, bf16[8,256,128]{2,1,0:T(8,128)(2,1)S(1)}, u32[]{:S(2)}, u32[]{:S(2)}) collective-permute-start(bf16[8,256,128]{2,1,0:T(8,128)(2,1)S(1)} %combine.4), channel_id=1, source_target_pairs={{0,32},{16,48},{32,0},{48,16},{1,33},{17,49},{33,1},{49,17},{2,34}... | collective-permute-start | bytes 1572872 | tf_op jit(solution)/shard_map/ppermute | solution.py:360
  102.2 24.3 %collective-permute-start.4 = (bf16[8,256,128]{2,1,0:T(8,128)(2,1)S(1)}, bf16[8,256,128]{2,1,0:T(8,128)(2,1)S(1)}, u32[]{:S(2)}, u32[]{:S(2)}) collective-permute-start(bf16[8,256,128]{2,1,0:T(8,128)(2,1)S(1)} %combine.5), channel_id=1, source_target_pairs={{0,48},{16,0},{32,16},{48,32},{1,49},{17,1},{33,17},{49,33},{2,50}... | collective-permute-start | bytes 1572872 | tf_op jit(solution)/shard_map/ppermute | solution.py:360
  106.9 19.8 %collective-permute-start.5 = (bf16[8,256,128]{2,1,0:T(8,128)(2,1)S(1)}, bf16[8,256,128]{2,1,0:T(8,128)(2,1)S(1)}, u32[]{:S(2)}, u32[]{:S(2)}) collective-permute-start(bf16[8,256,128]{2,1,0:T(8,128)(2,1)S(1)} %combine.6), channel_id=1, source_target_pairs={{0,16},{16,32},{32,48},{48,0},{1,17},{17,33},{33,49},{49,1},{2,18}... | collective-permute-start | bytes 1572872 | tf_op jit(solution)/shard_map/ppermute | solution.py:360
  110.2 52.2 %copy-start.2 = (f32[128]{0:T(128)S(1)}, f32[128]{0:T(128)}, u32[]{:S(2)}) copy-start(f32[128]{0:T(128)} %param.11) | copy-start | bytes 1540

commit v10 on v9

--- a/solution.py
+++ b/solution.py
@@ -161,7 +161,7 @@
         here = place_ref[pl.ds(line, 1), :] == token_of
         return jnp.sum(jnp.where(here, prod, 0.0), axis=0, keepdims=True)
 
-    per = 4 if len(members) == 1 else 2
+    per = 2
 
     def first(step, carry):
         jobs = [(g, step * per + j) for j in range(per) for g in members]
@@ -197,7 +197,7 @@
         weight = jnp.where(here, hidden_ref[pl.ds(line, 1), :], 0.0)
         high = weight.astype(jnp.bfloat16)
         low = (weight - high.astype(jnp.float32)).astype(jnp.bfloat16)
-        rows = values_ref[line]
+        rows = values_ref[z * chunks + c]
         return jnp.dot(
             jnp.concatenate([high, low], axis=1),
             jnp.concatenate([rows, rows], axis=0),
@@ -231,6 +231,10 @@
 
 def made(shape, dtype):
     return jax.ShapeDtypeStruct(shape, dtype) if INTERPRET else pltpu.VMEM(shape, dtype)
+
+
+def stored(shape, dtype):
+    return jax.ShapeDtypeStruct(shape, dtype) if INTERPRET else pltpu.HBM(shape, dtype)
 
 
 def held(value, where=pltpu.VMEM):
@@ -303,7 +307,7 @@
             jax.ShapeDtypeStruct((lines, LANES), jnp.int32),
             jax.ShapeDtypeStruct((lines, LANES), jnp.float32),
             picked,
-            picked,
+            stored((lines, LANES, width), jnp.bfloat16),
         ),
         in_specs=[smem(), smem(), smem(), vmem(), vmem(), vmem(), vmem()],
         out_specs=(smem(), vmem(), vmem(), vmem(), vmem()),
@@ -336,8 +340,8 @@
             name="score",
         )(count, held(place), held(keys), *toks, *before)
 
-    partial_score = scored((0, 1, 3))
-    partial_score = scored((2,), held(partial_score))
+    partial_score = scored((0, 1))
+    partial_score = scored((2, 3), held(partial_score))
     score = jnp.sum(lax.all_gather(partial_score, TP), axis=0)
     hidden = jnp.where(place >= 0, jax.nn.gelu(score, approximate=False) * gates, 0.0)
 
@@ -345,16 +349,22 @@
         return pl.pallas_call(
             lambda *refs: combine_kernel(*refs, group=group),
             out_shape=made((n_z, tok, width), jnp.bfloat16),
-            in_specs=[smem(), vmem(), vmem(), vmem()],
+            grid=(1,),
+            in_specs=[
+                smem(),
+                vmem(),
+                vmem(),
+                pl.BlockSpec((n_z * chunks, LANES, width), lambda i: (group, 0, 0)),
+            ],
             out_specs=vmem(),
             scratch_shapes=[pltpu.VMEM((n_z, tok, width), jnp.float32)],
             interpret=INTERPRET,
             compiler_params=pltpu.CompilerParams(vmem_limit_bytes=ROOM),
             name="combine",
-        )(count, held(place), held(hidden), held(values))
+        )(count, held(place), held(hidden), held(values, pltpu.HBM))
 
     parts = []
-    for g in (1, 2, 3, 0):
+    for g in (2, 3, 1, 0):
         part = combine(g)
         if g:
             part = lax.ppermute(part, "x", around(-SHIFTS[g]))

time: 164 us -> 166 us (1.012)
  waiting for transfers between devices: 27.2 us -> 30.8 us
  Pallas kernels: 20.5 us -> 22.9 us
  blocking collectives: 85.4 us -> 83.4 us
    ppermute x3, waiting for transfers between devices: 16.6 us -> 20 us  [body(): part = lax.ppermute(part, 'x', around(-SHIFTS[g]))]
    pallas_call x4, Pallas kernels: 5.33 us -> 7.74 us  [combine(): pl.pallas_call(lambda *refs: combine_kernel(*refs, group=group), out_shap...]
    all_to_all x1, blocking collectives: 21.6 us -> 19.5 us  [body(): back = lax.all_to_all(mine, 'z', 0, 0, tiled=True)]
  transfers between devices with their start and end apart: 7 -> 7, of which waited for: 4 -> 3; matrix products, arithmetic and copies ran while one was open for 0% -> 0% of each run, Pallas kernels for 8% -> 9%
where the time goes in v10:
time: 166 us; the launch traced here: 165 us
  blocking collectives  83.4 us (50%)
  waiting for transfers between devices  30.8 us (19%)
  starting transfers between devices  24.3 us (15%)
  Pallas kernels  22.9 us (14%)
  other arithmetic  2.06 us (1%)
    all_to_all x1, blocking collectives, body(): near = lax.all_to_all(copies, 'z', 0, 0, tiled=True)  26.8 us
    all_gather x1, blocking collectives, body(): score = jnp.sum(lax.all_gather(partial_score, TP), axis=0)  22.5 us
    ppermute x3, waiting for transfers between devices, body(): part = lax.ppermute(part, 'x', around(-SHIFTS[g]))  20 us
    all_to_all x1, blocking collectives, body(): back = lax.all_to_all(mine, 'z', 0, 0, tiled=True)  19.5 us
    all_to_all x1, blocking collectives, to_each(): lax.all_to_all(jnp.broadcast_to(value[None], (lax.axis_size(axis), *value...  14.6 us
    ppermute x3, starting transfers between devices, body(): groups.append(lax.ppermute(near, 'x', around(SHIFTS[g])))  11.1 us
    all_to_all x1, waiting for transfers between devices, body(): listed = lax.all_to_all(listed, EP, 0, 0, tiled=True)  10.8 us
    ppermute x3, starting transfers between devices, body(): part = lax.ppermute(part, 'x', around(-SHIFTS[g]))  9.32 us
  transfers between devices with their start and end apart: 7, of which 3 were waited for; matrix products, arithmetic and copies ran while one was open for 0% of the time, Pallas kernels for 9%

profile of v10, /device:TPU:1, one launch (start us, length us, event | category | flops | bytes accessed | tf_op | source)
XLA Modules:
  0.0 165.3 jit_solution(1670908832597210364)
XLA Ops:
  0.0 0.9 repeat.1
  0.9 26.8 %all_to_all.20.refs_3_ = bf16[8,256,128]{2,1,0:T(8,128)(2,1)S(1)} all-to-all(bf16[8,256,128]{2,1,0:T(8,128)(2,1)S(1)} %repeat.1), channel_id=1, replica_groups=mesh['z'=8,'x'=4,'y'=8,'core'=2] {'z'}, dimensions={0} | all-to-all | bytes 1048576 | tf_op jit(solution)/shard_map/all_to_all | solution.py:277
  27.7 4.6 %collective-permute-start.2 = (bf16[8,256,128]{2,1,0:T(8,128)(2,1)S(1)}, bf16[8,256,128]{2,1,0:T(8,128)(2,1)S(1)}, u32[]{:S(2)}, u32[]{:S(2)}) collective-permute-start(bf16[8,256,128]{2,1,0:T(8,128)(2,1)S(1)} %all_to_all.20.refs_3_), channel_id=1, source_target_pairs={{0,32},{16,48},{32,0},{48,16},{1,33},{17,49},{33,1},{49,17},{2,34}... | collective-permute-start | bytes 1572872 | tf_op jit(solution)/shard_map/ppermute | solution.py:280
  32.3 2.2 %collective-permute-start = (bf16[8,256,128]{2,1,0:T(8,128)(2,1)S(1)}, bf16[8,256,128]{2,1,0:T(8,128)(2,1)S(1)}, u32[]{:S(2)}, u32[]{:S(2)}) collective-permute-start(bf16[8,256,128]{2,1,0:T(8,128)(2,1)S(1)} %all_to_all.20.refs_3_), channel_id=1, source_target_pairs={{0,16},{16,32},{32,48},{48,0},{1,17},{17,33},{33,49},{49,1},{2,18}... | collective-permute-start | bytes 1572872 | tf_op jit(solution)/shard_map/ppermute | solution.py:280
  34.6 4.3 %collective-permute-start.1 = (bf16[8,256,128]{2,1,0:T(8,128)(2,1)S(1)}, bf16[8,256,128]{2,1,0:T(8,128)(2,1)S(1)}, u32[]{:S(2)}, u32[]{:S(2)}) collective-permute-start(bf16[8,256,128]{2,1,0:T(8,128)(2,1)S(1)} %all_to_all.20.refs_3_), channel_id=1, source_target_pairs={{0,48},{16,0},{32,16},{48,32},{1,49},{17,1},{33,17},{49,33},{2,50}... | collective-permute-start | bytes 1572872 | tf_op jit(solution)/shard_map/ppermute | solution.py:280
  38.8 0.0 copy-start
  38.8 0.7 copy-done
  39.6 0.0 copy-start.1
  39.6 0.7 copy-done.1
  40.3 2.2 %bucket.1 = f32[32,8,128]{2,1,0:T(8,128)} custom-call(s32[16,256]{1,0:T(8,128)S(1)} %bitcast.7, f32[16,256]{1,0:T(8,128)S(1)} %bitcast.8), custom_call_target="tpu_custom_call" | custom-call | tf_op jit(solution)/shard_map/bucket/pallas_call | solution.py:281
  42.5 3.9 %all-to-all-start = ((f32[32,8,128]{2,1,0:T(8,128)}), f32[32,8,128]{2,1,0:T(8,128)S(1)}, u32[]{:S(2)}, u32[]{:S(2)}) async-start(f32[32,8,128]{2,1,0:T(8,128)} %bucket.1), calls=%async_computation | async-start | bytes 262144 | tf_op jit(solution)/shard_map/all_to_all | solution.py:294
  46.4 10.8 %all-to-all-done = f32[32,8,128]{2,1,0:T(8,128)S(1)} async-done(((f32[32,8,128]{2,1,0:T(8,128)}), f32[32,8,128]{2,1,0:T(8,128)S(1)}, u32[]{:S(2)}, u32[]{:S(2)}) %all-to-all-start) | async-done | bytes 131104 | tf_op jit(solution)/shard_map/all_to_all | solution.py:294
  57.2 0.7 shift-right-arithmetic_add_fusion
  58.0 8.5 %pick.1 = (s32[32]{0:T(128)S(1)}, s32[96,128]{1,0:T(8,128)S(1)}, f32[96,128]{1,0:T(8,128)S(1)}, bf16[96,128,128]{2,1,0:T(8,128)(2,1)S(1)}, bf16[96,128,128]{2,1,0:T(8,128)(2,1)}) custom-call(s32[1]{0:T(128)} %bitcast.x_ref, s32[96,128]{1,0:T(8,128)S(1)} %reshape.28.rows_ref, s32[32]{0:T(128)S(1)} %get-tuple-element.16.count_ref, ...), custom_call_target="tpu_custom_call" | custom-call | tf_op jit(solution)/shard_map/pick/pallas_call | solution.py:303
  66.4 0.0 collective-permute-done.2.refs_4_
  66.5 1.8 %score.2.refs_5_ = f32[96,128]{1,0:T(8,128)S(1)} custom-call(s32[32]{0:T(128)S(1)} %get-tuple-element.10.refs_0_, s32[96,128]{1,0:T(8,128)S(1)} %get-tuple-element.11.refs_1_, bf16[96,128,128]{2,1,0:T(8,128)(2,1)S(1)} %get-tuple-element.12.refs_2_, bf16[8,256,128]{2,1,0:T(8,128)(2,1)S(1)} %all_to_all.20.refs_3_, ...), custom_call_target="tpu_custom_call" | custom-call | tf_op jit(solution)/shard_map/score/pallas_call | solution.py:333
  68.3 0.0 collective-permute-done.refs_3_
  68.3 0.0 collective-permute-done.1.refs_4_
  68.3 1.8 %score.3 = f32[96,128]{1,0:T(8,128)S(1)} custom-call(s32[32]{0:T(128)S(1)} %get-tuple-element.10.refs_0_, s32[96,128]{1,0:T(8,128)S(1)} %get-tuple-element.11.refs_1_, bf16[96,128,128]{2,1,0:T(8,128)(2,1)S(1)} %get-tuple-element.12.refs_2_, bf16[8,256,128]{2,1,0:T(8,128)(2,1)S(1)} %collective-permute-done.refs_3_, ...), custom_call_target="tpu_custom_call" | custom-call | tf_op jit(solution)/shard_map/score/pallas_call | solution.py:333
  70.1 22.5 %all-gather = f32[1536,128]{1,0:T(8,128)S(1)} all-gather(f32[96,128]{1,0:T(8,128)S(1)} %score.3), channel_id=2, replica_groups=mesh['z'=8,'x'=4,'y'=8,'core'=2] {'y','core'}, dimensions={0}, use_global_device_ids=true | all-gather | bytes 835584 | tf_op jit(solution)/shard_map/all_gather | solution.py:345
  92.6 0.1 fusion.3.refs_2_
  92.7 1.9 %combine.4 = bf16[8,256,128]{2,1,0:T(8,128)(2,1)S(1)} custom-call(s32[32]{0:T(128)S(1)} %get-tuple-element.10.refs_0_, s32[96,128]{1,0:T(8,128)S(1)} %get-tuple-element.11.refs_1_, f32[96,128]{1,0:T(8,128)S(1)} %fusion.3.refs_2_, bf16[96,128,128]{2,1,0:T(8,128)(2,1)} %get-tuple-element.14.refs_3_), custom_call_target="tpu_custom_call" | custom-call | tf_op jit(solution)/shard_map/combine/pallas_call | solution.py:349
  94.7 1.9 %combine.5 = bf16[8,256,128]{2,1,0:T(8,128)(2,1)S(1)} custom-call(s32[32]{0:T(128)S(1)} %get-tuple-element.10.refs_0_, s32[96,128]{1,0:T(8,128)S(1)} %get-tuple-element.11.refs_1_, f32[96,128]{1,0:T(8,128)S(1)} %fusion.3.refs_2_, bf16[96,128,128]{2,1,0:T(8,128)(2,1)} %get-tuple-element.14.refs_3_), custom_call_target="tpu_custom_call" | custom-call | tf_op jit(solution)/shard_map/combine/pallas_call | solution.py:349
  96.6 1.9 %combine.6 = bf16[8,256,128]{2,1,0:T(8,128)(2,1)S(1)} custom-call(s32[32]{0:T(128)S(1)} %get-tuple-element.10.refs_0_, s32[96,128]{1,0:T(8,128)S(1)} %get-tuple-element.11.refs_1_, f32[96,128]{1,0:T(8,128)S(1)} %fusion.3.refs_2_, bf16[96,128,128]{2,1,0:T(8,128)(2,1)} %get-tuple-element.14.refs_3_), custom_call_target="tpu_custom_call" | custom-call | tf_op jit(solution)/shard_map/combine/pallas_call | solution.py:349
  98.6 3.9 %collective-permute-start.3 = (bf16[8,256,128]{2,1,0:T(8,128)(2,1)S(1)}, bf16[8,256,128]{2,1,0:T(8,128)(2,1)S(1)}, u32[]{:S(2)}, u32[]{:S(2)}) collective-permute-start(bf16[8,256,128]{2,1,0:T(8,128)(2,1)S(1)} %combine.4), channel_id=1, source_target_pairs={{0,48},{16,0},{32,16},{48,32},{1,49},{17,1},{33,17},{49,33},{2,50}... | collective-permute-start | bytes 1572872 | tf_op jit(solution)/shard_map/ppermute | solution.py:370
  102.5 1.9 %collective-permute-start.4 = (bf16[8,256,128]{2,1,0:T(8,128)(2,1)S(1)}, bf16[8,256,128]{2,1,0:T(8,128)(2,1)S(1)}, u32[]{:S(2)}, u32[]{:S(2)}) collective-permute-start(bf16[8,256,128]{2,1,0:T(8,128)(2,1)S(1)} %combine.5), channel_id=1, source_target_pairs={{0,16},{16,32},{32,48},{48,0},{1,17},{17,33},{33,49},{49,1},{2,18}... | collective-permute-start | bytes 1572872 | tf_op jit(solution)/shard_map/ppermute | solution.py:370
  104.4 3.5 %collective-permute-start.5 = (bf16[8,256,128]{2,1,0:T(8,128)(2,1)S(1)}, bf16[8,256,128]{2,1,0:T(8,128)(2,1)S(1)}, u32[]{:S(2)}, u32[]{:S(2)}) collective-permute-start(bf16[8,256,128]{2,1,0:T(8,128)(2,1)S(1)} %combine.6), channel_id=1, source_target_pairs={{0,32},{16,48},{32,0},{48,16},{1,33},{17,49},{33,1},{49,17},{2,34}... | collective-permute-start | bytes 1572872 | tf_op jit(solution)/shard_map/ppermute | solution.py:370
  107.9 1.9 %combine.7 = bf16[8,256,128]{2,1,0:T(8,128)(2,1)S(1)} custom-call(s32[32]{0:T(128)S(1)} %get-tuple-element.10.refs_0_, s32[96,128]{1,0:T(8,128)S(1)} %get-tuple-element.11.refs_1_, f32[96,128]{1,0:T(8,128)S(1)} %fusion.3.refs_2_, bf16[96,128,128]{2,1,0:T(8,128)(2,1)} %get-tuple-element.14.refs_3_), custom_call_target="tpu_custom_call" | custom-call | tf_op jit(solution)/shard_map/combine/pallas_call | solution.py:349
  109.9 0.0 copy-start.2
  109.9 4.5 %collective-permute-done.3 = bf16[8,256,128]{2,1,0:T(8,128)(2,1)S(1)} collective-permute-done((bf16[8,256,128]{2,1,0:T(8,128)(2,1)S(1)}, bf16[8,256,128]{2,1,0:T(8,128)(2,1)S(1)}, u32[]{:S(2)}, u32[]{:S(2)}) %collective-permute-start.3) | collective-permute-done | bytes 524320 | tf_op jit(solution)/shard_map/ppermute | solution.py:370
  114.4 15.5 %collective-permute-done.4 = bf16[8,256,128]{2,1,0:T(8,128)(2,1)S(1)} collective-permute-done((bf16[8,256,128]{2,1,0:T(8,128)(2,1)S(1)}, bf16[8,256,128]{2,1,0:T(8,128)(2,1)S(1)}, u32[]{:S(2)}, u32[]{:S(2)}) %collective-permute-start.4) | collective-permute-done | bytes 524320 | tf_op jit(solution)/shard_map/ppermute | solution.py:370
  129.9 0.0 collective-permute-done.5
  129.9 0.3 add_convert_fusion
  130.2 19.5 %all_to_all.21 = bf16[8,256,128]{2,1,0:T(8,128)(2,1)S(1)} all-to-all(bf16[8,256,128]{2,1,0:T(8,128)(2,1)S(1)} %add_convert_fusion), channel_id=1, replica_groups=mesh['z'=8,'x'=4,'y'=8,'core'=2] {'z'}, dimensions={0} | all-to-all | bytes 1048576 | tf_op jit(solution)/shard_map/all_to_all | solution.py:373
  149.7 0.1 convert_reduce_fusion
  149.7 0.1 multiply_reduce_fusion
  149.9 14.6 %all_to_all.22 = f32[16,2,128]{2,1,0:T(2,128)S(1)} all-to-all(f32[16,2,128]{2,1,0:T(2,128)S(1)} %broadcast_in_dim.12), channel_id=1, replica_groups=mesh['z'=8,'x'=4,'y'=8,'core'=2] {'y','core'}, dimensions={0} | all-to-all | bytes 32768 | tf_op jit(solution)/shard_map/all_to_all | solution.py:249
  164.5 0.0 copy-done.2
  164.5 0.7 multiply_convert_fusion
  (8 shorter events, 0.2 us)
Async XLA Ops:
  27.7 38.8 %collective-permute-start.2 = (bf16[8,256,128]{2,1,0:T(8,128)(2,1)S(1)}, bf16[8,256,128]{2,1,0:T(8,128)(2,1)S(1)}, u32[]{:S(2)}, u32[]{:S(2)}) collective-permute-start(bf16[8,256,128]{2,1,0:T(8,128)(2,1)S(1)} %all_to_all.20.refs_3_), channel_id=1, source_target_pairs={{0,32},{16,48},{32,0},{48,16},{1,33},{17,49},{33,1},{49,17},{2,34}... | collective-permute-start | bytes 1572872 | tf_op jit(solution)/shard_map/ppermute | solution.py:280
  32.3 35.9 %collective-permute-start = (bf16[8,256,128]{2,1,0:T(8,128)(2,1)S(1)}, bf16[8,256,128]{2,1,0:T(8,128)(2,1)S(1)}, u32[]{:S(2)}, u32[]{:S(2)}) collective-permute-start(bf16[8,256,128]{2,1,0:T(8,128)(2,1)S(1)} %all_to_all.20.refs_3_), channel_id=1, source_target_pairs={{0,16},{16,32},{32,48},{48,0},{1,17},{17,33},{33,49},{49,1},{2,18}... | collective-permute-start | bytes 1572872 | tf_op jit(solution)/shard_map/ppermute | solution.py:280
  34.6 33.7 %collective-permute-start.1 = (bf16[8,256,128]{2,1,0:T(8,128)(2,1)S(1)}, bf16[8,256,128]{2,1,0:T(8,128)(2,1)S(1)}, u32[]{:S(2)}, u32[]{:S(2)}) collective-permute-start(bf16[8,256,128]{2,1,0:T(8,128)(2,1)S(1)} %all_to_all.20.refs_3_), channel_id=1, source_target_pairs={{0,48},{16,0},{32,16},{48,32},{1,49},{17,1},{33,17},{49,33},{2,50}... | collective-permute-start | bytes 1572872 | tf_op jit(solution)/shard_map/ppermute | solution.py:280
  38.8 0.7 copy-start
  39.6 0.7 copy-start.1
  42.5 14.7 %all-to-all-start = ((f32[32,8,128]{2,1,0:T(8,128)}), f32[32,8,128]{2,1,0:T(8,128)S(1)}, u32[]{:S(2)}, u32[]{:S(2)}) async-start(f32[32,8,128]{2,1,0:T(8,128)} %bucket.1), calls=%async_computation | async-start | bytes 262144 | tf_op jit(solution)/shard_map/all_to_all | solution.py:294
  98.6 15.8 %collective-permute-start.3 = (bf16[8,256,128]{2,1,0:T(8,128)(2,1)S(1)}, bf16[8,256,128]{2,1,0:T(8,128)(2,1)S(1)}, u32[]{:S(2)}, u32[]{:S(2)}) collective-permute-start(bf16[8,256,128]{2,1,0:T(8,128)(2,1)S(1)} %combine.4), channel_id=1, source_target_pairs={{0,48},{16,0},{32,16},{48,32},{1,49},{17,1},{33,17},{49,33},{2,50}... | collective-permute-start | bytes 1572872 | tf_op jit(solution)/shard_map/ppermute | solution.py:370
  102.5 27.4 %collective-permute-start.4 = (bf16[8,256,128]{2,1,0:T(8,128)(2,1)S(1)}, bf16[8,256,128]{2,1,0:T(8,128)(2,1)S(1)}, u32[]{:S(2)}, u32[]{:S(2)}) collective-permute-start(bf16[8,256,128]{2,1,0:T(8,128)(2,1)S(1)} %combine.5), channel_id=1, source_target_pairs={{0,16},{16,32},{32,48},{48,0},{1,17},{17,33},{33,49},{49,1},{2,18}... | collective-permute-start | bytes 1572872 | tf_op jit(solution)/shard_map/ppermute | solution.py:370
  104.4 25.5 %collective-permute-start.5 = (bf16[8,256,128]{2,1,0:T(8,128)(2,1)S(1)}, bf16[8,256,128]{2,1,0:T(8,128)(2,1)S(1)}, u32[]{:S(2)}, u32[]{:S(2)}) collective-permute-start(bf16[8,256,128]{2,1,0:T(8,128)(2,1)S(1)} %combine.6), channel_id=1, source_target_pairs={{0,32},{16,48},{32,0},{48,16},{1,33},{17,49},{33,1},{49,17},{2,34}... | collective-permute-start | bytes 1572872 | tf_op jit(solution)/shard_map/ppermute | solution.py:370
  109.9 54.7 %copy-start.2 = (f32[128]{0:T(128)S(1)}, f32[128]{0:T(128)}, u32[]{:S(2)}) copy-start(f32[128]{0:T(128)} %param.11) | copy-start | bytes 1540

commit v11 on v10

--- a/solution.py
+++ b/solution.py
@@ -161,7 +161,7 @@
         here = place_ref[pl.ds(line, 1), :] == token_of
         return jnp.sum(jnp.where(here, prod, 0.0), axis=0, keepdims=True)
 
-    per = 2
+    per = 4
 
     def first(step, carry):
         jobs = [(g, step * per + j) for j in range(per) for g in members]
@@ -231,10 +231,6 @@
 
 def made(shape, dtype):
     return jax.ShapeDtypeStruct(shape, dtype) if INTERPRET else pltpu.VMEM(shape, dtype)
-
-
-def stored(shape, dtype):
-    return jax.ShapeDtypeStruct(shape, dtype) if INTERPRET else pltpu.HBM(shape, dtype)
 
 
 def held(value, where=pltpu.VMEM):
@@ -307,7 +303,7 @@
             jax.ShapeDtypeStruct((lines, LANES), jnp.int32),
             jax.ShapeDtypeStruct((lines, LANES), jnp.float32),
             picked,
-            stored((lines, LANES, width), jnp.bfloat16),
+            jax.ShapeDtypeStruct(picked.shape, picked.dtype),
         ),
         in_specs=[smem(), smem(), smem(), vmem(), vmem(), vmem(), vmem()],
         out_specs=(smem(), vmem(), vmem(), vmem(), vmem()),
@@ -364,7 +360,7 @@
         )(count, held(place), held(hidden), held(values, pltpu.HBM))
 
     parts = []
-    for g in (2, 3, 1, 0):
+    for g in (1, 2, 3, 0):
         part = combine(g)
         if g:
             part = lax.ppermute(part, "x", around(-SHIFTS[g]))

time: 166 us -> 164 us (0.988)
  waiting for transfers between devices: 30.8 us -> 27.4 us
  Pallas kernels: 22.9 us -> 21.2 us
    ppermute x3, waiting for transfers between devices: 20 us -> 16.6 us  [body(): part = lax.ppermute(part, 'x', around(-SHIFTS[g]))]
    all_to_all x1, blocking collectives: 19.5 us -> 21.4 us  [body(): back = lax.all_to_all(mine, 'z', 0, 0, tiled=True)]
  transfers between devices with their start and end apart: 7 -> 7, of which waited for: 3 -> 4; matrix products, arithmetic and copies ran while one was open for 0% -> 0% of each run, Pallas kernels for 9% -> 8%
where the time goes in v11:
time: 164 us; the launch traced here: 163 us
  blocking collectives  84.2 us (51%)
  waiting for transfers between devices  27.4 us (17%)
  starting transfers between devices  24.9 us (15%)
  Pallas kernels  21.2 us (13%)
  local copies, waits for them, and re-layouts  3.19 us (2%)
  other arithmetic  2.06 us (1%)
    all_to_all x1, blocking collectives, body(): near = lax.all_to_all(copies, 'z', 0, 0, tiled=True)  26.8 us
    all_gather x1, blocking collectives, body(): score = jnp.sum(lax.all_gather(partial_score, TP), axis=0)  22.5 us
    all_to_all x1, blocking collectives, body(): back = lax.all_to_all(mine, 'z', 0, 0, tiled=True)  21.4 us
    ppermute x3, waiting for transfers between devices, body(): part = lax.ppermute(part, 'x', around(-SHIFTS[g]))  16.6 us
    all_to_all x1, blocking collectives, to_each(): lax.all_to_all(jnp.broadcast_to(value[None], (lax.axis_size(axis), *value...  13.5 us
    ppermute x3, starting transfers between devices, body(): groups.append(lax.ppermute(near, 'x', around(SHIFTS[g])))  11.1 us
    all_to_all x1, waiting for transfers between devices, body(): listed = lax.all_to_all(listed, EP, 0, 0, tiled=True)  10.8 us
    ppermute x3, starting transfers between devices, body(): part = lax.ppermute(part, 'x', around(-SHIFTS[g]))  9.93 us
  transfers between devices with their start and end apart: 7, of which 4 were waited for; matrix products, arithmetic and copies ran while one was open for 0% of the time, Pallas kernels for 8%

profile of v11, /device:TPU:1, one launch (start us, length us, event | category | flops | bytes accessed | tf_op | source)
XLA Modules:
  0.0 163.2 jit_solution(1375928046873023803)
XLA Ops:
  0.0 0.9 repeat.1
  0.9 26.8 %all_to_all.20.refs_3_ = bf16[8,256,128]{2,1,0:T(8,128)(2,1)S(1)} all-to-all(bf16[8,256,128]{2,1,0:T(8,128)(2,1)S(1)} %repeat.1), channel_id=1, replica_groups=mesh['z'=8,'x'=4,'y'=8,'core'=2] {'z'}, dimensions={0} | all-to-all | bytes 1048576 | tf_op jit(solution)/shard_map/all_to_all | solution.py:273
  27.7 4.6 %collective-permute-start.2 = (bf16[8,256,128]{2,1,0:T(8,128)(2,1)S(1)}, bf16[8,256,128]{2,1,0:T(8,128)(2,1)S(1)}, u32[]{:S(2)}, u32[]{:S(2)}) collective-permute-start(bf16[8,256,128]{2,1,0:T(8,128)(2,1)S(1)} %all_to_all.20.refs_3_), channel_id=1, source_target_pairs={{0,32},{16,48},{32,0},{48,16},{1,33},{17,49},{33,1},{49,17},{2,34}... | collective-permute-start | bytes 1572872 | tf_op jit(solution)/shard_map/ppermute | solution.py:276
  32.3 2.2 %collective-permute-start = (bf16[8,256,128]{2,1,0:T(8,128)(2,1)S(1)}, bf16[8,256,128]{2,1,0:T(8,128)(2,1)S(1)}, u32[]{:S(2)}, u32[]{:S(2)}) collective-permute-start(bf16[8,256,128]{2,1,0:T(8,128)(2,1)S(1)} %all_to_all.20.refs_3_), channel_id=1, source_target_pairs={{0,16},{16,32},{32,48},{48,0},{1,17},{17,33},{33,49},{49,1},{2,18}... | collective-permute-start | bytes 1572872 | tf_op jit(solution)/shard_map/ppermute | solution.py:276
  34.6 4.3 %collective-permute-start.1 = (bf16[8,256,128]{2,1,0:T(8,128)(2,1)S(1)}, bf16[8,256,128]{2,1,0:T(8,128)(2,1)S(1)}, u32[]{:S(2)}, u32[]{:S(2)}) collective-permute-start(bf16[8,256,128]{2,1,0:T(8,128)(2,1)S(1)} %all_to_all.20.refs_3_), channel_id=1, source_target_pairs={{0,48},{16,0},{32,16},{48,32},{1,49},{17,1},{33,17},{49,33},{2,50}... | collective-permute-start | bytes 1572872 | tf_op jit(solution)/shard_map/ppermute | solution.py:276
  38.8 0.0 copy-start.1
  38.8 0.7 copy-done.1
  39.6 0.0 copy-start.2
  39.6 0.7 copy-done.2
  40.3 2.2 %bucket.1 = f32[32,8,128]{2,1,0:T(8,128)} custom-call(s32[16,256]{1,0:T(8,128)S(1)} %bitcast.7, f32[16,256]{1,0:T(8,128)S(1)} %bitcast.8), custom_call_target="tpu_custom_call" | custom-call | tf_op jit(solution)/shard_map/bucket/pallas_call | solution.py:277
  42.5 3.9 %all-to-all-start = ((f32[32,8,128]{2,1,0:T(8,128)}), f32[32,8,128]{2,1,0:T(8,128)S(1)}, u32[]{:S(2)}, u32[]{:S(2)}) async-start(f32[32,8,128]{2,1,0:T(8,128)} %bucket.1), calls=%async_computation | async-start | bytes 262144 | tf_op jit(solution)/shard_map/all_to_all | solution.py:290
  46.4 10.8 %all-to-all-done = f32[32,8,128]{2,1,0:T(8,128)S(1)} async-done(((f32[32,8,128]{2,1,0:T(8,128)}), f32[32,8,128]{2,1,0:T(8,128)S(1)}, u32[]{:S(2)}, u32[]{:S(2)}) %all-to-all-start) | async-done | bytes 131104 | tf_op jit(solution)/shard_map/all_to_all | solution.py:290
  57.2 0.7 shift-right-arithmetic_add_fusion
  58.0 7.4 %pick.1 = (s32[32]{0:T(128)S(1)}, s32[96,128]{1,0:T(8,128)S(1)}, f32[96,128]{1,0:T(8,128)S(1)}, bf16[96,128,128]{2,1,0:T(8,128)(2,1)S(1)}, bf16[96,128,128]{2,1,0:T(8,128)(2,1)S(1)}) custom-call(s32[1]{0:T(128)} %bitcast.x_ref, s32[96,128]{1,0:T(8,128)S(1)} %reshape.28.rows_ref, s32[32]{0:T(128)S(1)} %get-tuple-element.16.count_ref, ...), custom_call_target="tpu_custom_call" | custom-call | tf_op jit(solution)/shard_map/pick/pallas_call | solution.py:299
  65.4 0.0 copy-start
  65.4 1.7 %copy-done = bf16[96,128,128]{2,1,0:T(8,128)(2,1)} copy-done((bf16[96,128,128]{2,1,0:T(8,128)(2,1)}, bf16[96,128,128]{2,1,0:T(8,128)(2,1)S(1)}, u32[]{:S(2)}) %copy-start) | copy-done | bytes 3145752
  67.0 0.0 collective-permute-done.2.refs_4_
  67.0 1.4 score.2.refs_5_
  68.5 0.0 collective-permute-done.refs_3_
  68.5 0.0 collective-permute-done.1.refs_4_
  68.5 1.5 score.3
  70.0 22.5 %all-gather = f32[1536,128]{1,0:T(8,128)S(1)} all-gather(f32[96,128]{1,0:T(8,128)S(1)} %score.3), channel_id=2, replica_groups=mesh['z'=8,'x'=4,'y'=8,'core'=2] {'y','core'}, dimensions={0}, use_global_device_ids=true | all-gather | bytes 835584 | tf_op jit(solution)/shard_map/all_gather | solution.py:341
  92.5 0.1 fusion.3.refs_2_
  92.6 1.9 %combine.4 = bf16[8,256,128]{2,1,0:T(8,128)(2,1)S(1)} custom-call(s32[32]{0:T(128)S(1)} %get-tuple-element.10.refs_0_, s32[96,128]{1,0:T(8,128)S(1)} %get-tuple-element.11.refs_1_, f32[96,128]{1,0:T(8,128)S(1)} %fusion.3.refs_2_, bf16[96,128,128]{2,1,0:T(8,128)(2,1)} %copy-done), custom_call_target="tpu_custom_call" | custom-call | tf_op jit(solution)/shard_map/combine/pallas_call | solution.py:345
  94.6 1.9 %combine.5 = bf16[8,256,128]{2,1,0:T(8,128)(2,1)S(1)} custom-call(s32[32]{0:T(128)S(1)} %get-tuple-element.10.refs_0_, s32[96,128]{1,0:T(8,128)S(1)} %get-tuple-element.11.refs_1_, f32[96,128]{1,0:T(8,128)S(1)} %fusion.3.refs_2_, bf16[96,128,128]{2,1,0:T(8,128)(2,1)} %copy-done), custom_call_target="tpu_custom_call" | custom-call | tf_op jit(solution)/shard_map/combine/pallas_call | solution.py:345
  96.5 1.9 %combine.6 = bf16[8,256,128]{2,1,0:T(8,128)(2,1)S(1)} custom-call(s32[32]{0:T(128)S(1)} %get-tuple-element.10.refs_0_, s32[96,128]{1,0:T(8,128)S(1)} %get-tuple-element.11.refs_1_, f32[96,128]{1,0:T(8,128)S(1)} %fusion.3.refs_2_, bf16[96,128,128]{2,1,0:T(8,128)(2,1)} %copy-done), custom_call_target="tpu_custom_call" | custom-call | tf_op jit(solution)/shard_map/combine/pallas_call | solution.py:345
  98.5 2.8 %collective-permute-start.3 = (bf16[8,256,128]{2,1,0:T(8,128)(2,1)S(1)}, bf16[8,256,128]{2,1,0:T(8,128)(2,1)S(1)}, u32[]{:S(2)}, u32[]{:S(2)}) collective-permute-start(bf16[8,256,128]{2,1,0:T(8,128)(2,1)S(1)} %combine.4), channel_id=1, source_target_pairs={{0,32},{16,48},{32,0},{48,16},{1,33},{17,49},{33,1},{49,17},{2,34}... | collective-permute-start | bytes 1572872 | tf_op jit(solution)/shard_map/ppermute | solution.py:366
  101.3 5.2 %collective-permute-start.4 = (bf16[8,256,128]{2,1,0:T(8,128)(2,1)S(1)}, bf16[8,256,128]{2,1,0:T(8,128)(2,1)S(1)}, u32[]{:S(2)}, u32[]{:S(2)}) collective-permute-start(bf16[8,256,128]{2,1,0:T(8,128)(2,1)S(1)} %combine.5), channel_id=1, source_target_pairs={{0,48},{16,0},{32,16},{48,32},{1,49},{17,1},{33,17},{49,33},{2,50}... | collective-permute-start | bytes 1572872 | tf_op jit(solution)/shard_map/ppermute | solution.py:366
  106.5 1.9 %collective-permute-start.5 = (bf16[8,256,128]{2,1,0:T(8,128)(2,1)S(1)}, bf16[8,256,128]{2,1,0:T(8,128)(2,1)S(1)}, u32[]{:S(2)}, u32[]{:S(2)}) collective-permute-start(bf16[8,256,128]{2,1,0:T(8,128)(2,1)S(1)} %combine.6), channel_id=1, source_target_pairs={{0,16},{16,32},{32,48},{48,0},{1,17},{17,33},{33,49},{49,1},{2,18}... | collective-permute-start | bytes 1572872 | tf_op jit(solution)/shard_map/ppermute | solution.py:366
  108.4 1.9 %combine.7 = bf16[8,256,128]{2,1,0:T(8,128)(2,1)S(1)} custom-call(s32[32]{0:T(128)S(1)} %get-tuple-element.10.refs_0_, s32[96,128]{1,0:T(8,128)S(1)} %get-tuple-element.11.refs_1_, f32[96,128]{1,0:T(8,128)S(1)} %fusion.3.refs_2_, bf16[96,128,128]{2,1,0:T(8,128)(2,1)} %copy-done), custom_call_target="tpu_custom_call" | custom-call | tf_op jit(solution)/shard_map/combine/pallas_call | solution.py:345
  110.4 0.0 copy-start.3
  110.4 4.9 %collective-permute-done.3 = bf16[8,256,128]{2,1,0:T(8,128)(2,1)S(1)} collective-permute-done((bf16[8,256,128]{2,1,0:T(8,128)(2,1)S(1)}, bf16[8,256,128]{2,1,0:T(8,128)(2,1)S(1)}, u32[]{:S(2)}, u32[]{:S(2)}) %collective-permute-start.3) | collective-permute-done | bytes 524320 | tf_op jit(solution)/shard_map/ppermute | solution.py:366
  115.2 10.9 %collective-permute-done.4 = bf16[8,256,128]{2,1,0:T(8,128)(2,1)S(1)} collective-permute-done((bf16[8,256,128]{2,1,0:T(8,128)(2,1)S(1)}, bf16[8,256,128]{2,1,0:T(8,128)(2,1)S(1)}, u32[]{:S(2)}, u32[]{:S(2)}) %collective-permute-start.4) | collective-permute-done | bytes 524320 | tf_op jit(solution)/shard_map/ppermute | solution.py:366
  126.1 0.9 collective-permute-done.5
  127.0 0.3 add_convert_fusion
  127.2 21.4 %all_to_all.21 = bf16[8,256,128]{2,1,0:T(8,128)(2,1)S(1)} all-to-all(bf16[8,256,128]{2,1,0:T(8,128)(2,1)S(1)} %add_convert_fusion), channel_id=1, replica_groups=mesh['z'=8,'x'=4,'y'=8,'core'=2] {'z'}, dimensions={0} | all-to-all | bytes 1048576 | tf_op jit(solution)/shard_map/all_to_all | solution.py:369
  148.7 0.1 convert_reduce_fusion
  148.7 0.1 multiply_reduce_fusion
  148.9 13.5 %all_to_all.22 = f32[16,2,128]{2,1,0:T(2,128)S(1)} all-to-all(f32[16,2,128]{2,1,0:T(2,128)S(1)} %broadcast_in_dim.12), channel_id=1, replica_groups=mesh['z'=8,'x'=4,'y'=8,'core'=2] {'y','core'}, dimensions={0} | all-to-all | bytes 32768 | tf_op jit(solution)/shard_map/all_to_all | solution.py:245
  162.4 0.0 copy-done.3
  162.4 0.7 multiply_convert_fusion
  (8 shorter events, 0.2 us)
Async XLA Ops:
  27.7 39.4 %collective-permute-start.2 = (bf16[8,256,128]{2,1,0:T(8,128)(2,1)S(1)}, bf16[8,256,128]{2,1,0:T(8,128)(2,1)S(1)}, u32[]{:S(2)}, u32[]{:S(2)}) collective-permute-start(bf16[8,256,128]{2,1,0:T(8,128)(2,1)S(1)} %all_to_all.20.refs_3_), channel_id=1, source_target_pairs={{0,32},{16,48},{32,0},{48,16},{1,33},{17,49},{33,1},{49,17},{2,34}... | collective-permute-start | bytes 1572872 | tf_op jit(solution)/shard_map/ppermute | solution.py:276
  32.3 36.2 %collective-permute-start = (bf16[8,256,128]{2,1,0:T(8,128)(2,1)S(1)}, bf16[8,256,128]{2,1,0:T(8,128)(2,1)S(1)}, u32[]{:S(2)}, u32[]{:S(2)}) collective-permute-start(bf16[8,256,128]{2,1,0:T(8,128)(2,1)S(1)} %all_to_all.20.refs_3_), channel_id=1, source_target_pairs={{0,16},{16,32},{32,48},{48,0},{1,17},{17,33},{33,49},{49,1},{2,18}... | collective-permute-start | bytes 1572872 | tf_op jit(solution)/shard_map/ppermute | solution.py:276
  34.6 33.9 %collective-permute-start.1 = (bf16[8,256,128]{2,1,0:T(8,128)(2,1)S(1)}, bf16[8,256,128]{2,1,0:T(8,128)(2,1)S(1)}, u32[]{:S(2)}, u32[]{:S(2)}) collective-permute-start(bf16[8,256,128]{2,1,0:T(8,128)(2,1)S(1)} %all_to_all.20.refs_3_), channel_id=1, source_target_pairs={{0,48},{16,0},{32,16},{48,32},{1,49},{17,1},{33,17},{49,33},{2,50}... | collective-permute-start | bytes 1572872 | tf_op jit(solution)/shard_map/ppermute | solution.py:276
  38.8 0.7 copy-start.1
  39.6 0.7 copy-start.2
  42.5 14.7 %all-to-all-start = ((f32[32,8,128]{2,1,0:T(8,128)}), f32[32,8,128]{2,1,0:T(8,128)S(1)}, u32[]{:S(2)}, u32[]{:S(2)}) async-start(f32[32,8,128]{2,1,0:T(8,128)} %bucket.1), calls=%async_computation | async-start | bytes 262144 | tf_op jit(solution)/shard_map/all_to_all | solution.py:290
  65.4 1.7 %copy-start = (bf16[96,128,128]{2,1,0:T(8,128)(2,1)}, bf16[96,128,128]{2,1,0:T(8,128)(2,1)S(1)}, u32[]{:S(2)}) copy-start(bf16[96,128,128]{2,1,0:T(8,128)(2,1)S(1)} %get-tuple-element.14.refs_3_) | copy-start | bytes 9437188
  98.5 16.8 %collective-permute-start.3 = (bf16[8,256,128]{2,1,0:T(8,128)(2,1)S(1)}, bf16[8,256,128]{2,1,0:T(8,128)(2,1)S(1)}, u32[]{:S(2)}, u32[]{:S(2)}) collective-permute-start(bf16[8,256,128]{2,1,0:T(8,128)(2,1)S(1)} %combine.4), channel_id=1, source_target_pairs={{0,32},{16,48},{32,0},{48,16},{1,33},{17,49},{33,1},{49,17},{2,34}... | collective-permute-start | bytes 1572872 | tf_op jit(solution)/shard_map/ppermute | solution.py:366
  101.3 24.8 %collective-permute-start.4 = (bf16[8,256,128]{2,1,0:T(8,128)(2,1)S(1)}, bf16[8,256,128]{2,1,0:T(8,128)(2,1)S(1)}, u32[]{:S(2)}, u32[]{:S(2)}) collective-permute-start(bf16[8,256,128]{2,1,0:T(8,128)(2,1)S(1)} %combine.5), channel_id=1, source_target_pairs={{0,48},{16,0},{32,16},{48,32},{1,49},{17,1},{33,17},{49,33},{2,50}... | collective-permute-start | bytes 1572872 | tf_op jit(solution)/shard_map/ppermute | solution.py:366
  106.5 20.5 %collective-permute-start.5 = (bf16[8,256,128]{2,1,0:T(8,128)(2,1)S(1)}, bf16[8,256,128]{2,1,0:T(8,128)(2,1)S(1)}, u32[]{:S(2)}, u32[]{:S(2)}) collective-permute-start(bf16[8,256,128]{2,1,0:T(8,128)(2,1)S(1)} %combine.6), channel_id=1, source_target_pairs={{0,16},{16,32},{32,48},{48,0},{1,17},{17,33},{33,49},{49,1},{2,18}... | collective-permute-start | bytes 1572872 | tf_op jit(solution)/shard_map/ppermute | solution.py:366
  110.4 52.0 %copy-start.3 = (f32[128]{0:T(128)S(1)}, f32[128]{0:T(128)}, u32[]{:S(2)}) copy-start(f32[128]{0:T(128)} %param.11) | copy-start | bytes 1540
